TPU v7x, 32 devices: a whole 2x2x4 slice. The times are simulated.
32 devices in a mesh: ep: 8 (over z, core), tp: 4 (over y, x).
Axes of the slice: x: 2, y: 2, z: 4, core: 2. Of those that a mesh axis runs over, the one named last changes fastest.
Arguments:
- query_pairs: bfloat16 [3072, 2048], P('ep', 'tp'), may hold values from -64 to 64
- key_pairs: bfloat16 [3072, 2048], P('ep', 'tp'), may hold values from -64 to 64
- value_rows: bfloat16 [3072, 2048], P('ep', 'tp'), may hold values from -6 to 6
- head_lambda: float32 [16], P('tp'), may hold values from 0.3 to 0.8
- head_gain: float32 [128], replicated, may hold values from 0.1 to 1.9
- out_weight: bfloat16 [2048, 2048], P('tp'), may hold values from -0.1875 to 0.1875
- moe_input: bfloat16 [1280, 2048], P('ep'), may hold values from -6 to 6
- ffn_gain: float32 [2048], replicated, may hold values from 0.1 to 1.9
- routes: int32 [1280, 2], P('ep'), may hold values from 0 to 7, all different within a row; in each aligned block of 160 rows (0 to 159, 160 to 319, ...) at most 50 rows name the same one
- route_weight: float32 [1280, 2], P('ep'), may hold values from 0.25 to 2.5
- gate_weight: bfloat16 [8, 2048, 2048], P('ep', None, 'tp'), may hold values from -0.125 to 0.125
- up_weight: bfloat16 [8, 2048, 2048], P('ep', None, 'tp'), may hold values from -0.125 to 0.125
- down_weight: bfloat16 [8, 2048, 2048], P('ep', 'tp'), may hold values from -0.1875 to 0.1875
- shared_gate: bfloat16 [2048, 2048], P(None, 'tp'), may hold values from -0.125 to 0.125
- shared_up: bfloat16 [2048, 2048], P(None, 'tp'), may hold values from -0.125 to 0.125
- shared_down: bfloat16 [2048, 2048], P('tp'), may hold values from -0.1875 to 0.1875
Outputs:
- attn_out: bfloat16 [3072, 2048], P('ep', 'tp')
- moe_out: bfloat16 [1280, 2048], P('ep', 'tp')
Inputs may be any that keep to these rules, and one draw needn't show every extreme that they name: `routes`: in each aligned block of 160 rows (the rows of one device along ep) no expert is named more than 50 times, a bound that some block reaches; a row names 2 different experts.
All inputs are finite; a program needn't handle non-finite values.
Results may differ from a plain program's by a relative error of at most 0.017.
The roundings to bfloat16 on the way count: a program that leaves them out, or rounds other values in their place, can miss the bound.
Values may be sent and summed in bfloat16 or wider, within the bound.
No kernel may reach another device: no remote copies, remote signals or barrier semaphores. Data moves between devices by JAX's collectives and lax.ppermute only.
A program may use at most 64 MiB of HBM per device.

v0:
```python
import math

import jax
import jax.numpy as jnp
from jax import lax
from jax.experimental import pallas as pl
from jax.experimental.pallas import tpu as pltpu
from jax.sharding import PartitionSpec as P


TOP_K = 2
KEY_BLOCK = 128

theta_base = 500000.0
norm_eps = 1e-06
masked_low = -1e30
LOG2E = 1.4426950408889634

VM = pl.BlockSpec(memory_space=pltpu.VMEM)
SM = pl.BlockSpec(memory_space=pltpu.SMEM)
ANY = pl.BlockSpec(memory_space=pl.ANY)


def sds(shape, dtype=jnp.bfloat16):
    return jax.ShapeDtypeStruct(shape, dtype)


def limit(mib):
    return pltpu.CompilerParams(vmem_limit_bytes=mib * 1024 * 1024)


def cost(flops):
    return pl.CostEstimate(flops=int(flops), bytes_accessed=0, transcendentals=0)


def place():
    ei = lax.axis_index("ep")
    return ei // 2, ei % 2, lax.axis_index("tp")


def column(row):
    n = row.shape[1]
    at = lax.broadcasted_iota(jnp.int32, (n, n), 0)
    diagonal = at == lax.broadcasted_iota(jnp.int32, (n, n), 1)
    return jnp.sum(jnp.where(diagonal, row, jnp.zeros_like(row)), axis=1, keepdims=True)


def dispatch_kernel(rows, gain, routes, xn_out, slots_out, *parts, cap, experts):
    z, core, ti = place()
    tokens = rows.shape[0]
    values = rows[...].astype(jnp.float32)
    inverse = lax.rsqrt(jnp.mean(values * values, axis=-1, keepdims=True) + norm_eps)
    xn_out[...] = (values * inverse * gain[...]).astype(jnp.bfloat16)
    group = 2 * cap
    t_row = lax.broadcasted_iota(jnp.int32, (tokens, tokens), 0)
    t_col = lax.broadcasted_iota(jnp.int32, (tokens, tokens), 1)
    e_row = lax.broadcasted_iota(jnp.int32, (experts, tokens), 0)
    before = (t_row < t_col).astype(jnp.float32).astype(jnp.bfloat16)
    hits = [(e_row == routes[k : k + 1, :]).astype(jnp.float32) for k in range(TOP_K)]
    count = jnp.dot(sum(hits).astype(jnp.bfloat16), before, preferred_element_type=jnp.float32)
    slots = []
    for k in range(TOP_K):
        expert = routes[k : k + 1, :]
        rank = jnp.sum(count * hits[k], axis=0, keepdims=True).astype(jnp.int32)
        slots.append(((expert // 2) ^ z) * group + ((expert % 2) ^ core) * cap + rank)
        slots_out[k : k + 1, :] = slots[k]
    width = parts[0].shape[1]
    mine = xn_out[:, pl.ds(pl.multiple_of(ti * width, width), width)]
    for s, part in enumerate(parts):
        slot_row = lax.broadcasted_iota(jnp.int32, (group, tokens), 0) + s * group
        pick = slot_row == slots[0]
        for k in range(1, TOP_K):
            pick = pick | (slot_row == slots[k])
        pick = pick.astype(jnp.float32).astype(jnp.bfloat16)
        part[...] = jnp.dot(pick, mine, preferred_element_type=jnp.float32).astype(jnp.bfloat16)


def expert_kernel(*refs, pieces, outs):
    ti = place()[2]
    xs, (gate_w, up_w, down_w), ys = refs[:pieces], refs[pieces : pieces + 3], refs[pieces + 3 :]
    width = xs[0].shape[1]
    gate = up = None
    for s in range(pieces):
        if pieces == 1:
            wg, wu = gate_w[...], up_w[...]
        else:
            at = pl.ds(pl.multiple_of((ti ^ s) * width, width), width)
            wg, wu = gate_w[at, :], up_w[at, :]
        x = xs[s][...]
        g = jnp.dot(x, wg, preferred_element_type=jnp.float32)
        u = jnp.dot(x, wu, preferred_element_type=jnp.float32)
        gate = g if gate is None else gate + g
        up = u if up is None else up + u
    hidden = (gate / (1.0 + jnp.exp(-gate)) * up).astype(jnp.bfloat16)
    cols = ys[0].shape[1]
    for s in range(outs):
        at = pl.ds(pl.multiple_of((ti ^ s) * cols, cols), cols)
        ys[s][...] = jnp.dot(hidden, down_w[:, at], preferred_element_type=jnp.float32).astype(
            jnp.bfloat16
        )


def run_expert(xs, gate_w, up_w, down_w, tp):
    rows = xs[0].shape[0]
    width, hidden = gate_w.shape
    cols = down_w.shape[1] // tp
    return pl.pallas_call(
        lambda *refs: expert_kernel(*refs, pieces=len(xs), outs=tp),
        out_shape=[sds((rows, cols))] * tp,
        in_specs=[VM] * (len(xs) + 3),
        out_specs=[VM] * tp,
        cost_estimate=cost(6 * rows * width * hidden),
        compiler_params=limit(24),
    )(*xs, gate_w, up_w, down_w)


def combine_kernel(slots, weights, *refs, count):
    back, shared, out = refs[:count], refs[count:-1], refs[-1]
    tokens = slots.shape[1]
    own = [column(slots[k : k + 1, :]) for k in range(TOP_K)]
    scale = [column(weights[k : k + 1, :]) for k in range(TOP_K)]
    group = back[0].shape[0]
    total = None
    for part in shared:
        part = part[...].astype(jnp.float32)
        total = part if total is None else total + part
    picked = [None] * TOP_K
    for s in range(count):
        slot_col = lax.broadcasted_iota(jnp.int32, (tokens, group), 1) + s * group
        rows = back[s][...]
        for k in range(TOP_K):
            pick = (slot_col == own[k]).astype(jnp.float32).astype(jnp.bfloat16)
            term = jnp.dot(pick, rows, preferred_element_type=jnp.float32)
            picked[k] = term if picked[k] is None else picked[k] + term
    routed = scale[0] * picked[0]
    for k in range(1, TOP_K):
        routed = routed + scale[k] * picked[k]
    out[...] = (routed + total).astype(jnp.bfloat16)


def rope_kernel(q, k, v, cosine, sine, *outs, size):
    z = place()[0]
    rows = q.shape[0]
    both = cosine.shape[1]
    half = size // 2
    lane = lax.broadcasted_iota(jnp.int32, (rows, both), 1)
    front = (lane % size) < half
    c, s_ = cosine[...], sine[...]
    for s, out in enumerate(outs):
        at = pl.ds(pl.multiple_of((z ^ s) * both, both), both)
        for n, ref in enumerate((q, k)):
            x = ref[:, at].astype(jnp.float32)
            turned = jnp.where(front, pltpu.roll(x, both - half, 1), pltpu.roll(x, half, 1))
            out[n * rows : (n + 1) * rows, :] = (x * c + turned * s_).astype(jnp.bfloat16)
        out[2 * rows : 3 * rows, :] = v[:, at]


def attend_kernel(lam, gain, *refs, count, rows, size):
    own, other = refs[:count], refs[count]
    outs = refs[count + 1 : 2 * count + 1]
    qs, ks, vs, scores, weights, heads, sems = refs[2 * count + 1 :]
    z, core, _ = place()
    both = 2 * size
    value = vs.shape[1] // 2
    keys = 2 * rows
    copies = []
    for s in range(count):
        at = pl.multiple_of((z ^ s) * rows, rows)
        mine = pl.multiple_of((2 * (z ^ s) + core) * rows, rows)
        theirs = pl.multiple_of((2 * (z ^ s) + 1 - core) * rows, rows)
        pairs = (
            (own[s].at[pl.ds(0, rows), :], qs.at[pl.ds(at, rows), :]),
            (own[s].at[pl.ds(rows, rows), :], ks.at[pl.ds(mine, rows), :]),
            (own[s].at[pl.ds(2 * rows, rows), :], vs.at[pl.ds(mine, rows), pl.ds(0, value)]),
            (other.at[pl.ds(2 * s * rows, rows), :], ks.at[pl.ds(theirs, rows), :]),
            (
                other.at[pl.ds((2 * s + 1) * rows, rows), :],
                vs.at[pl.ds(theirs, rows), pl.ds(0, value)],
            ),
        )
        for n, (src, dst) in enumerate(pairs):
            copy = pltpu.make_async_copy(src, dst, sems.at[5 * s + n])
            copy.start()
            copies.append(copy)
    vs[:, value:] = jnp.ones((vs.shape[0], value), jnp.bfloat16)
    for copy in copies:
        copy.wait()
    factor = LOG2E * size ** (-0.5)
    lane = lax.broadcasted_iota(jnp.int32, (rows, both), 1)
    tile = math.gcd(rows, 64)
    ahead = lax.broadcasted_iota(jnp.int32, (tile, keys), 1) - lax.broadcasted_iota(
        jnp.int32, (tile, keys), 0
    )
    contract = (((1,), (1,)), ((), ()))
    units = [(block, m) for block in reversed(range(count)) for m in range(2)]
    maps = {}

    def score(u):
        block, m = units[u]
        q = qs[block * rows : (block + 1) * rows, :]
        q = jnp.where((lane < size) == (m == 0), q, jnp.zeros_like(q))
        for j in range(block + 1):
            at = slice(j * keys, (j + 1) * keys)
            scores[u % 2, :, at] = lax.dot_general(
                q, ks[at, :], contract, preferred_element_type=jnp.float32
            )

    def weigh(u):
        block, _ = units[u]
        for r in range(0, rows, tile):
            pieces = []
            for j in range(block + 1):
                piece = scores[u % 2, r : r + tile, j * keys : (j + 1) * keys]
                if j == block:
                    piece = jnp.where(ahead <= core * rows + r, piece, masked_low)
                pieces.append(piece)
            top = None
            for piece in pieces:
                one = jnp.max(piece, axis=1, keepdims=True)
                top = one if top is None else jnp.maximum(top, one)
            for j, piece in enumerate(pieces):
                weights[u % 2, r : r + tile, j * keys : (j + 1) * keys] = jnp.exp2(
                    (piece - top) * factor
                ).astype(jnp.bfloat16)

    def mix(u):
        block, m = units[u]
        span = (block + 1) * keys
        acc = jnp.dot(weights[u % 2, :, :span], vs[:span, :], preferred_element_type=jnp.float32)
        maps[m] = acc[:, :value] / acc[:, value:]
        if m == 1:
            diff = maps[0] - lam[z] * maps[1]
            inverse = lax.rsqrt(jnp.mean(diff * diff, axis=1, keepdims=True) + norm_eps)
            heads[block * rows : (block + 1) * rows, :] = (diff * inverse * gain[...]).astype(
                jnp.bfloat16
            )

    score(0)
    for u in range(len(units)):
        if u + 1 < len(units):
            score(u + 1)
        if u > 0:
            mix(u - 1)
        weigh(u)
    mix(len(units) - 1)
    for s in range(count):
        outs[s][...] = heads[pl.ds(pl.multiple_of((z ^ s) * rows, rows), rows), :]


def project_kernel(*refs, count, tp):
    heads, weight, outs, rows_ref = refs[:count], refs[count], refs[count + 1 : -1], refs[-1]
    z, _, ti = place()
    value = heads[0].shape[1]
    for s in range(count):
        rows_ref[:, pl.ds(pl.multiple_of((z ^ s) * value, value), value)] = heads[s][...]
    rows = rows_ref[...]
    cols = outs[0].shape[1]
    for s in range(tp):
        at = pl.ds(pl.multiple_of((ti ^ s) * cols, cols), cols)
        outs[s][...] = jnp.dot(rows, weight[:, at], preferred_element_type=jnp.float32).astype(
            jnp.bfloat16
        )


def rotate(inputs, positions):
    half_size = inputs.shape[-1] // 2
    frequency = theta_base ** (-(jnp.arange(half_size, dtype=jnp.float32) * 2.0) / inputs.shape[-1])
    angles = positions.astype(jnp.float32)[:, None] * frequency[None, :]
    cosine = jnp.cos(angles)[:, None, None, :]
    sine_part = jnp.sin(angles)[:, None, None, :]
    front_half = inputs[..., :half_size]
    back_half = inputs[..., half_size:]
    return jnp.concatenate(
        [front_half * cosine - back_half * sine_part, back_half * cosine + front_half * sine_part],
        axis=-1,
    )


def gathered_attention(query_pairs, key_pairs, value_rows, head_lambda, head_gain):
    local_rows = query_pairs.shape[0]
    local_heads = head_lambda.shape[0]
    head_size = query_pairs.shape[1] // (2 * local_heads)
    value_size = value_rows.shape[1] // local_heads
    positions = lax.axis_index("ep") * local_rows + jnp.arange(local_rows, dtype=jnp.int32)
    rot_queries = rotate(
        query_pairs.astype(jnp.float32).reshape(local_rows, local_heads, 2, head_size), positions
    ).astype(jnp.bfloat16)
    rot_keys = rotate(
        key_pairs.astype(jnp.float32).reshape(local_rows, local_heads, 2, head_size), positions
    ).astype(jnp.bfloat16)
    rot_keys = rot_keys.reshape(local_rows, local_heads * 2 * head_size)
    zero_init = (
        jnp.full((local_heads, 2, local_rows), masked_low, jnp.float32),
        jnp.zeros((local_heads, 2, local_rows), jnp.float32),
        jnp.zeros((local_heads, 2, local_rows, value_size), jnp.float32),
    )
    piece_keys = lax.all_gather(rot_keys, "ep", axis=0, tiled=True)
    piece_values = lax.all_gather(value_rows, "ep", axis=0, tiled=True)
    block_count = piece_keys.shape[0] // KEY_BLOCK
    group_size = 4 if block_count % 4 == 0 else 1
    group_count = block_count // group_size
    grouped_keys = piece_keys.reshape(group_count, group_size, KEY_BLOCK, local_heads, 2, head_size)
    grouped_values = piece_values.reshape(
        group_count, group_size, KEY_BLOCK, local_heads, value_size
    )

    def one_group(current, inputs):
        block_keys, block_values, group_index = inputs
        key_positions = group_index * group_size * KEY_BLOCK + jnp.arange(
            group_size * KEY_BLOCK, dtype=jnp.int32
        ).reshape(group_size, KEY_BLOCK)
        scores = jnp.einsum(
            "qhmd,gkhmd->hmqgk", rot_queries, block_keys, preferred_element_type=jnp.float32
        ) * head_size ** (-0.5)
        allowed = key_positions[None, :, :] <= positions[:, None, None]
        scores = jnp.where(allowed, scores, masked_low)
        block_max = jnp.max(scores, axis=-1)
        weights = jnp.where(allowed, jnp.exp(scores - block_max[..., None]), 0.0)
        block_sum = jnp.sum(weights, axis=-1)
        block_out = jnp.einsum(
            "hmqgk,gkhc->hmqgc",
            weights.astype(jnp.bfloat16),
            block_values,
            preferred_element_type=jnp.float32,
        )
        run_max, run_sum, run_out = current
        new_max = jnp.maximum(run_max, jnp.max(block_max, axis=-1))
        old_scale = jnp.exp(run_max - new_max)
        new_scale = jnp.exp(block_max - new_max[..., None])
        run_sum = run_sum * old_scale + jnp.sum(new_scale * block_sum, axis=-1)
        run_out = run_out * old_scale[..., None] + jnp.sum(
            new_scale[..., None] * block_out, axis=-2
        )
        return ((new_max, run_sum, run_out), None)

    result, _ = lax.scan(
        one_group,
        zero_init,
        (grouped_keys, grouped_values, jnp.arange(group_count, dtype=jnp.int32)),
    )
    _, run_sum, run_out = result
    map_outputs = run_out / run_sum[..., None]
    difference = map_outputs[:, 0] - head_lambda[:, None, None] * map_outputs[:, 1]
    inverse_rms = lax.rsqrt(jnp.mean(difference * difference, axis=-1, keepdims=True) + norm_eps)
    normed_heads = (difference * inverse_rms * head_gain).astype(jnp.bfloat16)
    return [normed_heads.transpose(1, 0, 2).reshape(local_rows, local_heads * value_size)]


def inner(
    query_pairs,
    key_pairs,
    value_rows,
    head_lambda,
    head_gain,
    out_weight,
    moe_input,
    ffn_gain,
    routes,
    route_weight,
    gate_weight,
    up_weight,
    down_weight,
    shared_gate,
    shared_up,
    shared_down,
):
    ep, tp = lax.axis_size("ep"), lax.axis_size("tp")
    chips = ep // 2
    ei = lax.axis_index("ep")

    def along_z(x, s):
        return lax.ppermute(x, "ep", [(i, 2 * ((i // 2) ^ s) + i % 2) for i in range(ep)])

    def swap(x):
        return lax.ppermute(x, "ep", [(i, i ^ 1) for i in range(ep)])

    def along_tp(x, s):
        return lax.ppermute(x, "tp", [(i, i ^ s) for i in range(tp)])

    def exchange(parts, move):
        return [parts[0]] + [move(parts[s], s) for s in range(1, len(parts))]

    tokens, width = moe_input.shape
    cap = tokens * TOP_K * 5 // (4 * ep)
    slice_width = width // tp
    xn, slots, *parts = pl.pallas_call(
        lambda *refs: dispatch_kernel(*refs, cap=cap, experts=ep),
        out_shape=[sds((tokens, width)), sds((TOP_K, tokens), jnp.int32)]
        + [sds((2 * cap, slice_width))] * chips,
        in_specs=[VM] * 3,
        out_specs=[VM] * (2 + chips),
        cost_estimate=cost(4e8),
        name="dispatch",
        compiler_params=limit(8),
    )(moe_input, ffn_gain.reshape(1, -1), routes.T)
    arrived = exchange(parts, along_z)

    rows = query_pairs.shape[0]
    heads = head_lambda.shape[0]
    size = query_pairs.shape[1] // (2 * heads)
    value = value_rows.shape[1] // heads
    spread = heads == chips and value == 2 * size and value % 128 == 0
    if spread:
        positions = (ei * rows + jnp.arange(rows, dtype=jnp.int32)).astype(jnp.float32)
        index = jnp.arange(2 * size, dtype=jnp.int32)
        frequency = theta_base ** (-((index % (size // 2)).astype(jnp.float32) * 2.0) / size)
        angles = positions[:, None] * frequency[None, :]
        sign = jnp.where(index % size < size // 2, -1.0, 1.0).astype(jnp.float32)
        cosine = jnp.cos(angles)
        sine = jnp.sin(angles) * sign
        packs = pl.pallas_call(
            lambda *refs: rope_kernel(*refs, size=size),
            out_shape=[sds((3 * rows, value))] * chips,
            in_specs=[VM] * 5,
            out_specs=[VM] * chips,
            cost_estimate=cost(4e8),
            name="rope",
        compiler_params=limit(8),
        )(query_pairs, key_pairs, value_rows, cosine, sine)
        packs = exchange(packs, along_z)
        other = jnp.concatenate([p[rows:] for p in packs], axis=0)
        other = swap(other)

    shared = run_expert([xn], shared_gate, shared_up, shared_down, tp)
    shared = exchange(shared, along_tp)

    swapped = swap(jnp.concatenate([p[cap:] for p in arrived], axis=0))
    held = jnp.concatenate([p[:cap] for p in arrived] + [swapped], axis=0)
    slices = [held] + [along_tp(held, s) for s in range(1, tp)]
    terms = run_expert(slices, gate_weight[0], up_weight[0], down_weight[0], tp)
    terms = exchange(terms, along_tp)
    summed = sum(t.astype(jnp.float32) for t in terms).astype(jnp.bfloat16)

    if spread:
        heads_out = pl.pallas_call(
            lambda *refs: attend_kernel(*refs, count=chips, rows=rows, size=size),
            out_shape=[sds((rows, value))] * chips,
            in_specs=[SM, VM] + [ANY] * (chips + 1),
            out_specs=[VM] * chips,
            scratch_shapes=[
                pltpu.VMEM((chips * rows, value), jnp.bfloat16),
                pltpu.VMEM((ep * rows, value), jnp.bfloat16),
                pltpu.VMEM((ep * rows, 2 * value), jnp.bfloat16),
                pltpu.VMEM((2, rows, ep * rows), jnp.float32),
                pltpu.VMEM((2, rows, ep * rows), jnp.bfloat16),
                pltpu.VMEM((chips * rows, value), jnp.bfloat16),
                pltpu.SemaphoreType.DMA((5 * chips,)),
            ],
            cost_estimate=cost(4e9),
            name="attend",
        compiler_params=limit(32),
        )(head_lambda, head_gain.reshape(1, -1), *packs, other)
        normed = exchange(heads_out, along_z)
        mixer = pl.pallas_call(
            lambda *refs: project_kernel(*refs, count=chips, tp=tp),
            out_shape=[sds((rows, out_weight.shape[1] // tp))] * tp,
            in_specs=[VM] * (chips + 1),
            out_specs=[VM] * tp,
            scratch_shapes=[pltpu.VMEM((rows, chips * value), jnp.bfloat16)],
            cost_estimate=cost(1e9),
            name="project",
        compiler_params=limit(10),
        )(*normed, out_weight)
        mixer = exchange(mixer, along_tp)
        attn_out = sum(m.astype(jnp.float32) for m in mixer).astype(jnp.bfloat16)
    else:
        head_rows = gathered_attention(query_pairs, key_pairs, value_rows, head_lambda, head_gain)[0]
        mixer = jnp.dot(head_rows, out_weight, preferred_element_type=jnp.float32)
        attn_out = lax.psum_scatter(
            mixer.astype(jnp.bfloat16), "tp", scatter_dimension=1, tiled=True
        )

    half = chips * cap
    back = swap(summed[half:])
    groups = [
        jnp.concatenate([summed[s * cap : (s + 1) * cap], back[s * cap : (s + 1) * cap]], axis=0)
        for s in range(chips)
    ]
    groups = exchange(groups, along_z)
    moe_out = pl.pallas_call(
        lambda *refs: combine_kernel(*refs, count=chips),
        out_shape=sds((tokens, slice_width)),
        in_specs=[VM] * (2 + chips + tp),
        out_specs=VM,
        cost_estimate=cost(4e8),
        name="combine",
        compiler_params=limit(10),
    )(slots, route_weight.T, *groups, *shared)
    return (attn_out, moe_out)


def solution(mesh):
    return jax.shard_map(
        inner,
        mesh=mesh,
        in_specs=(
            P("ep", "tp"),
            P("ep", "tp"),
            P("ep", "tp"),
            P("tp"),
            P(),
            P("tp", None),
            P("ep", None),
            P(),
            P("ep", None),
            P("ep", None),
            P("ep", None, "tp"),
            P("ep", None, "tp"),
            P("ep", "tp", None),
            P(None, "tp"),
            P(None, "tp"),
            P("tp", None),
        ),
        out_specs=(P("ep", "tp"), P("ep", "tp")),
        check_vma=False,
    )
```

profile of v0, /device:TPU:0, one launch (start us, length us, event | category | flops | bytes accessed | tf_op | source)
XLA Modules:
  0.0 134.4 jit_solution(5086141601003822386)
XLA Ops:
  0.6 1.1 copy-done.10
  1.7 0.7 copy-done.11
  2.4 0.7 copy-done.12
  3.1 0.6 dispatch.1
  3.7 3.1 %collective-permute-start.10 = (bf16[100,512]{1,0:T(8,128)(2,1)S(1)}, bf16[100,512]{1,0:T(8,128)(2,1)S(1)}, u32[]{:S(2)}, u32[]{:S(2)}) collective-permute-start(bf16[100,512]{1,0:T(8,128)(2,1)S(1)} %get-tuple-element.42), channel_id=1, source_target_pairs={{0,8},{4,12},{8,0},{12,4},{16,24},{20,28},{24,16},{28,20},{1,9},{5... | collective-permute-start | bytes 307208 | tf_op jit(solution)/shard_map/ppermute | solution.py:372
  6.8 2.6 %collective-permute-start.11 = (bf16[100,512]{1,0:T(8,128)(2,1)S(1)}, bf16[100,512]{1,0:T(8,128)(2,1)S(1)}, u32[]{:S(2)}, u32[]{:S(2)}) collective-permute-start(bf16[100,512]{1,0:T(8,128)(2,1)S(1)} %get-tuple-element.43), channel_id=1, source_target_pairs={{0,16},{4,20},{8,24},{12,28},{16,0},{20,4},{24,8},{28,12},{1,17},{... | collective-permute-start | bytes 307208 | tf_op jit(solution)/shard_map/ppermute | solution.py:372
  9.4 0.0 collective-permute-start.12
  9.4 0.8 fusion
  10.2 0.0 copy-start.3
  10.2 1.0 copy-done.3
  11.2 1.0 copy-done.4
  12.2 1.0 copy-done.5
  13.2 0.7 rope.1
  13.9 1.0 collective-permute-start
  14.8 3.5 %collective-permute-start.1 = (bf16[1152,128]{1,0:T(8,128)(2,1)S(1)}, bf16[1152,128]{1,0:T(8,128)(2,1)S(1)}, u32[]{:S(2)}, u32[]{:S(2)}) collective-permute-start(bf16[1152,128]{1,0:T(8,128)(2,1)S(1)} %get-tuple-element.30), channel_id=1, source_target_pairs={{0,16},{4,20},{8,24},{12,28},{16,0},{20,4},{24,8},{28,12},{1,17},{... | collective-permute-start | bytes 884744 | tf_op jit(solution)/shard_map/ppermute | solution.py:372
  18.4 0.1 collective-permute-start.2
  18.5 0.0 collective-permute-done.11
  18.5 0.1 pad_maximum_fusion.1
  18.6 0.1 collective-permute-start.13
  18.7 9.9 %collective-permute-done.refs_3_ = bf16[1152,128]{1,0:T(8,128)(2,1)S(1)} collective-permute-done((bf16[1152,128]{1,0:T(8,128)(2,1)S(1)}, bf16[1152,128]{1,0:T(8,128)(2,1)S(1)}, u32[]{:S(2)}, u32[]{:S(2)}) %collective-permute-start) | collective-permute-done | bytes 294944 | tf_op jit(solution)/shard_map/ppermute | solution.py:372
  28.6 10.4 %collective-permute-done.1.refs_4_ = bf16[1152,128]{1,0:T(8,128)(2,1)S(1)} collective-permute-done((bf16[1152,128]{1,0:T(8,128)(2,1)S(1)}, bf16[1152,128]{1,0:T(8,128)(2,1)S(1)}, u32[]{:S(2)}, u32[]{:S(2)}) %collective-permute-start.1) | collective-permute-done | bytes 294944 | tf_op jit(solution)/shard_map/ppermute | solution.py:372
  39.1 0.0 collective-permute-done.2.refs_5_
  39.1 1.0 pad_maximum_fusion
  40.1 0.0 collective-permute-start.3
  40.1 0.6 concatenate.23.refs_0_
  40.7 1.6 %collective-permute-start.14 = (bf16[400,512]{1,0:T(8,128)(2,1)S(1)}, bf16[400,512]{1,0:T(8,128)(2,1)S(1)}, u32[]{:S(2)}, u32[]{:S(2)}) collective-permute-start(bf16[400,512]{1,0:T(8,128)(2,1)S(1)} %concatenate.23.refs_0_), channel_id=1, source_target_pairs={{0,1},{1,0},{2,3},{3,2},{4,5},{5,4},{6,7},{7,6},{8,9},{9,8},{10,11... | collective-permute-start | bytes 1228808 | tf_op jit(solution)/shard_map/ppermute | solution.py:378
  42.3 1.5 %collective-permute-start.15 = (bf16[400,512]{1,0:T(8,128)(2,1)S(1)}, bf16[400,512]{1,0:T(8,128)(2,1)S(1)}, u32[]{:S(2)}, u32[]{:S(2)}) collective-permute-start(bf16[400,512]{1,0:T(8,128)(2,1)S(1)} %concatenate.23.refs_0_), channel_id=1, source_target_pairs={{0,2},{1,3},{2,0},{3,1},{4,6},{5,7},{6,4},{7,5},{8,10},{9,11},{10,... | collective-permute-start | bytes 1228808 | tf_op jit(solution)/shard_map/ppermute | solution.py:378
  43.8 0.4 collective-permute-start.16
  44.3 8.8 %collective-permute-done.14.refs_1_ = bf16[400,512]{1,0:T(8,128)(2,1)S(1)} collective-permute-done((bf16[400,512]{1,0:T(8,128)(2,1)S(1)}, bf16[400,512]{1,0:T(8,128)(2,1)S(1)}, u32[]{:S(2)}, u32[]{:S(2)}) %collective-permute-start.14) | collective-permute-done | bytes 409632 | tf_op jit(solution)/shard_map/ppermute | solution.py:378
  53.1 9.6 %collective-permute-done.15.refs_2_ = bf16[400,512]{1,0:T(8,128)(2,1)S(1)} collective-permute-done((bf16[400,512]{1,0:T(8,128)(2,1)S(1)}, bf16[400,512]{1,0:T(8,128)(2,1)S(1)}, u32[]{:S(2)}, u32[]{:S(2)}) %collective-permute-start.15) | collective-permute-done | bytes 409632 | tf_op jit(solution)/shard_map/ppermute | solution.py:378
  62.7 0.0 collective-permute-done.16.refs_3_
  62.7 1.6 %copy-done.6 = bf16[1,2048,512]{2,1,0:T(8,128)(2,1)S(1)} copy-done((bf16[1,2048,512]{2,1,0:T(8,128)(2,1)S(1)}, bf16[1,2048,512]{2,1,0:T(8,128)(2,1)}, u32[]{:S(2)}) %copy-start.6) | copy-done | bytes 2097176
  64.3 1.6 %copy-done.7 = bf16[1,2048,512]{2,1,0:T(8,128)(2,1)S(1)} copy-done((bf16[1,2048,512]{2,1,0:T(8,128)(2,1)S(1)}, bf16[1,2048,512]{2,1,0:T(8,128)(2,1)}, u32[]{:S(2)}) %copy-start.7) | copy-done | bytes 2097176
  65.9 1.6 %copy-done.8 = bf16[1,512,2048]{2,1,0:T(8,128)(2,1)S(1)} copy-done((bf16[1,512,2048]{2,1,0:T(8,128)(2,1)S(1)}, bf16[1,512,2048]{2,1,0:T(8,128)(2,1)}, u32[]{:S(2)}) %copy-start.8) | copy-done | bytes 2097176
  67.5 2.8 %shard_map.167 = (bf16[400,512]{1,0:T(8,128)(2,1)S(1)}, bf16[400,512]{1,0:T(8,128)(2,1)S(1)}, bf16[400,512]{1,0:T(8,128)(2,1)S(1)}, bf16[400,512]{1,0:T(8,128)(2,1)S(1)}) custom-call(bf16[400,512]{1,0:T(8,128)(2,1)S(1)} %concatenate.23.refs_0_, bf16[400,512]{1,0:T(8,128)(2,1)S(1)} %collective-permute-done.14.refs_1_, ...), custom_call_target="tpu_custom_call" | custom-call | flops 2516582400 | tf_op jit(solution)/shard_map/pallas_call | solution.py:107
  70.2 1.3 collective-permute-start.17
  71.5 0.8 collective-permute-start.18
  72.4 1.4 %collective-permute-start.19 = (bf16[400,512]{1,0:T(8,128)(2,1)S(1)}, bf16[400,512]{1,0:T(8,128)(2,1)S(1)}, u32[]{:S(2)}, u32[]{:S(2)}) collective-permute-start(bf16[400,512]{1,0:T(8,128)(2,1)S(1)} %get-tuple-element.48), channel_id=1, source_target_pairs={{0,3},{1,2},{2,1},{3,0},{4,7},{5,6},{6,5},{7,4},{8,11},{9,10},{10,... | collective-permute-start | bytes 1228808 | tf_op jit(solution)/shard_map/ppermute | solution.py:378
  73.8 0.0 copy-start.15
  73.8 1.3 shard_map.168
  75.1 1.3 collective-permute-start.24
  76.4 10.4 %attend.1 = (bf16[384,128]{1,0:T(8,128)(2,1)S(1)}, bf16[384,128]{1,0:T(8,128)(2,1)S(1)}, bf16[384,128]{1,0:T(8,128)(2,1)S(1)}, bf16[384,128]{1,0:T(8,128)(2,1)S(1)}) custom-call(f32[4]{0:T(128)S(1)} %copy-done.14, f32[1,128]{1,0:T(1,128)S(1)} %bitcast.13, bf16[1152,128]{1,0:T(8,128)(2,1)S(1)} %get-tuple-element.28.refs_2_, ...), custom_call_target="tpu_custom_call" | custom-call | flops 4000000000 | tf_op jit(solution)/shard_map/attend/pallas_call | solution.py:435
  86.9 0.0 copy-start.9
  86.9 5.8 %collective-permute-start.4 = (bf16[384,128]{1,0:T(8,128)(2,1)S(1)}, bf16[384,128]{1,0:T(8,128)(2,1)S(1)}, u32[]{:S(2)}, u32[]{:S(2)}) collective-permute-start(bf16[384,128]{1,0:T(8,128)(2,1)S(1)} %get-tuple-element.33), channel_id=1, source_target_pairs={{0,8},{4,12},{8,0},{12,4},{16,24},{20,28},{24,16},{28,20},{1,9},{5... | collective-permute-start | bytes 294920 | tf_op jit(solution)/shard_map/ppermute | solution.py:372
  92.7 0.0 collective-permute-done.17
  92.7 1.1 collective-permute-start.5
  93.8 1.4 %collective-permute-start.6 = (bf16[384,128]{1,0:T(8,128)(2,1)S(1)}, bf16[384,128]{1,0:T(8,128)(2,1)S(1)}, u32[]{:S(2)}, u32[]{:S(2)}) collective-permute-start(bf16[384,128]{1,0:T(8,128)(2,1)S(1)} %get-tuple-element.35), channel_id=1, source_target_pairs={{0,24},{4,28},{8,16},{12,20},{16,8},{20,12},{24,0},{28,4},{1,25},{... | collective-permute-start | bytes 294920 | tf_op jit(solution)/shard_map/ppermute | solution.py:372
  95.2 0.2 add_convert_fusion
  95.5 0.1 collective-permute-start.20
  95.6 0.7 collective-permute-done.4.refs_1_
  96.3 0.7 collective-permute-start.25
  97.0 4.8 %collective-permute-done.5.refs_2_ = bf16[384,128]{1,0:T(8,128)(2,1)S(1)} collective-permute-done((bf16[384,128]{1,0:T(8,128)(2,1)S(1)}, bf16[384,128]{1,0:T(8,128)(2,1)S(1)}, u32[]{:S(2)}, u32[]{:S(2)}) %collective-permute-start.5) | collective-permute-done | bytes 98336 | tf_op jit(solution)/shard_map/ppermute | solution.py:372
  101.8 1.0 project.1
  102.8 0.7 collective-permute-start.7
  103.5 1.4 %collective-permute-start.8 = (bf16[384,512]{1,0:T(8,128)(2,1)S(1)}, bf16[384,512]{1,0:T(8,128)(2,1)S(1)}, u32[]{:S(2)}, u32[]{:S(2)}) collective-permute-start(bf16[384,512]{1,0:T(8,128)(2,1)S(1)} %get-tuple-element.38), channel_id=1, source_target_pairs={{0,2},{1,3},{2,0},{3,1},{4,6},{5,7},{6,4},{7,5},{8,10},{9,11},{10,... | collective-permute-start | bytes 1179656 | tf_op jit(solution)/shard_map/ppermute | solution.py:378
  104.9 1.5 %collective-permute-start.9 = (bf16[384,512]{1,0:T(8,128)(2,1)S(1)}, bf16[384,512]{1,0:T(8,128)(2,1)S(1)}, u32[]{:S(2)}, u32[]{:S(2)}) collective-permute-start(bf16[384,512]{1,0:T(8,128)(2,1)S(1)} %get-tuple-element.39), channel_id=1, source_target_pairs={{0,3},{1,2},{2,1},{3,0},{4,7},{5,6},{6,5},{7,4},{8,11},{9,10},{10,... | collective-permute-start | bytes 1179656 | tf_op jit(solution)/shard_map/ppermute | solution.py:378
  106.5 1.5 %collective-permute-start.26 = (bf16[160,512]{1,0:T(8,128)(2,1)S(1)}, bf16[160,512]{1,0:T(8,128)(2,1)S(1)}, u32[]{:S(2)}, u32[]{:S(2)}) collective-permute-start(bf16[160,512]{1,0:T(8,128)(2,1)S(1)} %get-tuple-element.53), channel_id=1, source_target_pairs={{0,3},{1,2},{2,1},{3,0},{4,7},{5,6},{6,5},{7,4},{8,11},{9,10},{10,... | collective-permute-start | bytes 491528 | tf_op jit(solution)/shard_map/ppermute | solution.py:378
  108.0 2.4 %collective-permute-start.23 = (bf16[100,512]{1,0:T(8,128)(2,1)S(1)}, bf16[100,512]{1,0:T(8,128)(2,1)S(1)}, u32[]{:S(2)}, u32[]{:S(2)}) collective-permute-start(bf16[100,512]{1,0:T(8,128)(2,1)S(1)} %pad_maximum_fusion.5), channel_id=1, source_target_pairs={{0,24},{4,28},{8,16},{12,20},{16,8},{20,12},{24,0},{28,4},{1,25},{... | collective-permute-start | bytes 307208 | tf_op jit(solution)/shard_map/ppermute | solution.py:372
  110.5 11.4 %collective-permute-done.26.refs_9_ = bf16[160,512]{1,0:T(8,128)(2,1)S(1)} collective-permute-done((bf16[160,512]{1,0:T(8,128)(2,1)S(1)}, bf16[160,512]{1,0:T(8,128)(2,1)S(1)}, u32[]{:S(2)}, u32[]{:S(2)}) %collective-permute-start.26) | collective-permute-done | bytes 163872 | tf_op jit(solution)/shard_map/ppermute | solution.py:378
  121.9 5.6 %collective-permute-start.22 = (bf16[100,512]{1,0:T(8,128)(2,1)S(1)}, bf16[100,512]{1,0:T(8,128)(2,1)S(1)}, u32[]{:S(2)}, u32[]{:S(2)}) collective-permute-start(bf16[100,512]{1,0:T(8,128)(2,1)S(1)} %pad_maximum_fusion.4), channel_id=1, source_target_pairs={{0,16},{4,20},{8,24},{12,28},{16,0},{20,4},{24,8},{28,12},{1,17},{... | collective-permute-start | bytes 307208 | tf_op jit(solution)/shard_map/ppermute | solution.py:372
  127.5 2.7 %collective-permute-done.22.refs_4_ = bf16[100,512]{1,0:T(8,128)(2,1)S(1)} collective-permute-done((bf16[100,512]{1,0:T(8,128)(2,1)S(1)}, bf16[100,512]{1,0:T(8,128)(2,1)S(1)}, u32[]{:S(2)}, u32[]{:S(2)}) %collective-permute-start.22) | collective-permute-done | bytes 102432 | tf_op jit(solution)/shard_map/ppermute | solution.py:372
  130.2 2.0 %collective-permute-done.21.refs_3_ = bf16[100,512]{1,0:T(8,128)(2,1)S(1)} collective-permute-done((bf16[100,512]{1,0:T(8,128)(2,1)S(1)}, bf16[100,512]{1,0:T(8,128)(2,1)S(1)}, u32[]{:S(2)}, u32[]{:S(2)}) %collective-permute-start.21) | collective-permute-done | bytes 102432 | tf_op jit(solution)/shard_map/ppermute | solution.py:372
  132.2 1.3 combine.1
  133.5 0.9 add_convert_fusion.1
  (52 shorter events, 0.4 us)
Async XLA Ops:
  0.6 1.1 copy-start.10
  1.7 0.7 copy-start.11
  2.4 0.7 copy-start.12
  3.7 14.7 %collective-permute-start.10 = (bf16[100,512]{1,0:T(8,128)(2,1)S(1)}, bf16[100,512]{1,0:T(8,128)(2,1)S(1)}, u32[]{:S(2)}, u32[]{:S(2)}) collective-permute-start(bf16[100,512]{1,0:T(8,128)(2,1)S(1)} %get-tuple-element.42), channel_id=1, source_target_pairs={{0,8},{4,12},{8,0},{12,4},{16,24},{20,28},{24,16},{28,20},{1,9},{5... | collective-permute-start | bytes 307208 | tf_op jit(solution)/shard_map/ppermute | solution.py:372
  6.8 11.7 %collective-permute-start.11 = (bf16[100,512]{1,0:T(8,128)(2,1)S(1)}, bf16[100,512]{1,0:T(8,128)(2,1)S(1)}, u32[]{:S(2)}, u32[]{:S(2)}) collective-permute-start(bf16[100,512]{1,0:T(8,128)(2,1)S(1)} %get-tuple-element.43), channel_id=1, source_target_pairs={{0,16},{4,20},{8,24},{12,28},{16,0},{20,4},{24,8},{28,12},{1,17},{... | collective-permute-start | bytes 307208 | tf_op jit(solution)/shard_map/ppermute | solution.py:372
  9.4 9.1 %collective-permute-start.12 = (bf16[100,512]{1,0:T(8,128)(2,1)S(1)}, bf16[100,512]{1,0:T(8,128)(2,1)S(1)}, u32[]{:S(2)}, u32[]{:S(2)}) collective-permute-start(bf16[100,512]{1,0:T(8,128)(2,1)S(1)} %get-tuple-element.44), channel_id=1, source_target_pairs={{0,24},{4,28},{8,16},{12,20},{16,8},{20,12},{24,0},{28,4},{1,25},{... | collective-permute-start | bytes 307208 | tf_op jit(solution)/shard_map/ppermute | solution.py:372
  10.2 1.0 copy-start.3
  11.2 1.0 copy-start.4
  12.2 1.0 copy-start.5
  13.9 14.7 %collective-permute-start = (bf16[1152,128]{1,0:T(8,128)(2,1)S(1)}, bf16[1152,128]{1,0:T(8,128)(2,1)S(1)}, u32[]{:S(2)}, u32[]{:S(2)}) collective-permute-start(bf16[1152,128]{1,0:T(8,128)(2,1)S(1)} %get-tuple-element.29), channel_id=1, source_target_pairs={{0,8},{4,12},{8,0},{12,4},{16,24},{20,28},{24,16},{28,20},{1,9},{5... | collective-permute-start | bytes 884744 | tf_op jit(solution)/shard_map/ppermute | solution.py:372
  14.8 24.2 %collective-permute-start.1 = (bf16[1152,128]{1,0:T(8,128)(2,1)S(1)}, bf16[1152,128]{1,0:T(8,128)(2,1)S(1)}, u32[]{:S(2)}, u32[]{:S(2)}) collective-permute-start(bf16[1152,128]{1,0:T(8,128)(2,1)S(1)} %get-tuple-element.30), channel_id=1, source_target_pairs={{0,16},{4,20},{8,24},{12,28},{16,0},{20,4},{24,8},{28,12},{1,17},{... | collective-permute-start | bytes 884744 | tf_op jit(solution)/shard_map/ppermute | solution.py:372
  18.4 20.7 %collective-permute-start.2 = (bf16[1152,128]{1,0:T(8,128)(2,1)S(1)}, bf16[1152,128]{1,0:T(8,128)(2,1)S(1)}, u32[]{:S(2)}, u32[]{:S(2)}) collective-permute-start(bf16[1152,128]{1,0:T(8,128)(2,1)S(1)} %get-tuple-element.31), channel_id=1, source_target_pairs={{0,24},{4,28},{8,16},{12,20},{16,8},{20,12},{24,0},{28,4},{1,25},{... | collective-permute-start | bytes 884744 | tf_op jit(solution)/shard_map/ppermute | solution.py:372
  18.6 21.5 %collective-permute-start.13 = (bf16[200,512]{1,0:T(8,128)(2,1)S(1)}, bf16[200,512]{1,0:T(8,128)(2,1)S(1)}, u32[]{:S(2)}, u32[]{:S(2)}) collective-permute-start(bf16[200,512]{1,0:T(8,128)(2,1)S(1)} %pad_maximum_fusion.1), channel_id=1, source_target_pairs={{0,4},{4,0},{8,12},{12,8},{16,20},{20,16},{24,28},{28,24},{1,5},{5... | collective-permute-start | bytes 614408 | tf_op jit(solution)/shard_map/ppermute | solution.py:375
  40.1 36.4 %collective-permute-start.3 = (bf16[3072,128]{1,0:T(8,128)(2,1)}, bf16[3072,128]{1,0:T(8,128)(2,1)S(1)}, u32[]{:S(2)}, u32[]{:S(2)}) collective-permute-start(bf16[3072,128]{1,0:T(8,128)(2,1)} %pad_maximum_fusion), channel_id=1, source_target_pairs={{0,4},{4,0},{8,12},{12,8},{16,20},{20,16},{24,28},{28,24},{1,5},{5... | collective-permute-start | bytes 2359304 | tf_op jit(solution)/shard_map/ppermute | solution.py:375
  40.7 12.4 %collective-permute-start.14 = (bf16[400,512]{1,0:T(8,128)(2,1)S(1)}, bf16[400,512]{1,0:T(8,128)(2,1)S(1)}, u32[]{:S(2)}, u32[]{:S(2)}) collective-permute-start(bf16[400,512]{1,0:T(8,128)(2,1)S(1)} %concatenate.23.refs_0_), channel_id=1, source_target_pairs={{0,1},{1,0},{2,3},{3,2},{4,5},{5,4},{6,7},{7,6},{8,9},{9,8},{10,11... | collective-permute-start | bytes 1228808 | tf_op jit(solution)/shard_map/ppermute | solution.py:378
  42.3 20.4 %collective-permute-start.15 = (bf16[400,512]{1,0:T(8,128)(2,1)S(1)}, bf16[400,512]{1,0:T(8,128)(2,1)S(1)}, u32[]{:S(2)}, u32[]{:S(2)}) collective-permute-start(bf16[400,512]{1,0:T(8,128)(2,1)S(1)} %concatenate.23.refs_0_), channel_id=1, source_target_pairs={{0,2},{1,3},{2,0},{3,1},{4,6},{5,7},{6,4},{7,5},{8,10},{9,11},{10,... | collective-permute-start | bytes 1228808 | tf_op jit(solution)/shard_map/ppermute | solution.py:378
  43.8 18.9 %collective-permute-start.16 = (bf16[400,512]{1,0:T(8,128)(2,1)S(1)}, bf16[400,512]{1,0:T(8,128)(2,1)S(1)}, u32[]{:S(2)}, u32[]{:S(2)}) collective-permute-start(bf16[400,512]{1,0:T(8,128)(2,1)S(1)} %concatenate.23.refs_0_), channel_id=1, source_target_pairs={{0,3},{1,2},{2,1},{3,0},{4,7},{5,6},{6,5},{7,4},{8,11},{9,10},{10,... | collective-permute-start | bytes 1228808 | tf_op jit(solution)/shard_map/ppermute | solution.py:378
  62.7 1.6 %copy-start.6 = (bf16[1,2048,512]{2,1,0:T(8,128)(2,1)S(1)}, bf16[1,2048,512]{2,1,0:T(8,128)(2,1)}, u32[]{:S(2)}) copy-start(bf16[1,2048,512]{2,1,0:T(8,128)(2,1)} %param.26) | copy-start | bytes 6291460
  64.3 1.6 %copy-start.7 = (bf16[1,2048,512]{2,1,0:T(8,128)(2,1)S(1)}, bf16[1,2048,512]{2,1,0:T(8,128)(2,1)}, u32[]{:S(2)}) copy-start(bf16[1,2048,512]{2,1,0:T(8,128)(2,1)} %param.27) | copy-start | bytes 6291460
  65.9 1.6 %copy-start.8 = (bf16[1,512,2048]{2,1,0:T(8,128)(2,1)S(1)}, bf16[1,512,2048]{2,1,0:T(8,128)(2,1)}, u32[]{:S(2)}) copy-start(bf16[1,512,2048]{2,1,0:T(8,128)(2,1)} %param.28) | copy-start | bytes 6291460
  67.5 6.3 %copy-start = (bf16[2048,512]{1,0:T(8,128)(2,1)S(1)}, bf16[2048,512]{1,0:T(8,128)(2,1)}, u32[]{:S(2)}) copy-start(bf16[2048,512]{1,0:T(8,128)(2,1)} %refs_1_.3) | copy-start | bytes 6291460
  67.5 6.3 %copy-start.1 = (bf16[2048,512]{1,0:T(8,128)(2,1)S(1)}, bf16[2048,512]{1,0:T(8,128)(2,1)}, u32[]{:S(2)}) copy-start(bf16[2048,512]{1,0:T(8,128)(2,1)} %refs_2_.3) | copy-start | bytes 6291460
  67.5 6.3 %copy-start.2 = (bf16[512,2048]{1,0:T(8,128)(2,1)S(1)}, bf16[512,2048]{1,0:T(8,128)(2,1)}, u32[]{:S(2)}) copy-start(bf16[512,2048]{1,0:T(8,128)(2,1)} %refs_3_.1) | copy-start | bytes 6291460
  70.2 22.4 %collective-permute-start.17 = (bf16[400,512]{1,0:T(8,128)(2,1)S(1)}, bf16[400,512]{1,0:T(8,128)(2,1)S(1)}, u32[]{:S(2)}, u32[]{:S(2)}) collective-permute-start(bf16[400,512]{1,0:T(8,128)(2,1)S(1)} %get-tuple-element.46), channel_id=1, source_target_pairs={{0,1},{1,0},{2,3},{3,2},{4,5},{5,4},{6,7},{7,6},{8,9},{9,8},{10,11... | collective-permute-start | bytes 1228808 | tf_op jit(solution)/shard_map/ppermute | solution.py:378
  71.5 22.2 %collective-permute-start.18 = (bf16[400,512]{1,0:T(8,128)(2,1)S(1)}, bf16[400,512]{1,0:T(8,128)(2,1)S(1)}, u32[]{:S(2)}, u32[]{:S(2)}) collective-permute-start(bf16[400,512]{1,0:T(8,128)(2,1)S(1)} %get-tuple-element.47), channel_id=1, source_target_pairs={{0,2},{1,3},{2,0},{3,1},{4,6},{5,7},{6,4},{7,5},{8,10},{9,11},{10,... | collective-permute-start | bytes 1228808 | tf_op jit(solution)/shard_map/ppermute | solution.py:378
  72.4 22.9 %collective-permute-start.19 = (bf16[400,512]{1,0:T(8,128)(2,1)S(1)}, bf16[400,512]{1,0:T(8,128)(2,1)S(1)}, u32[]{:S(2)}, u32[]{:S(2)}) collective-permute-start(bf16[400,512]{1,0:T(8,128)(2,1)S(1)} %get-tuple-element.48), channel_id=1, source_target_pairs={{0,3},{1,2},{2,1},{3,0},{4,7},{5,6},{6,5},{7,4},{8,11},{9,10},{10,... | collective-permute-start | bytes 1228808 | tf_op jit(solution)/shard_map/ppermute | solution.py:378
  73.8 2.6 %copy-start.14 = (f32[4]{0:T(128)S(1)}, f32[4]{0:T(128)}, u32[]{:S(2)}) copy-start(f32[4]{0:T(128)} %refs_0_.4) | copy-start | bytes 52
  73.8 2.6 %copy-start.15 = (f32[128]{0:T(128)S(1)}, f32[128]{0:T(128)}, u32[]{:S(2)}) copy-start(f32[128]{0:T(128)} %param.20) | copy-start | bytes 1540
  75.1 31.3 %collective-permute-start.24 = (bf16[160,512]{1,0:T(8,128)(2,1)S(1)}, bf16[160,512]{1,0:T(8,128)(2,1)S(1)}, u32[]{:S(2)}, u32[]{:S(2)}) collective-permute-start(bf16[160,512]{1,0:T(8,128)(2,1)S(1)} %get-tuple-element.51), channel_id=1, source_target_pairs={{0,1},{1,0},{2,3},{3,2},{4,5},{5,4},{6,7},{7,6},{8,9},{9,8},{10,11... | collective-permute-start | bytes 491528 | tf_op jit(solution)/shard_map/ppermute | solution.py:378
  86.9 14.9 %copy-start.9 = (bf16[512,2048]{1,0:T(8,128)(2,1)S(1)}, bf16[512,2048]{1,0:T(8,128)(2,1)}, u32[]{:S(2)}) copy-start(bf16[512,2048]{1,0:T(8,128)(2,1)} %refs_4_.1) | copy-start | bytes 6291460
  86.9 9.4 %collective-permute-start.4 = (bf16[384,128]{1,0:T(8,128)(2,1)S(1)}, bf16[384,128]{1,0:T(8,128)(2,1)S(1)}, u32[]{:S(2)}, u32[]{:S(2)}) collective-permute-start(bf16[384,128]{1,0:T(8,128)(2,1)S(1)} %get-tuple-element.33), channel_id=1, source_target_pairs={{0,8},{4,12},{8,0},{12,4},{16,24},{20,28},{24,16},{28,20},{1,9},{5... | collective-permute-start | bytes 294920 | tf_op jit(solution)/shard_map/ppermute | solution.py:372
  92.7 9.1 %collective-permute-start.5 = (bf16[384,128]{1,0:T(8,128)(2,1)S(1)}, bf16[384,128]{1,0:T(8,128)(2,1)S(1)}, u32[]{:S(2)}, u32[]{:S(2)}) collective-permute-start(bf16[384,128]{1,0:T(8,128)(2,1)S(1)} %get-tuple-element.34), channel_id=1, source_target_pairs={{0,16},{4,20},{8,24},{12,28},{16,0},{20,4},{24,8},{28,12},{1,17},{... | collective-permute-start | bytes 294920 | tf_op jit(solution)/shard_map/ppermute | solution.py:372
  93.8 8.0 %collective-permute-start.6 = (bf16[384,128]{1,0:T(8,128)(2,1)S(1)}, bf16[384,128]{1,0:T(8,128)(2,1)S(1)}, u32[]{:S(2)}, u32[]{:S(2)}) collective-permute-start(bf16[384,128]{1,0:T(8,128)(2,1)S(1)} %get-tuple-element.35), channel_id=1, source_target_pairs={{0,24},{4,28},{8,16},{12,20},{16,8},{20,12},{24,0},{28,4},{1,25},{... | collective-permute-start | bytes 294920 | tf_op jit(solution)/shard_map/ppermute | solution.py:372
  95.5 9.5 %collective-permute-start.20 = (bf16[200,512]{1,0:T(8,128)(2,1)S(1)}, bf16[200,512]{1,0:T(8,128)(2,1)S(1)}, u32[]{:S(2)}, u32[]{:S(2)}) collective-permute-start(bf16[200,512]{1,0:T(8,128)(2,1)S(1)} %slice.94), channel_id=1, source_target_pairs={{0,4},{4,0},{8,12},{12,8},{16,20},{20,16},{24,28},{28,24},{1,5},{5... | collective-permute-start | bytes 614408 | tf_op jit(solution)/shard_map/ppermute | solution.py:375
  96.3 11.8 %collective-permute-start.25 = (bf16[160,512]{1,0:T(8,128)(2,1)S(1)}, bf16[160,512]{1,0:T(8,128)(2,1)S(1)}, u32[]{:S(2)}, u32[]{:S(2)}) collective-permute-start(bf16[160,512]{1,0:T(8,128)(2,1)S(1)} %get-tuple-element.52), channel_id=1, source_target_pairs={{0,2},{1,3},{2,0},{3,1},{4,6},{5,7},{6,4},{7,5},{8,10},{9,11},{10,... | collective-permute-start | bytes 491528 | tf_op jit(solution)/shard_map/ppermute | solution.py:378
  101.8 30.4 %copy-start.13 = (f32[160,2]{0,1:T(2,128)S(1)}, f32[160,2]{0,1:T(2,128)}, u32[]{:S(2)}) copy-start(f32[160,2]{0,1:T(2,128)} %param.25) | copy-start | bytes 3844
  102.8 30.6 %collective-permute-start.7 = (bf16[384,512]{1,0:T(8,128)(2,1)S(1)}, bf16[384,512]{1,0:T(8,128)(2,1)S(1)}, u32[]{:S(2)}, u32[]{:S(2)}) collective-permute-start(bf16[384,512]{1,0:T(8,128)(2,1)S(1)} %get-tuple-element.37), channel_id=1, source_target_pairs={{0,1},{1,0},{2,3},{3,2},{4,5},{5,4},{6,7},{7,6},{8,9},{9,8},{10,11... | collective-permute-start | bytes 1179656 | tf_op jit(solution)/shard_map/ppermute | solution.py:378
  103.5 30.0 %collective-permute-start.8 = (bf16[384,512]{1,0:T(8,128)(2,1)S(1)}, bf16[384,512]{1,0:T(8,128)(2,1)S(1)}, u32[]{:S(2)}, u32[]{:S(2)}) collective-permute-start(bf16[384,512]{1,0:T(8,128)(2,1)S(1)} %get-tuple-element.38), channel_id=1, source_target_pairs={{0,2},{1,3},{2,0},{3,1},{4,6},{5,7},{6,4},{7,5},{8,10},{9,11},{10,... | collective-permute-start | bytes 1179656 | tf_op jit(solution)/shard_map/ppermute | solution.py:378
  104.9 28.5 %collective-permute-start.9 = (bf16[384,512]{1,0:T(8,128)(2,1)S(1)}, bf16[384,512]{1,0:T(8,128)(2,1)S(1)}, u32[]{:S(2)}, u32[]{:S(2)}) collective-permute-start(bf16[384,512]{1,0:T(8,128)(2,1)S(1)} %get-tuple-element.39), channel_id=1, source_target_pairs={{0,3},{1,2},{2,1},{3,0},{4,7},{5,6},{6,5},{7,4},{8,11},{9,10},{10,... | collective-permute-start | bytes 1179656 | tf_op jit(solution)/shard_map/ppermute | solution.py:378
  106.5 15.4 %collective-permute-start.26 = (bf16[160,512]{1,0:T(8,128)(2,1)S(1)}, bf16[160,512]{1,0:T(8,128)(2,1)S(1)}, u32[]{:S(2)}, u32[]{:S(2)}) collective-permute-start(bf16[160,512]{1,0:T(8,128)(2,1)S(1)} %get-tuple-element.53), channel_id=1, source_target_pairs={{0,3},{1,2},{2,1},{3,0},{4,7},{5,6},{6,5},{7,4},{8,11},{9,10},{10,... | collective-permute-start | bytes 491528 | tf_op jit(solution)/shard_map/ppermute | solution.py:378
  108.0 19.5 %collective-permute-start.23 = (bf16[100,512]{1,0:T(8,128)(2,1)S(1)}, bf16[100,512]{1,0:T(8,128)(2,1)S(1)}, u32[]{:S(2)}, u32[]{:S(2)}) collective-permute-start(bf16[100,512]{1,0:T(8,128)(2,1)S(1)} %pad_maximum_fusion.5), channel_id=1, source_target_pairs={{0,24},{4,28},{8,16},{12,20},{16,8},{20,12},{24,0},{28,4},{1,25},{... | collective-permute-start | bytes 307208 | tf_op jit(solution)/shard_map/ppermute | solution.py:372
  121.9 8.3 %collective-permute-start.22 = (bf16[100,512]{1,0:T(8,128)(2,1)S(1)}, bf16[100,512]{1,0:T(8,128)(2,1)S(1)}, u32[]{:S(2)}, u32[]{:S(2)}) collective-permute-start(bf16[100,512]{1,0:T(8,128)(2,1)S(1)} %pad_maximum_fusion.4), channel_id=1, source_target_pairs={{0,16},{4,20},{8,24},{12,28},{16,0},{20,4},{24,8},{28,12},{1,17},{... | collective-permute-start | bytes 307208 | tf_op jit(solution)/shard_map/ppermute | solution.py:372
  127.5 4.7 %collective-permute-start.21 = (bf16[100,512]{1,0:T(8,128)(2,1)S(1)}, bf16[100,512]{1,0:T(8,128)(2,1)S(1)}, u32[]{:S(2)}, u32[]{:S(2)}) collective-permute-start(bf16[100,512]{1,0:T(8,128)(2,1)S(1)} %pad_maximum_fusion.3), channel_id=1, source_target_pairs={{0,8},{4,12},{8,0},{12,4},{16,24},{20,28},{24,16},{28,20},{1,9},{5... | collective-permute-start | bytes 307208 | tf_op jit(solution)/shard_map/ppermute | solution.py:372
where the time goes:
time: 135 us; the launch traced here: 134 us
  waiting for transfers between devices  60.3 us (45%)
  starting transfers between devices  41 us (30%)
  Pallas kernels  18 us (13%)
  local copies, waits for them, and re-layouts  11.1 us (8%)
  other arithmetic  3.03 us (2%)
    ppermute x12, waiting for transfers between devices, along_z(): lax.ppermute(x, 'ep', [(i, 2 * (i // 2 ^ s) + i % 2) for i in range(ep)])  30.5 us
    ppermute x12, waiting for transfers between devices, along_tp(): return lax.ppermute(x, 'tp', [(i, i ^ s) for i in range(tp)])  29.8 us
    ppermute x12, starting transfers between devices, along_z(): lax.ppermute(x, 'ep', [(i, 2 * (i // 2 ^ s) + i % 2) for i in range(ep)])  26.6 us
    ppermute x12, starting transfers between devices, along_tp(): return lax.ppermute(x, 'tp', [(i, i ^ s) for i in range(tp)])  14.3 us
    pallas_call x1, Pallas kernels, inner(): pl.pallas_call(lambda *refs: attend_kernel(*refs, count=chips, rows=rows,...  10.4 us
    unnamed x32, local copies, waits for them, and re-layouts  10.2 us
    pallas_call x2, Pallas kernels, run_expert(): pl.pallas_call(lambda *refs: expert_kernel(*refs, pieces=len(xs), outs=tp...  4.07 us
  transfers between devices with their start and end apart: 27, of which 9 were waited for; matrix products, arithmetic and copies ran while one was open for 2% of the time, Pallas kernels for 13%

commit v1 on v0

--- a/solution.py
+++ b/solution.py
@@ -19,6 +19,8 @@
 VM = pl.BlockSpec(memory_space=pltpu.VMEM)
 SM = pl.BlockSpec(memory_space=pltpu.SMEM)
 ANY = pl.BlockSpec(memory_space=pl.ANY)
+FAR = pl.BlockSpec(memory_space=pltpu.HBM)
+DMA = pltpu.SemaphoreType.DMA
 
 
 def sds(shape, dtype=jnp.bfloat16):
@@ -27,6 +29,17 @@
 
 def limit(mib):
     return pltpu.CompilerParams(vmem_limit_bytes=mib * 1024 * 1024)
+
+
+def far(x):
+    return pltpu.with_memory_space_constraint(x, pltpu.HBM)
+
+
+def begin(pairs, sems):
+    copies = [pltpu.make_async_copy(a, b, sems.at[n]) for n, (a, b) in enumerate(pairs)]
+    for copy in copies:
+        copy.start()
+    return copies
 
 
 def cost(flops):
@@ -45,9 +58,12 @@
     return jnp.sum(jnp.where(diagonal, row, jnp.zeros_like(row)), axis=1, keepdims=True)
 
 
-def dispatch_kernel(rows, gain, routes, xn_out, slots_out, *parts, cap, experts):
+def dispatch_kernel(rows_far, gain_far, routes_far, xn_out, slots_out, *refs, cap, experts):
+    *parts, rows, gain, routes, sems = refs
     z, core, ti = place()
     tokens = rows.shape[0]
+    for copy in begin(((rows_far, rows), (gain_far, gain), (routes_far, routes)), sems):
+        copy.wait()
     values = rows[...].astype(jnp.float32)
     inverse = lax.rsqrt(jnp.mean(values * values, axis=-1, keepdims=True) + norm_eps)
     xn_out[...] = (values * inverse * gain[...]).astype(jnp.bfloat16)
@@ -75,40 +91,98 @@
         part[...] = jnp.dot(pick, mine, preferred_element_type=jnp.float32).astype(jnp.bfloat16)
 
 
-def expert_kernel(*refs, pieces, outs):
+def pack_kernel(*refs, count, cap):
+    parts, own, other = refs[:count], refs[count], refs[count + 1]
+    for s in range(count):
+        own[s * cap : (s + 1) * cap, :] = parts[s][:cap, :]
+        other[s * cap : (s + 1) * cap, :] = parts[s][cap:, :]
+
+
+def spread_out(block, ti, outs, direct):
+    if direct:
+        for s, out in enumerate(outs):
+            out[...] = block(ti ^ s).astype(jnp.bfloat16)
+        return
+    send_x, keep_x, send_y, keep_y = outs
+    half = send_x.shape[0] // 2
+    for s, upper, lower in ((0, (keep_x, 0), (keep_y, 0)), (1, (send_x, 0), (keep_y, half)),
+                            (2, (keep_x, half), (send_y, 0)), (3, (send_x, half), (send_y, half))):
+        values = block(ti ^ s).astype(jnp.bfloat16)
+        for (ref, at), piece in ((upper, values[:half]), (lower, values[half:])):
+            ref[at : at + half, :] = piece
+
+
+def expert_kernel(*refs, pieces, halves, direct, staged):
     ti = place()[2]
-    xs, (gate_w, up_w, down_w), ys = refs[:pieces], refs[pieces : pieces + 3], refs[pieces + 3 :]
-    width = xs[0].shape[1]
+    xs, (gate_w, up_w, down_w) = refs[: pieces * halves], refs[pieces * halves :][:3]
+    rest = refs[pieces * halves + 3 :]
+    chunks = pieces
+    if staged:
+        *ys, rows_ref, gates, ups, downs, sems = rest
+        chunks = gates.shape[0]
+        width = gates.shape[1]
+        pairs = []
+        for s in range(chunks):
+            at = pl.ds(pl.multiple_of((ti ^ s) * width, width), width)
+            pairs += [(gate_w.at[at, :], gates.at[s]), (up_w.at[at, :], ups.at[s])]
+        copies = begin(pairs + [(down_w, downs)], sems)
+    else:
+        *ys, rows_ref = rest
+        width = gate_w.shape[0] // chunks
+        downs = down_w
     gate = up = None
-    for s in range(pieces):
+    for s in range(chunks):
+        part = xs[0].shape[0]
+        at = pl.ds(pl.multiple_of((ti ^ s) * width, width), width)
         if pieces == 1:
-            wg, wu = gate_w[...], up_w[...]
+            x = xs[0][:, at]
         else:
-            at = pl.ds(pl.multiple_of((ti ^ s) * width, width), width)
+            for h in range(halves):
+                rows_ref[s % 2, h * part : (h + 1) * part, :] = xs[h * pieces + s][...]
+            x = rows_ref[s % 2]
+        if staged:
+            copies[2 * s].wait()
+            copies[2 * s + 1].wait()
+            wg, wu = gates[s], ups[s]
+        else:
             wg, wu = gate_w[at, :], up_w[at, :]
-        x = xs[s][...]
         g = jnp.dot(x, wg, preferred_element_type=jnp.float32)
         u = jnp.dot(x, wu, preferred_element_type=jnp.float32)
         gate = g if gate is None else gate + g
         up = u if up is None else up + u
     hidden = (gate / (1.0 + jnp.exp(-gate)) * up).astype(jnp.bfloat16)
+    if staged:
+        copies[-1].wait()
     cols = ys[0].shape[1]
-    for s in range(outs):
-        at = pl.ds(pl.multiple_of((ti ^ s) * cols, cols), cols)
-        ys[s][...] = jnp.dot(hidden, down_w[:, at], preferred_element_type=jnp.float32).astype(
-            jnp.bfloat16
-        )
-
-
-def run_expert(xs, gate_w, up_w, down_w, tp):
-    rows = xs[0].shape[0]
+
+    def block(n):
+        at = pl.ds(pl.multiple_of(n * cols, cols), cols)
+        return jnp.dot(hidden, downs[:, at], preferred_element_type=jnp.float32)
+
+    spread_out(block, ti, ys, direct)
+
+
+def out_shapes(rows, cols, tp, direct):
+    return [sds((rows, cols))] * (tp if direct else 4)
+
+
+def run_expert(xs, halves, gate_w, up_w, down_w, tp, direct):
+    rows = xs[0].shape[0] * halves
     width, hidden = gate_w.shape
-    cols = down_w.shape[1] // tp
+    shapes = out_shapes(rows, down_w.shape[1] // tp, tp, direct)
+    pieces = len(xs) // halves
+    staged = pieces == 1
+    scratch = [pltpu.VMEM((2, rows, width // tp), jnp.bfloat16)]
+    if staged:
+        part = pltpu.VMEM((tp, width // tp, hidden), jnp.bfloat16)
+        scratch += [part, part, pltpu.VMEM(down_w.shape, jnp.bfloat16), DMA((2 * tp + 1,))]
+        gate_w, up_w, down_w = far(gate_w), far(up_w), far(down_w)
     return pl.pallas_call(
-        lambda *refs: expert_kernel(*refs, pieces=len(xs), outs=tp),
-        out_shape=[sds((rows, cols))] * tp,
-        in_specs=[VM] * (len(xs) + 3),
-        out_specs=[VM] * tp,
+        lambda *refs: expert_kernel(*refs, pieces=pieces, halves=halves, direct=direct, staged=staged),
+        out_shape=shapes,
+        in_specs=[VM] * len(xs) + [FAR if staged else VM] * 3,
+        out_specs=[VM] * len(shapes),
+        scratch_shapes=scratch,
         cost_estimate=cost(6 * rows * width * hidden),
         compiler_params=limit(24),
     )(*xs, gate_w, up_w, down_w)
@@ -138,7 +212,9 @@
     out[...] = (routed + total).astype(jnp.bfloat16)
 
 
-def rope_kernel(q, k, v, cosine, sine, *outs, size):
+def rope_kernel(q_far, k_far, v_far, cosine, sine, *refs, size):
+    *outs, q, k, v, sems = refs
+    copies = begin(((q_far, q), (k_far, k), (v_far, v)), sems)
     z = place()[0]
     rows = q.shape[0]
     both = cosine.shape[1]
@@ -146,6 +222,8 @@
     lane = lax.broadcasted_iota(jnp.int32, (rows, both), 1)
     front = (lane % size) < half
     c, s_ = cosine[...], sine[...]
+    for copy in copies:
+        copy.wait()
     for s, out in enumerate(outs):
         at = pl.ds(pl.multiple_of((z ^ s) * both, both), both)
         for n, ref in enumerate((q, k)):
@@ -155,33 +233,24 @@
         out[2 * rows : 3 * rows, :] = v[:, at]
 
 
-def attend_kernel(lam, gain, *refs, count, rows, size):
-    own, other = refs[:count], refs[count]
-    outs = refs[count + 1 : 2 * count + 1]
-    qs, ks, vs, scores, weights, heads, sems = refs[2 * count + 1 :]
+def attend_kernel(lam_far, gain_far, *refs, count, rows, size):
+    own, other, outs = refs[:count], refs[count : 2 * count], refs[2 * count : 3 * count]
+    qs, ks, vs, scores, weights, heads, lam, gain, sems = refs[3 * count :]
     z, core, _ = place()
     both = 2 * size
     value = vs.shape[1] // 2
     keys = 2 * rows
-    copies = []
+    pairs = [(lam_far, lam), (gain_far, gain)]
     for s in range(count):
         at = pl.multiple_of((z ^ s) * rows, rows)
         mine = pl.multiple_of((2 * (z ^ s) + core) * rows, rows)
         theirs = pl.multiple_of((2 * (z ^ s) + 1 - core) * rows, rows)
-        pairs = (
-            (own[s].at[pl.ds(0, rows), :], qs.at[pl.ds(at, rows), :]),
-            (own[s].at[pl.ds(rows, rows), :], ks.at[pl.ds(mine, rows), :]),
-            (own[s].at[pl.ds(2 * rows, rows), :], vs.at[pl.ds(mine, rows), pl.ds(0, value)]),
-            (other.at[pl.ds(2 * s * rows, rows), :], ks.at[pl.ds(theirs, rows), :]),
-            (
-                other.at[pl.ds((2 * s + 1) * rows, rows), :],
-                vs.at[pl.ds(theirs, rows), pl.ds(0, value)],
-            ),
-        )
-        for n, (src, dst) in enumerate(pairs):
-            copy = pltpu.make_async_copy(src, dst, sems.at[5 * s + n])
-            copy.start()
-            copies.append(copy)
+        pairs.append((own[s].at[pl.ds(0, rows), :], qs.at[pl.ds(at, rows), :]))
+        for ref, to in ((own[s], mine), (other[s], theirs)):
+            k_rows, v_rows, to = pl.ds(rows, rows), pl.ds(2 * rows, rows), pl.ds(to, rows)
+            pairs.append((ref.at[k_rows, :], ks.at[to, :]))
+            pairs.append((ref.at[v_rows, :], vs.at[to, pl.ds(0, value)]))
+    copies = begin(pairs, sems)
     vs[:, value:] = jnp.ones((vs.shape[0], value), jnp.bfloat16)
     for copy in copies:
         copy.wait()
@@ -229,7 +298,9 @@
         acc = jnp.dot(weights[u % 2, :, :span], vs[:span, :], preferred_element_type=jnp.float32)
         maps[m] = acc[:, :value] / acc[:, value:]
         if m == 1:
-            diff = maps[0] - lam[z] * maps[1]
+            heads_at = lax.broadcasted_iota(jnp.int32, lam.shape, 1)
+            factor2 = jnp.sum(jnp.where(heads_at == z, lam[...], 0.0), axis=1, keepdims=True)
+            diff = maps[0] - factor2 * maps[1]
             inverse = lax.rsqrt(jnp.mean(diff * diff, axis=1, keepdims=True) + norm_eps)
             heads[block * rows : (block + 1) * rows, :] = (diff * inverse * gain[...]).astype(
                 jnp.bfloat16
@@ -247,19 +318,20 @@
         outs[s][...] = heads[pl.ds(pl.multiple_of((z ^ s) * rows, rows), rows), :]
 
 
-def project_kernel(*refs, count, tp):
-    heads, weight, outs, rows_ref = refs[:count], refs[count], refs[count + 1 : -1], refs[-1]
+def project_kernel(*refs, count, direct):
+    heads, weight, (*outs, rows_ref) = refs[:count], refs[count], refs[count + 1 :]
     z, _, ti = place()
     value = heads[0].shape[1]
     for s in range(count):
         rows_ref[:, pl.ds(pl.multiple_of((z ^ s) * value, value), value)] = heads[s][...]
     rows = rows_ref[...]
     cols = outs[0].shape[1]
-    for s in range(tp):
-        at = pl.ds(pl.multiple_of((ti ^ s) * cols, cols), cols)
-        outs[s][...] = jnp.dot(rows, weight[:, at], preferred_element_type=jnp.float32).astype(
-            jnp.bfloat16
-        )
+
+    def block(n):
+        at = pl.ds(pl.multiple_of(n * cols, cols), cols)
+        return jnp.dot(rows, weight[:, at], preferred_element_type=jnp.float32)
+
+    spread_out(block, ti, outs, direct)
 
 
 def rotate(inputs, positions):
@@ -380,6 +452,37 @@
     def exchange(parts, move):
         return [parts[0]] + [move(parts[s], s) for s in range(1, len(parts))]
 
+    direct = tp != 4
+
+    def gather_tp(own, other):
+        if direct:
+            return [
+                piece
+                for half in (own, other)
+                for piece in [half] + [along_tp(half, s) for s in range(1, tp)]
+            ]
+        own_1, other_2 = along_tp(own, 1), along_tp(other, 2)
+        own_2, other_1 = along_tp(own, 2), along_tp(other, 1)
+        own_3, other_3 = along_tp(own_1, 2), along_tp(other_2, 1)
+        return [own, own_1, own_2, own_3, other, other_1, other_2, other_3]
+
+    def reduce_tp(parts):
+        up = lambda x: x.astype(jnp.float32)
+        if direct:
+            total = sum(up(p) for p in exchange(parts, along_tp))
+            half = total.shape[0] // 2
+            return total[:half], total[half:]
+        send_x, keep_x, send_y, keep_y = parts
+        half = send_x.shape[0] // 2
+        got_x, got_y = along_tp(send_x, 1), along_tp(send_y, 2)
+        mid_x = (up(keep_x[half:]) + up(got_x[half:])).astype(jnp.bfloat16)
+        mid_y = (up(keep_y[half:]) + up(got_y[half:])).astype(jnp.bfloat16)
+        mid_x, mid_y = along_tp(mid_x, 2), along_tp(mid_y, 1)
+        return (
+            up(keep_x[:half]) + up(got_x[:half]) + up(mid_x),
+            up(keep_y[:half]) + up(got_y[:half]) + up(mid_y),
+        )
+
     tokens, width = moe_input.shape
     cap = tokens * TOP_K * 5 // (4 * ep)
     slice_width = width // tp
@@ -387,12 +490,18 @@
         lambda *refs: dispatch_kernel(*refs, cap=cap, experts=ep),
         out_shape=[sds((tokens, width)), sds((TOP_K, tokens), jnp.int32)]
         + [sds((2 * cap, slice_width))] * chips,
-        in_specs=[VM] * 3,
+        in_specs=[FAR] * 3,
         out_specs=[VM] * (2 + chips),
+        scratch_shapes=[
+            pltpu.VMEM(moe_input.shape, jnp.bfloat16),
+            pltpu.VMEM((1, width), jnp.float32),
+            pltpu.VMEM((TOP_K, tokens), jnp.int32),
+            DMA((3,)),
+        ],
         cost_estimate=cost(4e8),
         name="dispatch",
         compiler_params=limit(8),
-    )(moe_input, ffn_gain.reshape(1, -1), routes.T)
+    )(far(moe_input), far(ffn_gain.reshape(1, -1)), far(routes.T))
     arrived = exchange(parts, along_z)
 
     rows = query_pairs.shape[0]
@@ -411,31 +520,39 @@
         packs = pl.pallas_call(
             lambda *refs: rope_kernel(*refs, size=size),
             out_shape=[sds((3 * rows, value))] * chips,
-            in_specs=[VM] * 5,
+            in_specs=[FAR] * 3 + [VM] * 2,
             out_specs=[VM] * chips,
+            scratch_shapes=[pltpu.VMEM(query_pairs.shape, jnp.bfloat16)] * 3 + [DMA((3,))],
             cost_estimate=cost(4e8),
             name="rope",
         compiler_params=limit(8),
-        )(query_pairs, key_pairs, value_rows, cosine, sine)
+        )(far(query_pairs), far(key_pairs), far(value_rows), cosine, sine)
         packs = exchange(packs, along_z)
-        other = jnp.concatenate([p[rows:] for p in packs], axis=0)
-        other = swap(other)
-
-    shared = run_expert([xn], shared_gate, shared_up, shared_down, tp)
+        others = [swap(packs[0])]
+        others += [swap(p) for p in packs[1:]]
+
+    shared = run_expert([xn], 1, shared_gate, shared_up, shared_down, tp, True)
     shared = exchange(shared, along_tp)
 
-    swapped = swap(jnp.concatenate([p[cap:] for p in arrived], axis=0))
-    held = jnp.concatenate([p[:cap] for p in arrived] + [swapped], axis=0)
-    slices = [held] + [along_tp(held, s) for s in range(1, tp)]
-    terms = run_expert(slices, gate_weight[0], up_weight[0], down_weight[0], tp)
-    terms = exchange(terms, along_tp)
-    summed = sum(t.astype(jnp.float32) for t in terms).astype(jnp.bfloat16)
+    own, other = pl.pallas_call(
+        lambda *refs: pack_kernel(*refs, count=chips, cap=cap),
+        out_shape=[sds((chips * cap, slice_width))] * 2,
+        in_specs=[VM] * chips,
+        out_specs=[VM] * 2,
+        cost_estimate=cost(1e8),
+        compiler_params=limit(8),
+        name="pack",
+    )(*arrived)
+    other = swap(other)
+    slices = gather_tp(own, other)
+    terms = run_expert(slices, 2, gate_weight[0], up_weight[0], down_weight[0], tp, direct)
+    summed = [x.astype(jnp.bfloat16) for x in reduce_tp(terms)]
 
     if spread:
         heads_out = pl.pallas_call(
             lambda *refs: attend_kernel(*refs, count=chips, rows=rows, size=size),
             out_shape=[sds((rows, value))] * chips,
-            in_specs=[SM, VM] + [ANY] * (chips + 1),
+            in_specs=[FAR, FAR] + [ANY] * (2 * chips),
             out_specs=[VM] * chips,
             scratch_shapes=[
                 pltpu.VMEM((chips * rows, value), jnp.bfloat16),
@@ -444,25 +561,27 @@
                 pltpu.VMEM((2, rows, ep * rows), jnp.float32),
                 pltpu.VMEM((2, rows, ep * rows), jnp.bfloat16),
                 pltpu.VMEM((chips * rows, value), jnp.bfloat16),
-                pltpu.SemaphoreType.DMA((5 * chips,)),
+                pltpu.VMEM((1, heads), jnp.float32),
+                pltpu.VMEM((1, value), jnp.float32),
+                DMA((5 * chips + 2,)),
             ],
             cost_estimate=cost(4e9),
             name="attend",
         compiler_params=limit(32),
-        )(head_lambda, head_gain.reshape(1, -1), *packs, other)
+        )(head_lambda.reshape(1, -1), head_gain.reshape(1, -1), *packs, *others)
         normed = exchange(heads_out, along_z)
+        shapes = out_shapes(rows, out_weight.shape[1] // tp, tp, direct)
         mixer = pl.pallas_call(
-            lambda *refs: project_kernel(*refs, count=chips, tp=tp),
-            out_shape=[sds((rows, out_weight.shape[1] // tp))] * tp,
+            lambda *refs: project_kernel(*refs, count=chips, direct=direct),
+            out_shape=shapes,
             in_specs=[VM] * (chips + 1),
-            out_specs=[VM] * tp,
+            out_specs=[VM] * len(shapes),
             scratch_shapes=[pltpu.VMEM((rows, chips * value), jnp.bfloat16)],
             cost_estimate=cost(1e9),
             name="project",
-        compiler_params=limit(10),
+            compiler_params=limit(12),
         )(*normed, out_weight)
-        mixer = exchange(mixer, along_tp)
-        attn_out = sum(m.astype(jnp.float32) for m in mixer).astype(jnp.bfloat16)
+        attn_out = jnp.concatenate(reduce_tp(mixer), axis=0).astype(jnp.bfloat16)
     else:
         head_rows = gathered_attention(query_pairs, key_pairs, value_rows, head_lambda, head_gain)[0]
         mixer = jnp.dot(head_rows, out_weight, preferred_element_type=jnp.float32)
@@ -470,10 +589,9 @@
             mixer.astype(jnp.bfloat16), "tp", scatter_dimension=1, tiled=True
         )
 
-    half = chips * cap
-    back = swap(summed[half:])
+    back = swap(summed[1])
     groups = [
-        jnp.concatenate([summed[s * cap : (s + 1) * cap], back[s * cap : (s + 1) * cap]], axis=0)
+        jnp.concatenate([x[s * cap : (s + 1) * cap] for x in (summed[0], back)], axis=0)
         for s in range(chips)
     ]
     groups = exchange(groups, along_z)

time: 135 us -> 132 us (0.978)
  local copies, waits for them, and re-layouts: 11.1 us -> 0.12 us
  Pallas kernels: 18 us -> 22.5 us
  starting transfers between devices: 41 us -> 43.5 us
  waiting for transfers between devices: 60.3 us -> 62.5 us
    unnamed x32 -> x14, local copies, waits for them, and re-layouts: 10.2 us -> 0.03 us
    ppermute x12, waiting for transfers between devices: 30.5 us -> 36.2 us  [along_z(): lax.ppermute(x, 'ep', [(i, 2 * (i // 2 ^ s) + i % 2) for i in range(ep)])]
    ppermute x12 -> x17, starting transfers between devices: 14.3 us -> 19.6 us  [along_tp(): return lax.ppermute(x, 'tp', [(i, i ^ s) for i in range(tp)])]
    ppermute x12 -> x17, waiting for transfers between devices: 29.8 us -> 24.6 us  [along_tp(): return lax.ppermute(x, 'tp', [(i, i ^ s) for i in range(tp)])]
    ppermute x12, starting transfers between devices: 26.6 us -> 22.6 us  [along_z(): lax.ppermute(x, 'ep', [(i, 2 * (i // 2 ^ s) + i % 2) for i in range(ep)])]
    pallas_call x3 -> x4, Pallas kernels: 5.1 us -> 7.68 us  [the longest x2 6.6 us: run_expert(): pl.pallas_call(lambda *refs: expert_kernel(*refs, pieces=pieces, halves=h...]
    ppermute x3 -> x6, waiting for transfers between devices: 0.01 us -> 1.73 us  [swap(): return lax.ppermute(x, 'ep', [(i, i ^ 1) for i in range(ep)])]
  transfers between devices with their start and end apart: 27 -> 35, of which waited for: 9 -> 15; matrix products, arithmetic and copies ran while one was open for 2% -> 1% of each run, Pallas kernels for 13% -> 15%
where the time goes in v1:
time: 132 us
  waiting for transfers between devices  62.5 us (47%)
  starting transfers between devices  43.5 us (33%)
  Pallas kernels  22.5 us (17%)
  other arithmetic  2.19 us (2%)
    ppermute x12, waiting for transfers between devices, along_z(): lax.ppermute(x, 'ep', [(i, 2 * (i // 2 ^ s) + i % 2) for i in range(ep)])  36.2 us
    ppermute x17, waiting for transfers between devices, along_tp(): return lax.ppermute(x, 'tp', [(i, i ^ s) for i in range(tp)])  24.6 us
    ppermute x12, starting transfers between devices, along_z(): lax.ppermute(x, 'ep', [(i, 2 * (i // 2 ^ s) + i % 2) for i in range(ep)])  22.6 us
    ppermute x17, starting transfers between devices, along_tp(): return lax.ppermute(x, 'tp', [(i, i ^ s) for i in range(tp)])  19.6 us
    pallas_call x1, Pallas kernels, inner(): pl.pallas_call(lambda *refs: attend_kernel(*refs, count=chips, rows=rows,...  9.95 us
    pallas_call x2, Pallas kernels, run_expert(): pl.pallas_call(lambda *refs: expert_kernel(*refs, pieces=pieces, halves=h...  6.6 us
  transfers between devices with their start and end apart: 35, of which 15 were waited for; matrix products, arithmetic and copies ran while one was open for 1% of the time, Pallas kernels for 15%

profile of v1, /device:TPU:0, one launch (start us, length us, event | category | flops | bytes accessed | tf_op | source)
XLA Modules:
  0.0 131.7 jit_solution(9705857883106604391)
XLA Ops:
  0.7 0.8 fusion
  1.4 1.9 %rope.1 = (bf16[1152,128]{1,0:T(8,128)(2,1)S(1)}, bf16[1152,128]{1,0:T(8,128)(2,1)S(1)}, bf16[1152,128]{1,0:T(8,128)(2,1)S(1)}, bf16[1152,128]{1,0:T(8,128)(2,1)S(1)}) custom-call(bf16[384,512]{1,0:T(8,128)(2,1)} %refs_0_.2, bf16[384,512]{1,0:T(8,128)(2,1)} %refs_1_.2, bf16[384,512]{1,0:T(8,128)(2,1)} %refs_2_.2, f32[384,128]{1,0:T(8,128)S(1)} %get-tuple-element.67.refs_3_, ...), custom_call_target="tpu_custom_call" | custom-call | flops 400000000 | tf_op jit(solution)/shard_map/rope/pallas_call | solution.py:520
  3.4 3.1 %collective-permute-start = (bf16[1152,128]{1,0:T(8,128)(2,1)S(1)}, bf16[1152,128]{1,0:T(8,128)(2,1)S(1)}, u32[]{:S(2)}, u32[]{:S(2)}) collective-permute-start(bf16[1152,128]{1,0:T(8,128)(2,1)S(1)} %get-tuple-element.31), channel_id=1, source_target_pairs={{0,8},{4,12},{8,0},{12,4},{16,24},{20,28},{24,16},{28,20},{1,9},{5... | collective-permute-start | bytes 884744 | tf_op jit(solution)/shard_map/ppermute | solution.py:444
  6.5 2.6 %collective-permute-start.1 = (bf16[1152,128]{1,0:T(8,128)(2,1)S(1)}, bf16[1152,128]{1,0:T(8,128)(2,1)S(1)}, u32[]{:S(2)}, u32[]{:S(2)}) collective-permute-start(bf16[1152,128]{1,0:T(8,128)(2,1)S(1)} %get-tuple-element.32), channel_id=1, source_target_pairs={{0,16},{4,20},{8,24},{12,28},{16,0},{20,4},{24,8},{28,12},{1,17},{... | collective-permute-start | bytes 884744 | tf_op jit(solution)/shard_map/ppermute | solution.py:444
  9.1 1.7 %dispatch.1 = (bf16[160,2048]{1,0:T(8,128)(2,1)S(1)}, s32[2,160]{1,0:T(2,128)S(1)}, bf16[100,512]{1,0:T(8,128)(2,1)S(1)}, bf16[100,512]{1,0:T(8,128)(2,1)S(1)}, ...) custom-call(bf16[160,2048]{1,0:T(8,128)(2,1)} %refs_0_.3, f32[1,2048]{1,0:T(1,128)} %bitcast.14, s32[2,160]{1,0:T(2,128)} %bitcast.15), custom_call_target="tpu_custom_call" | custom-call | flops 400000000 | tf_op jit(solution)/shard_map/dispatch/pallas_call | solution.py:489
  10.8 1.0 collective-permute-start.14
  11.8 3.5 %collective-permute-start.15 = (bf16[100,512]{1,0:T(8,128)(2,1)S(1)}, bf16[100,512]{1,0:T(8,128)(2,1)S(1)}, u32[]{:S(2)}, u32[]{:S(2)}) collective-permute-start(bf16[100,512]{1,0:T(8,128)(2,1)S(1)} %get-tuple-element.45), channel_id=1, source_target_pairs={{0,16},{4,20},{8,24},{12,28},{16,0},{20,4},{24,8},{28,12},{1,17},{... | collective-permute-start | bytes 307208 | tf_op jit(solution)/shard_map/ppermute | solution.py:444
  15.2 13.7 %collective-permute-done.14.refs_1_ = bf16[100,512]{1,0:T(8,128)(2,1)S(1)} collective-permute-done((bf16[100,512]{1,0:T(8,128)(2,1)S(1)}, bf16[100,512]{1,0:T(8,128)(2,1)S(1)}, u32[]{:S(2)}, u32[]{:S(2)}) %collective-permute-start.14) | collective-permute-done | bytes 102432 | tf_op jit(solution)/shard_map/ppermute | solution.py:444
  28.9 2.7 %collective-permute-start.16 = (bf16[100,512]{1,0:T(8,128)(2,1)S(1)}, bf16[100,512]{1,0:T(8,128)(2,1)S(1)}, u32[]{:S(2)}, u32[]{:S(2)}) collective-permute-start(bf16[100,512]{1,0:T(8,128)(2,1)S(1)} %get-tuple-element.46), channel_id=1, source_target_pairs={{0,24},{4,28},{8,16},{12,20},{16,8},{20,12},{24,0},{28,4},{1,25},{... | collective-permute-start | bytes 307208 | tf_op jit(solution)/shard_map/ppermute | solution.py:444
  31.6 11.3 %collective-permute-done.15.refs_2_ = bf16[100,512]{1,0:T(8,128)(2,1)S(1)} collective-permute-done((bf16[100,512]{1,0:T(8,128)(2,1)S(1)}, bf16[100,512]{1,0:T(8,128)(2,1)S(1)}, u32[]{:S(2)}, u32[]{:S(2)}) %collective-permute-start.15) | collective-permute-done | bytes 102432 | tf_op jit(solution)/shard_map/ppermute | solution.py:444
  42.9 0.5 collective-permute-start.4
  43.4 0.1 collective-permute-start.5
  43.4 0.4 collective-permute-start.6
  43.9 0.1 collective-permute-start.20
  44.1 0.4 collective-permute-done.3.refs_6_
  44.4 1.5 %collective-permute-start.17 = (bf16[200,512]{1,0:T(8,128)(2,1)S(1)}, bf16[200,512]{1,0:T(8,128)(2,1)S(1)}, u32[]{:S(2)}, u32[]{:S(2)}) collective-permute-start(bf16[200,512]{1,0:T(8,128)(2,1)S(1)} %get-tuple-element.47.refs_0_), channel_id=1, source_target_pairs={{0,1},{1,0},{2,3},{3,2},{4,5},{5,4},{6,7},{7,6},{8,9},{9,8},{10,11... | collective-permute-start | bytes 614408 | tf_op jit(solution)/shard_map/ppermute | solution.py:450
  45.9 0.1 collective-permute-done.20.refs_4_
  46.0 1.5 %collective-permute-start.22 = (bf16[200,512]{1,0:T(8,128)(2,1)S(1)}, bf16[200,512]{1,0:T(8,128)(2,1)S(1)}, u32[]{:S(2)}, u32[]{:S(2)}) collective-permute-start(bf16[200,512]{1,0:T(8,128)(2,1)S(1)} %collective-permute-done.20.refs_4_), channel_id=1, source_target_pairs={{0,2},{1,3},{2,0},{3,1},{4,6},{5,7},{6,4},{7,5},{8,10},{9,11},{10,... | collective-permute-start | bytes 614408 | tf_op jit(solution)/shard_map/ppermute | solution.py:450
  47.6 9.9 %attend.1 = (bf16[384,128]{1,0:T(8,128)(2,1)S(1)}, bf16[384,128]{1,0:T(8,128)(2,1)S(1)}, bf16[384,128]{1,0:T(8,128)(2,1)S(1)}, bf16[384,128]{1,0:T(8,128)(2,1)S(1)}) custom-call(f32[1,4]{1,0:T(1,128)S(1)} %bitcast.12, f32[1,128]{1,0:T(1,128)S(1)} %bitcast.13, bf16[1152,128]{1,0:T(8,128)(2,1)S(1)} %get-tuple-element.30.refs_2_, ...), custom_call_target="tpu_custom_call" | custom-call | flops 4000000000 | tf_op jit(solution)/shard_map/attend/pallas_call | solution.py:552
  57.5 0.3 collective-permute-start.7
  57.8 2.8 %collective-permute-start.8 = (bf16[384,128]{1,0:T(8,128)(2,1)S(1)}, bf16[384,128]{1,0:T(8,128)(2,1)S(1)}, u32[]{:S(2)}, u32[]{:S(2)}) collective-permute-start(bf16[384,128]{1,0:T(8,128)(2,1)S(1)} %get-tuple-element.36), channel_id=1, source_target_pairs={{0,16},{4,20},{8,24},{12,28},{16,0},{20,4},{24,8},{28,12},{1,17},{... | collective-permute-start | bytes 294920 | tf_op jit(solution)/shard_map/ppermute | solution.py:444
  60.6 1.3 %collective-permute-start.9 = (bf16[384,128]{1,0:T(8,128)(2,1)S(1)}, bf16[384,128]{1,0:T(8,128)(2,1)S(1)}, u32[]{:S(2)}, u32[]{:S(2)}) collective-permute-start(bf16[384,128]{1,0:T(8,128)(2,1)S(1)} %get-tuple-element.37), channel_id=1, source_target_pairs={{0,24},{4,28},{8,16},{12,20},{16,8},{20,12},{24,0},{28,4},{1,25},{... | collective-permute-start | bytes 294920 | tf_op jit(solution)/shard_map/ppermute | solution.py:444
  62.0 0.5 collective-permute-start.18
  62.5 1.5 %collective-permute-start.21 = (bf16[200,512]{1,0:T(8,128)(2,1)S(1)}, bf16[200,512]{1,0:T(8,128)(2,1)S(1)}, u32[]{:S(2)}, u32[]{:S(2)}) collective-permute-start(bf16[200,512]{1,0:T(8,128)(2,1)S(1)} %collective-permute-done.20.refs_4_), channel_id=1, source_target_pairs={{0,1},{1,0},{2,3},{3,2},{4,5},{5,4},{6,7},{7,6},{8,9},{9,8},{10,11... | collective-permute-start | bytes 614408 | tf_op jit(solution)/shard_map/ppermute | solution.py:450
  64.0 1.5 %collective-permute-start.19 = (bf16[200,512]{1,0:T(8,128)(2,1)S(1)}, bf16[200,512]{1,0:T(8,128)(2,1)S(1)}, u32[]{:S(2)}, u32[]{:S(2)}) collective-permute-start(bf16[200,512]{1,0:T(8,128)(2,1)S(1)} %collective-permute-done.17.refs_1_), channel_id=1, source_target_pairs={{0,2},{1,3},{2,0},{3,1},{4,6},{5,7},{6,4},{7,5},{8,10},{9,11},{10,... | collective-permute-start | bytes 614408 | tf_op jit(solution)/shard_map/ppermute | solution.py:450
  65.5 3.0 %collective-permute-done.8.refs_2_ = bf16[384,128]{1,0:T(8,128)(2,1)S(1)} collective-permute-done((bf16[384,128]{1,0:T(8,128)(2,1)S(1)}, bf16[384,128]{1,0:T(8,128)(2,1)S(1)}, u32[]{:S(2)}, u32[]{:S(2)}) %collective-permute-start.8) | collective-permute-done | bytes 98336 | tf_op jit(solution)/shard_map/ppermute | solution.py:444
  68.5 1.4 %collective-permute-start.23 = (bf16[200,512]{1,0:T(8,128)(2,1)S(1)}, bf16[200,512]{1,0:T(8,128)(2,1)S(1)}, u32[]{:S(2)}, u32[]{:S(2)}) collective-permute-start(bf16[200,512]{1,0:T(8,128)(2,1)S(1)} %collective-permute-done.22.refs_6_), channel_id=1, source_target_pairs={{0,1},{1,0},{2,3},{3,2},{4,5},{5,4},{6,7},{7,6},{8,9},{9,8},{10,11... | collective-permute-start | bytes 614408 | tf_op jit(solution)/shard_map/ppermute | solution.py:450
  69.9 1.0 project.1
  70.9 0.7 collective-permute-start.10
  71.7 3.6 %shard_map.168 = (bf16[160,512]{1,0:T(8,128)(2,1)S(1)}, bf16[160,512]{1,0:T(8,128)(2,1)S(1)}, bf16[160,512]{1,0:T(8,128)(2,1)S(1)}, bf16[160,512]{1,0:T(8,128)(2,1)S(1)}) custom-call(bf16[160,2048]{1,0:T(8,128)(2,1)S(1)} %get-tuple-element.53.refs_0_, bf16[2048,512]{1,0:T(8,128)(2,1)} %refs_1_.3, bf16[2048,512]{1,0:T(8,128)(2,1)} %refs_2_.3, ...), custom_call_target="tpu_custom_call" | custom-call | flops 1006632960 | tf_op jit(solution)/shard_map/pallas_call | solution.py:180
  75.3 1.4 %collective-permute-start.32 = (bf16[160,512]{1,0:T(8,128)(2,1)S(1)}, bf16[160,512]{1,0:T(8,128)(2,1)S(1)}, u32[]{:S(2)}, u32[]{:S(2)}) collective-permute-start(bf16[160,512]{1,0:T(8,128)(2,1)S(1)} %get-tuple-element.55), channel_id=1, source_target_pairs={{0,1},{1,0},{2,3},{3,2},{4,5},{5,4},{6,7},{7,6},{8,9},{9,8},{10,11... | collective-permute-start | bytes 491528 | tf_op jit(solution)/shard_map/ppermute | solution.py:450
  76.7 0.5 collective-permute-start.33
  77.2 1.6 %collective-permute-start.34 = (bf16[160,512]{1,0:T(8,128)(2,1)S(1)}, bf16[160,512]{1,0:T(8,128)(2,1)S(1)}, u32[]{:S(2)}, u32[]{:S(2)}) collective-permute-start(bf16[160,512]{1,0:T(8,128)(2,1)S(1)} %get-tuple-element.57), channel_id=1, source_target_pairs={{0,3},{1,2},{2,1},{3,0},{4,7},{5,6},{6,5},{7,4},{8,11},{9,10},{10,... | collective-permute-start | bytes 491528 | tf_op jit(solution)/shard_map/ppermute | solution.py:450
  78.9 0.5 collective-permute-start.12
  79.4 3.0 %shard_map.167 = (bf16[400,512]{1,0:T(8,128)(2,1)S(1)}, bf16[400,512]{1,0:T(8,128)(2,1)S(1)}, bf16[400,512]{1,0:T(8,128)(2,1)S(1)}, bf16[400,512]{1,0:T(8,128)(2,1)S(1)}) custom-call(bf16[200,512]{1,0:T(8,128)(2,1)S(1)} %get-tuple-element.47.refs_0_, bf16[200,512]{1,0:T(8,128)(2,1)S(1)} %collective-permute-done.17.refs_1_, ...), custom_call_target="tpu_custom_call" | custom-call | flops 2516582400 | tf_op jit(solution)/shard_map/pallas_call | solution.py:180
  82.4 2.5 %collective-permute-done.10 = bf16[384,512]{1,0:T(8,128)(2,1)S(1)} collective-permute-done((bf16[384,512]{1,0:T(8,128)(2,1)S(1)}, bf16[384,512]{1,0:T(8,128)(2,1)S(1)}, u32[]{:S(2)}, u32[]{:S(2)}) %collective-permute-start.10) | collective-permute-done | bytes 393248 | tf_op jit(solution)/shard_map/ppermute | solution.py:450
  84.9 1.4 %collective-permute-start.24 = (bf16[400,512]{1,0:T(8,128)(2,1)S(1)}, bf16[400,512]{1,0:T(8,128)(2,1)S(1)}, u32[]{:S(2)}, u32[]{:S(2)}) collective-permute-start(bf16[400,512]{1,0:T(8,128)(2,1)S(1)} %get-tuple-element.50), channel_id=1, source_target_pairs={{0,1},{1,0},{2,3},{3,2},{4,5},{5,4},{6,7},{7,6},{8,9},{9,8},{10,11... | collective-permute-start | bytes 1228808 | tf_op jit(solution)/shard_map/ppermute | solution.py:450
  86.3 0.1 add_convert_fusion.7
  86.3 7.8 %collective-permute-done.12 = bf16[384,512]{1,0:T(8,128)(2,1)S(1)} collective-permute-done((bf16[384,512]{1,0:T(8,128)(2,1)S(1)}, bf16[384,512]{1,0:T(8,128)(2,1)S(1)}, u32[]{:S(2)}, u32[]{:S(2)}) %collective-permute-start.12) | collective-permute-done | bytes 393248 | tf_op jit(solution)/shard_map/ppermute | solution.py:450
  94.1 0.1 add_convert_fusion.5
  94.2 2.7 %collective-permute-done.24 = bf16[400,512]{1,0:T(8,128)(2,1)S(1)} collective-permute-done((bf16[400,512]{1,0:T(8,128)(2,1)S(1)}, bf16[400,512]{1,0:T(8,128)(2,1)S(1)}, u32[]{:S(2)}, u32[]{:S(2)}) %collective-permute-start.24) | collective-permute-done | bytes 409632 | tf_op jit(solution)/shard_map/ppermute | solution.py:450
  96.9 1.5 %collective-permute-start.11 = (bf16[192,512]{1,0:T(8,128)(2,1)S(1)}, bf16[192,512]{1,0:T(8,128)(2,1)S(1)}, u32[]{:S(2)}, u32[]{:S(2)}) collective-permute-start(bf16[192,512]{1,0:T(8,128)(2,1)S(1)} %add_convert_fusion.7), channel_id=1, source_target_pairs={{0,2},{1,3},{2,0},{3,1},{4,6},{5,7},{6,4},{7,5},{8,10},{9,11},{10,... | collective-permute-start | bytes 589832 | tf_op jit(solution)/shard_map/ppermute | solution.py:450
  98.3 0.1 add_convert_fusion.3
  98.4 4.5 %collective-permute-done.26 = bf16[400,512]{1,0:T(8,128)(2,1)S(1)} collective-permute-done((bf16[400,512]{1,0:T(8,128)(2,1)S(1)}, bf16[400,512]{1,0:T(8,128)(2,1)S(1)}, u32[]{:S(2)}, u32[]{:S(2)}) %collective-permute-start.26) | collective-permute-done | bytes 409632 | tf_op jit(solution)/shard_map/ppermute | solution.py:450
  102.9 1.6 %collective-permute-start.13 = (bf16[192,512]{1,0:T(8,128)(2,1)S(1)}, bf16[192,512]{1,0:T(8,128)(2,1)S(1)}, u32[]{:S(2)}, u32[]{:S(2)}) collective-permute-start(bf16[192,512]{1,0:T(8,128)(2,1)S(1)} %add_convert_fusion.5), channel_id=1, source_target_pairs={{0,1},{1,0},{2,3},{3,2},{4,5},{5,4},{6,7},{7,6},{8,9},{9,8},{10,11... | collective-permute-start | bytes 589832 | tf_op jit(solution)/shard_map/ppermute | solution.py:450
  104.6 0.1 add_convert_fusion.1
  104.6 2.1 %collective-permute-done.11 = bf16[192,512]{1,0:T(8,128)(2,1)S(1)} collective-permute-done((bf16[192,512]{1,0:T(8,128)(2,1)S(1)}, bf16[192,512]{1,0:T(8,128)(2,1)S(1)}, u32[]{:S(2)}, u32[]{:S(2)}) %collective-permute-start.11) | collective-permute-done | bytes 196640 | tf_op jit(solution)/shard_map/ppermute | solution.py:450
  106.7 0.8 collective-permute-start.25
  107.5 0.1 add_convert_fusion.6
  107.6 1.7 %collective-permute-done.13 = bf16[192,512]{1,0:T(8,128)(2,1)S(1)} collective-permute-done((bf16[192,512]{1,0:T(8,128)(2,1)S(1)}, bf16[192,512]{1,0:T(8,128)(2,1)S(1)}, u32[]{:S(2)}, u32[]{:S(2)}) %collective-permute-start.13) | collective-permute-done | bytes 196640 | tf_op jit(solution)/shard_map/ppermute | solution.py:450
  109.3 1.6 %collective-permute-start.27 = (bf16[200,512]{1,0:T(8,128)(2,1)S(1)}, bf16[200,512]{1,0:T(8,128)(2,1)S(1)}, u32[]{:S(2)}, u32[]{:S(2)}) collective-permute-start(bf16[200,512]{1,0:T(8,128)(2,1)S(1)} %add_convert_fusion.1), channel_id=1, source_target_pairs={{0,1},{1,0},{2,3},{3,2},{4,5},{5,4},{6,7},{7,6},{8,9},{9,8},{10,11... | collective-permute-start | bytes 614408 | tf_op jit(solution)/shard_map/ppermute | solution.py:450
  110.9 0.1 add_convert_fusion.4
  111.0 0.8 pad_maximum_fusion
  111.8 3.3 %collective-permute-done.27 = bf16[200,512]{1,0:T(8,128)(2,1)S(1)} collective-permute-done((bf16[200,512]{1,0:T(8,128)(2,1)S(1)}, bf16[200,512]{1,0:T(8,128)(2,1)S(1)}, u32[]{:S(2)}, u32[]{:S(2)}) %collective-permute-start.27) | collective-permute-done | bytes 204832 | tf_op jit(solution)/shard_map/ppermute | solution.py:450
  115.0 0.1 add_convert_fusion
  115.1 0.1 collective-permute-start.28
  115.2 0.1 add_convert_fusion.2
  115.3 1.3 collective-permute-done.28
  116.7 2.7 %collective-permute-start.31 = (bf16[100,512]{1,0:T(8,128)(2,1)S(1)}, bf16[100,512]{1,0:T(8,128)(2,1)S(1)}, u32[]{:S(2)}, u32[]{:S(2)}) collective-permute-start(bf16[100,512]{1,0:T(8,128)(2,1)S(1)} %pad_maximum_fusion.4), channel_id=1, source_target_pairs={{0,24},{4,28},{8,16},{12,20},{16,8},{20,12},{24,0},{28,4},{1,25},{... | collective-permute-start | bytes 307208 | tf_op jit(solution)/shard_map/ppermute | solution.py:444
  119.4 2.6 %collective-permute-start.30 = (bf16[100,512]{1,0:T(8,128)(2,1)S(1)}, bf16[100,512]{1,0:T(8,128)(2,1)S(1)}, u32[]{:S(2)}, u32[]{:S(2)}) collective-permute-start(bf16[100,512]{1,0:T(8,128)(2,1)S(1)} %pad_maximum_fusion.3), channel_id=1, source_target_pairs={{0,16},{4,20},{8,24},{12,28},{16,0},{20,4},{24,8},{28,12},{1,17},{... | collective-permute-start | bytes 307208 | tf_op jit(solution)/shard_map/ppermute | solution.py:444
  122.1 0.1 collective-permute-start.29
  122.2 1.5 %collective-permute-done.31.refs_5_ = bf16[100,512]{1,0:T(8,128)(2,1)S(1)} collective-permute-done((bf16[100,512]{1,0:T(8,128)(2,1)S(1)}, bf16[100,512]{1,0:T(8,128)(2,1)S(1)}, u32[]{:S(2)}, u32[]{:S(2)}) %collective-permute-start.31) | collective-permute-done | bytes 102432 | tf_op jit(solution)/shard_map/ppermute | solution.py:444
  123.7 6.7 %collective-permute-done.30.refs_4_ = bf16[100,512]{1,0:T(8,128)(2,1)S(1)} collective-permute-done((bf16[100,512]{1,0:T(8,128)(2,1)S(1)}, bf16[100,512]{1,0:T(8,128)(2,1)S(1)}, u32[]{:S(2)}, u32[]{:S(2)}) %collective-permute-start.30) | collective-permute-done | bytes 102432 | tf_op jit(solution)/shard_map/ppermute | solution.py:444
  130.4 1.3 combine.1
  (46 shorter events, 0.3 us)
Async XLA Ops:
  0.6 46.9 %copy-start.5 = (f32[4]{0:T(128)S(1)}, f32[4]{0:T(128)}, u32[]{:S(2)}) copy-start(f32[4]{0:T(128)} %param.19) | copy-start | bytes 52
  0.6 46.9 %copy-start.6 = (f32[128]{0:T(128)S(1)}, f32[128]{0:T(128)}, u32[]{:S(2)}) copy-start(f32[128]{0:T(128)} %param.20) | copy-start | bytes 1540
  3.4 39.5 %collective-permute-start = (bf16[1152,128]{1,0:T(8,128)(2,1)S(1)}, bf16[1152,128]{1,0:T(8,128)(2,1)S(1)}, u32[]{:S(2)}, u32[]{:S(2)}) collective-permute-start(bf16[1152,128]{1,0:T(8,128)(2,1)S(1)} %get-tuple-element.31), channel_id=1, source_target_pairs={{0,8},{4,12},{8,0},{12,4},{16,24},{20,28},{24,16},{28,20},{1,9},{5... | collective-permute-start | bytes 884744 | tf_op jit(solution)/shard_map/ppermute | solution.py:444
  6.5 36.9 %collective-permute-start.1 = (bf16[1152,128]{1,0:T(8,128)(2,1)S(1)}, bf16[1152,128]{1,0:T(8,128)(2,1)S(1)}, u32[]{:S(2)}, u32[]{:S(2)}) collective-permute-start(bf16[1152,128]{1,0:T(8,128)(2,1)S(1)} %get-tuple-element.32), channel_id=1, source_target_pairs={{0,16},{4,20},{8,24},{12,28},{16,0},{20,4},{24,8},{28,12},{1,17},{... | collective-permute-start | bytes 884744 | tf_op jit(solution)/shard_map/ppermute | solution.py:444
  9.1 34.4 %collective-permute-start.2 = (bf16[1152,128]{1,0:T(8,128)(2,1)S(1)}, bf16[1152,128]{1,0:T(8,128)(2,1)S(1)}, u32[]{:S(2)}, u32[]{:S(2)}) collective-permute-start(bf16[1152,128]{1,0:T(8,128)(2,1)S(1)} %get-tuple-element.33), channel_id=1, source_target_pairs={{0,24},{4,28},{8,16},{12,20},{16,8},{20,12},{24,0},{28,4},{1,25},{... | collective-permute-start | bytes 884744 | tf_op jit(solution)/shard_map/ppermute | solution.py:444
  10.8 18.1 %collective-permute-start.14 = (bf16[100,512]{1,0:T(8,128)(2,1)S(1)}, bf16[100,512]{1,0:T(8,128)(2,1)S(1)}, u32[]{:S(2)}, u32[]{:S(2)}) collective-permute-start(bf16[100,512]{1,0:T(8,128)(2,1)S(1)} %get-tuple-element.44), channel_id=1, source_target_pairs={{0,8},{4,12},{8,0},{12,4},{16,24},{20,28},{24,16},{28,20},{1,9},{5... | collective-permute-start | bytes 307208 | tf_op jit(solution)/shard_map/ppermute | solution.py:444
  11.8 31.1 %collective-permute-start.15 = (bf16[100,512]{1,0:T(8,128)(2,1)S(1)}, bf16[100,512]{1,0:T(8,128)(2,1)S(1)}, u32[]{:S(2)}, u32[]{:S(2)}) collective-permute-start(bf16[100,512]{1,0:T(8,128)(2,1)S(1)} %get-tuple-element.45), channel_id=1, source_target_pairs={{0,16},{4,20},{8,24},{12,28},{16,0},{20,4},{24,8},{28,12},{1,17},{... | collective-permute-start | bytes 307208 | tf_op jit(solution)/shard_map/ppermute | solution.py:444
  28.9 15.0 %collective-permute-start.16 = (bf16[100,512]{1,0:T(8,128)(2,1)S(1)}, bf16[100,512]{1,0:T(8,128)(2,1)S(1)}, u32[]{:S(2)}, u32[]{:S(2)}) collective-permute-start(bf16[100,512]{1,0:T(8,128)(2,1)S(1)} %get-tuple-element.46), channel_id=1, source_target_pairs={{0,24},{4,28},{8,16},{12,20},{16,8},{20,12},{24,0},{28,4},{1,25},{... | collective-permute-start | bytes 307208 | tf_op jit(solution)/shard_map/ppermute | solution.py:444
  42.9 1.6 %collective-permute-start.3 = (bf16[1152,128]{1,0:T(8,128)(2,1)S(1)}, bf16[1152,128]{1,0:T(8,128)(2,1)S(1)}, u32[]{:S(2)}, u32[]{:S(2)}) collective-permute-start(bf16[1152,128]{1,0:T(8,128)(2,1)S(1)} %get-tuple-element.30.refs_2_), channel_id=1, source_target_pairs={{0,4},{4,0},{8,12},{12,8},{16,20},{20,16},{24,28},{28,24},{1,5},{5... | collective-permute-start | bytes 884744 | tf_op jit(solution)/shard_map/ppermute | solution.py:447
  42.9 4.7 %collective-permute-start.4 = (bf16[1152,128]{1,0:T(8,128)(2,1)S(1)}, bf16[1152,128]{1,0:T(8,128)(2,1)S(1)}, u32[]{:S(2)}, u32[]{:S(2)}) collective-permute-start(bf16[1152,128]{1,0:T(8,128)(2,1)S(1)} %collective-permute-done.refs_3_), channel_id=1, source_target_pairs={{0,4},{4,0},{8,12},{12,8},{16,20},{20,16},{24,28},{28,24},{1,5},{5... | collective-permute-start | bytes 884744 | tf_op jit(solution)/shard_map/ppermute | solution.py:447
  43.4 4.1 %collective-permute-start.5 = (bf16[1152,128]{1,0:T(8,128)(2,1)S(1)}, bf16[1152,128]{1,0:T(8,128)(2,1)S(1)}, u32[]{:S(2)}, u32[]{:S(2)}) collective-permute-start(bf16[1152,128]{1,0:T(8,128)(2,1)S(1)} %collective-permute-done.1.refs_4_), channel_id=1, source_target_pairs={{0,4},{4,0},{8,12},{12,8},{16,20},{20,16},{24,28},{28,24},{1,5},{5... | collective-permute-start | bytes 884744 | tf_op jit(solution)/shard_map/ppermute | solution.py:447
  43.4 4.1 %collective-permute-start.6 = (bf16[1152,128]{1,0:T(8,128)(2,1)S(1)}, bf16[1152,128]{1,0:T(8,128)(2,1)S(1)}, u32[]{:S(2)}, u32[]{:S(2)}) collective-permute-start(bf16[1152,128]{1,0:T(8,128)(2,1)S(1)} %collective-permute-done.2.refs_5_), channel_id=1, source_target_pairs={{0,4},{4,0},{8,12},{12,8},{16,20},{20,16},{24,28},{28,24},{1,5},{5... | collective-permute-start | bytes 884744 | tf_op jit(solution)/shard_map/ppermute | solution.py:447
  43.9 2.1 %collective-permute-start.20 = (bf16[200,512]{1,0:T(8,128)(2,1)S(1)}, bf16[200,512]{1,0:T(8,128)(2,1)S(1)}, u32[]{:S(2)}, u32[]{:S(2)}) collective-permute-start(bf16[200,512]{1,0:T(8,128)(2,1)S(1)} %get-tuple-element.48), channel_id=1, source_target_pairs={{0,4},{4,0},{8,12},{12,8},{16,20},{20,16},{24,28},{28,24},{1,5},{5... | collective-permute-start | bytes 614408 | tf_op jit(solution)/shard_map/ppermute | solution.py:447
  44.4 17.5 %collective-permute-start.17 = (bf16[200,512]{1,0:T(8,128)(2,1)S(1)}, bf16[200,512]{1,0:T(8,128)(2,1)S(1)}, u32[]{:S(2)}, u32[]{:S(2)}) collective-permute-start(bf16[200,512]{1,0:T(8,128)(2,1)S(1)} %get-tuple-element.47.refs_0_), channel_id=1, source_target_pairs={{0,1},{1,0},{2,3},{3,2},{4,5},{5,4},{6,7},{7,6},{8,9},{9,8},{10,11... | collective-permute-start | bytes 614408 | tf_op jit(solution)/shard_map/ppermute | solution.py:450
  46.0 16.5 %collective-permute-start.22 = (bf16[200,512]{1,0:T(8,128)(2,1)S(1)}, bf16[200,512]{1,0:T(8,128)(2,1)S(1)}, u32[]{:S(2)}, u32[]{:S(2)}) collective-permute-start(bf16[200,512]{1,0:T(8,128)(2,1)S(1)} %collective-permute-done.20.refs_4_), channel_id=1, source_target_pairs={{0,2},{1,3},{2,0},{3,1},{4,6},{5,7},{6,4},{7,5},{8,10},{9,11},{10,... | collective-permute-start | bytes 614408 | tf_op jit(solution)/shard_map/ppermute | solution.py:450
  47.5 22.3 %copy-start = (bf16[512,2048]{1,0:T(8,128)(2,1)S(1)}, bf16[512,2048]{1,0:T(8,128)(2,1)}, u32[]{:S(2)}) copy-start(bf16[512,2048]{1,0:T(8,128)(2,1)} %refs_4_.1) | copy-start | bytes 6291460
  57.5 6.5 %collective-permute-start.7 = (bf16[384,128]{1,0:T(8,128)(2,1)S(1)}, bf16[384,128]{1,0:T(8,128)(2,1)S(1)}, u32[]{:S(2)}, u32[]{:S(2)}) collective-permute-start(bf16[384,128]{1,0:T(8,128)(2,1)S(1)} %get-tuple-element.35), channel_id=1, source_target_pairs={{0,8},{4,12},{8,0},{12,4},{16,24},{20,28},{24,16},{28,20},{1,9},{5... | collective-permute-start | bytes 294920 | tf_op jit(solution)/shard_map/ppermute | solution.py:444
  57.8 10.7 %collective-permute-start.8 = (bf16[384,128]{1,0:T(8,128)(2,1)S(1)}, bf16[384,128]{1,0:T(8,128)(2,1)S(1)}, u32[]{:S(2)}, u32[]{:S(2)}) collective-permute-start(bf16[384,128]{1,0:T(8,128)(2,1)S(1)} %get-tuple-element.36), channel_id=1, source_target_pairs={{0,16},{4,20},{8,24},{12,28},{16,0},{20,4},{24,8},{28,12},{1,17},{... | collective-permute-start | bytes 294920 | tf_op jit(solution)/shard_map/ppermute | solution.py:444
  60.6 9.3 %collective-permute-start.9 = (bf16[384,128]{1,0:T(8,128)(2,1)S(1)}, bf16[384,128]{1,0:T(8,128)(2,1)S(1)}, u32[]{:S(2)}, u32[]{:S(2)}) collective-permute-start(bf16[384,128]{1,0:T(8,128)(2,1)S(1)} %get-tuple-element.37), channel_id=1, source_target_pairs={{0,24},{4,28},{8,16},{12,20},{16,8},{20,12},{24,0},{28,4},{1,25},{... | collective-permute-start | bytes 294920 | tf_op jit(solution)/shard_map/ppermute | solution.py:444
  62.0 13.3 %collective-permute-start.18 = (bf16[200,512]{1,0:T(8,128)(2,1)S(1)}, bf16[200,512]{1,0:T(8,128)(2,1)S(1)}, u32[]{:S(2)}, u32[]{:S(2)}) collective-permute-start(bf16[200,512]{1,0:T(8,128)(2,1)S(1)} %get-tuple-element.47.refs_0_), channel_id=1, source_target_pairs={{0,2},{1,3},{2,0},{3,1},{4,6},{5,7},{6,4},{7,5},{8,10},{9,11},{10,... | collective-permute-start | bytes 614408 | tf_op jit(solution)/shard_map/ppermute | solution.py:450
  62.5 14.7 %collective-permute-start.21 = (bf16[200,512]{1,0:T(8,128)(2,1)S(1)}, bf16[200,512]{1,0:T(8,128)(2,1)S(1)}, u32[]{:S(2)}, u32[]{:S(2)}) collective-permute-start(bf16[200,512]{1,0:T(8,128)(2,1)S(1)} %collective-permute-done.20.refs_4_), channel_id=1, source_target_pairs={{0,1},{1,0},{2,3},{3,2},{4,5},{5,4},{6,7},{7,6},{8,9},{9,8},{10,11... | collective-permute-start | bytes 614408 | tf_op jit(solution)/shard_map/ppermute | solution.py:450
  64.0 12.7 %collective-permute-start.19 = (bf16[200,512]{1,0:T(8,128)(2,1)S(1)}, bf16[200,512]{1,0:T(8,128)(2,1)S(1)}, u32[]{:S(2)}, u32[]{:S(2)}) collective-permute-start(bf16[200,512]{1,0:T(8,128)(2,1)S(1)} %collective-permute-done.17.refs_1_), channel_id=1, source_target_pairs={{0,2},{1,3},{2,0},{3,1},{4,6},{5,7},{6,4},{7,5},{8,10},{9,11},{10,... | collective-permute-start | bytes 614408 | tf_op jit(solution)/shard_map/ppermute | solution.py:450
  68.5 10.3 %collective-permute-start.23 = (bf16[200,512]{1,0:T(8,128)(2,1)S(1)}, bf16[200,512]{1,0:T(8,128)(2,1)S(1)}, u32[]{:S(2)}, u32[]{:S(2)}) collective-permute-start(bf16[200,512]{1,0:T(8,128)(2,1)S(1)} %collective-permute-done.22.refs_6_), channel_id=1, source_target_pairs={{0,1},{1,0},{2,3},{3,2},{4,5},{5,4},{6,7},{7,6},{8,9},{9,8},{10,11... | collective-permute-start | bytes 614408 | tf_op jit(solution)/shard_map/ppermute | solution.py:450
  70.9 14.0 %collective-permute-start.10 = (bf16[384,512]{1,0:T(8,128)(2,1)S(1)}, bf16[384,512]{1,0:T(8,128)(2,1)S(1)}, u32[]{:S(2)}, u32[]{:S(2)}) collective-permute-start(bf16[384,512]{1,0:T(8,128)(2,1)S(1)} %get-tuple-element.39), channel_id=1, source_target_pairs={{0,1},{1,0},{2,3},{3,2},{4,5},{5,4},{6,7},{7,6},{8,9},{9,8},{10,11... | collective-permute-start | bytes 1179656 | tf_op jit(solution)/shard_map/ppermute | solution.py:450
  71.7 7.7 %copy-start.1 = (bf16[1,2048,512]{2,1,0:T(8,128)(2,1)S(1)}, bf16[1,2048,512]{2,1,0:T(8,128)(2,1)}, u32[]{:S(2)}) copy-start(bf16[1,2048,512]{2,1,0:T(8,128)(2,1)} %param.26) | copy-start | bytes 6291460
  71.7 7.7 %copy-start.2 = (bf16[1,2048,512]{2,1,0:T(8,128)(2,1)S(1)}, bf16[1,2048,512]{2,1,0:T(8,128)(2,1)}, u32[]{:S(2)}) copy-start(bf16[1,2048,512]{2,1,0:T(8,128)(2,1)} %param.27) | copy-start | bytes 6291460
  71.7 7.7 %copy-start.3 = (bf16[1,512,2048]{2,1,0:T(8,128)(2,1)S(1)}, bf16[1,512,2048]{2,1,0:T(8,128)(2,1)}, u32[]{:S(2)}) copy-start(bf16[1,512,2048]{2,1,0:T(8,128)(2,1)} %param.28) | copy-start | bytes 6291460
  75.3 46.8 %collective-permute-start.32 = (bf16[160,512]{1,0:T(8,128)(2,1)S(1)}, bf16[160,512]{1,0:T(8,128)(2,1)S(1)}, u32[]{:S(2)}, u32[]{:S(2)}) collective-permute-start(bf16[160,512]{1,0:T(8,128)(2,1)S(1)} %get-tuple-element.55), channel_id=1, source_target_pairs={{0,1},{1,0},{2,3},{3,2},{4,5},{5,4},{6,7},{7,6},{8,9},{9,8},{10,11... | collective-permute-start | bytes 491528 | tf_op jit(solution)/shard_map/ppermute | solution.py:450
  76.7 45.5 %collective-permute-start.33 = (bf16[160,512]{1,0:T(8,128)(2,1)S(1)}, bf16[160,512]{1,0:T(8,128)(2,1)S(1)}, u32[]{:S(2)}, u32[]{:S(2)}) collective-permute-start(bf16[160,512]{1,0:T(8,128)(2,1)S(1)} %get-tuple-element.56), channel_id=1, source_target_pairs={{0,2},{1,3},{2,0},{3,1},{4,6},{5,7},{6,4},{7,5},{8,10},{9,11},{10,... | collective-permute-start | bytes 491528 | tf_op jit(solution)/shard_map/ppermute | solution.py:450
  77.2 45.0 %collective-permute-start.34 = (bf16[160,512]{1,0:T(8,128)(2,1)S(1)}, bf16[160,512]{1,0:T(8,128)(2,1)S(1)}, u32[]{:S(2)}, u32[]{:S(2)}) collective-permute-start(bf16[160,512]{1,0:T(8,128)(2,1)S(1)} %get-tuple-element.57), channel_id=1, source_target_pairs={{0,3},{1,2},{2,1},{3,0},{4,7},{5,6},{6,5},{7,4},{8,11},{9,10},{10,... | collective-permute-start | bytes 491528 | tf_op jit(solution)/shard_map/ppermute | solution.py:450
  78.9 15.3 %collective-permute-start.12 = (bf16[384,512]{1,0:T(8,128)(2,1)S(1)}, bf16[384,512]{1,0:T(8,128)(2,1)S(1)}, u32[]{:S(2)}, u32[]{:S(2)}) collective-permute-start(bf16[384,512]{1,0:T(8,128)(2,1)S(1)} %get-tuple-element.41), channel_id=1, source_target_pairs={{0,2},{1,3},{2,0},{3,1},{4,6},{5,7},{6,4},{7,5},{8,10},{9,11},{10,... | collective-permute-start | bytes 1179656 | tf_op jit(solution)/shard_map/ppermute | solution.py:450
  84.9 12.0 %collective-permute-start.24 = (bf16[400,512]{1,0:T(8,128)(2,1)S(1)}, bf16[400,512]{1,0:T(8,128)(2,1)S(1)}, u32[]{:S(2)}, u32[]{:S(2)}) collective-permute-start(bf16[400,512]{1,0:T(8,128)(2,1)S(1)} %get-tuple-element.50), channel_id=1, source_target_pairs={{0,1},{1,0},{2,3},{3,2},{4,5},{5,4},{6,7},{7,6},{8,9},{9,8},{10,11... | collective-permute-start | bytes 1228808 | tf_op jit(solution)/shard_map/ppermute | solution.py:450
  94.1 8.8 %collective-permute-start.26 = (bf16[400,512]{1,0:T(8,128)(2,1)S(1)}, bf16[400,512]{1,0:T(8,128)(2,1)S(1)}, u32[]{:S(2)}, u32[]{:S(2)}) collective-permute-start(bf16[400,512]{1,0:T(8,128)(2,1)S(1)} %get-tuple-element.52), channel_id=1, source_target_pairs={{0,2},{1,3},{2,0},{3,1},{4,6},{5,7},{6,4},{7,5},{8,10},{9,11},{10,... | collective-permute-start | bytes 1228808 | tf_op jit(solution)/shard_map/ppermute | solution.py:450
  96.9 9.9 %collective-permute-start.11 = (bf16[192,512]{1,0:T(8,128)(2,1)S(1)}, bf16[192,512]{1,0:T(8,128)(2,1)S(1)}, u32[]{:S(2)}, u32[]{:S(2)}) collective-permute-start(bf16[192,512]{1,0:T(8,128)(2,1)S(1)} %add_convert_fusion.7), channel_id=1, source_target_pairs={{0,2},{1,3},{2,0},{3,1},{4,6},{5,7},{6,4},{7,5},{8,10},{9,11},{10,... | collective-permute-start | bytes 589832 | tf_op jit(solution)/shard_map/ppermute | solution.py:450
  102.9 6.3 %collective-permute-start.13 = (bf16[192,512]{1,0:T(8,128)(2,1)S(1)}, bf16[192,512]{1,0:T(8,128)(2,1)S(1)}, u32[]{:S(2)}, u32[]{:S(2)}) collective-permute-start(bf16[192,512]{1,0:T(8,128)(2,1)S(1)} %add_convert_fusion.5), channel_id=1, source_target_pairs={{0,1},{1,0},{2,3},{3,2},{4,5},{5,4},{6,7},{7,6},{8,9},{9,8},{10,11... | collective-permute-start | bytes 589832 | tf_op jit(solution)/shard_map/ppermute | solution.py:450
  106.7 8.5 %collective-permute-start.25 = (bf16[200,512]{1,0:T(8,128)(2,1)S(1)}, bf16[200,512]{1,0:T(8,128)(2,1)S(1)}, u32[]{:S(2)}, u32[]{:S(2)}) collective-permute-start(bf16[200,512]{1,0:T(8,128)(2,1)S(1)} %add_convert_fusion.3), channel_id=1, source_target_pairs={{0,2},{1,3},{2,0},{3,1},{4,6},{5,7},{6,4},{7,5},{8,10},{9,11},{10,... | collective-permute-start | bytes 614408 | tf_op jit(solution)/shard_map/ppermute | solution.py:450
  109.3 5.8 %collective-permute-start.27 = (bf16[200,512]{1,0:T(8,128)(2,1)S(1)}, bf16[200,512]{1,0:T(8,128)(2,1)S(1)}, u32[]{:S(2)}, u32[]{:S(2)}) collective-permute-start(bf16[200,512]{1,0:T(8,128)(2,1)S(1)} %add_convert_fusion.1), channel_id=1, source_target_pairs={{0,1},{1,0},{2,3},{3,2},{4,5},{5,4},{6,7},{7,6},{8,9},{9,8},{10,11... | collective-permute-start | bytes 614408 | tf_op jit(solution)/shard_map/ppermute | solution.py:450
  111.0 19.4 %copy-start.4 = (f32[160,2]{0,1:T(2,128)S(1)}, f32[160,2]{0,1:T(2,128)}, u32[]{:S(2)}) copy-start(f32[160,2]{0,1:T(2,128)} %param.25) | copy-start | bytes 3844
  115.1 1.5 %collective-permute-start.28 = (bf16[200,512]{1,0:T(8,128)(2,1)S(1)}, bf16[200,512]{1,0:T(8,128)(2,1)S(1)}, u32[]{:S(2)}, u32[]{:S(2)}) collective-permute-start(bf16[200,512]{1,0:T(8,128)(2,1)S(1)} %add_convert_fusion), channel_id=1, source_target_pairs={{0,4},{4,0},{8,12},{12,8},{16,20},{20,16},{24,28},{28,24},{1,5},{5... | collective-permute-start | bytes 614408 | tf_op jit(solution)/shard_map/ppermute | solution.py:447
  116.7 7.0 %collective-permute-start.31 = (bf16[100,512]{1,0:T(8,128)(2,1)S(1)}, bf16[100,512]{1,0:T(8,128)(2,1)S(1)}, u32[]{:S(2)}, u32[]{:S(2)}) collective-permute-start(bf16[100,512]{1,0:T(8,128)(2,1)S(1)} %pad_maximum_fusion.4), channel_id=1, source_target_pairs={{0,24},{4,28},{8,16},{12,20},{16,8},{20,12},{24,0},{28,4},{1,25},{... | collective-permute-start | bytes 307208 | tf_op jit(solution)/shard_map/ppermute | solution.py:444
  119.4 11.0 %collective-permute-start.30 = (bf16[100,512]{1,0:T(8,128)(2,1)S(1)}, bf16[100,512]{1,0:T(8,128)(2,1)S(1)}, u32[]{:S(2)}, u32[]{:S(2)}) collective-permute-start(bf16[100,512]{1,0:T(8,128)(2,1)S(1)} %pad_maximum_fusion.3), channel_id=1, source_target_pairs={{0,16},{4,20},{8,24},{12,28},{16,0},{20,4},{24,8},{28,12},{1,17},{... | collective-permute-start | bytes 307208 | tf_op jit(solution)/shard_map/ppermute | solution.py:444
  122.1 8.4 %collective-permute-start.29 = (bf16[100,512]{1,0:T(8,128)(2,1)S(1)}, bf16[100,512]{1,0:T(8,128)(2,1)S(1)}, u32[]{:S(2)}, u32[]{:S(2)}) collective-permute-start(bf16[100,512]{1,0:T(8,128)(2,1)S(1)} %pad_maximum_fusion.2), channel_id=1, source_target_pairs={{0,8},{4,12},{8,0},{12,4},{16,24},{20,28},{24,16},{28,20},{1,9},{5... | collective-permute-start | bytes 307208 | tf_op jit(solution)/shard_map/ppermute | solution.py:444

commit v2 on v1

--- a/solution.py
+++ b/solution.py
@@ -99,21 +99,39 @@
 
 
 def spread_out(block, ti, outs, direct):
+    def put(ref, at, pieces):
+        for piece in pieces:
+            ref[at : at + piece.shape[0], :] = piece.astype(jnp.bfloat16)
+            at += piece.shape[0]
+
     if direct:
         for s, out in enumerate(outs):
-            out[...] = block(ti ^ s).astype(jnp.bfloat16)
+            upper, lower = block(ti ^ s)
+            put(out, 0, upper + lower)
         return
     send_x, keep_x, send_y, keep_y = outs
     half = send_x.shape[0] // 2
-    for s, upper, lower in ((0, (keep_x, 0), (keep_y, 0)), (1, (send_x, 0), (keep_y, half)),
-                            (2, (keep_x, half), (send_y, 0)), (3, (send_x, half), (send_y, half))):
-        values = block(ti ^ s).astype(jnp.bfloat16)
-        for (ref, at), piece in ((upper, values[:half]), (lower, values[half:])):
-            ref[at : at + half, :] = piece
-
-
-def expert_kernel(*refs, pieces, halves, direct, staged):
+    places = (
+        (0, (keep_x, 0), (keep_y, 0)),
+        (1, (send_x, 0), (keep_y, half)),
+        (2, (keep_x, half), (send_y, 0)),
+        (3, (send_x, half), (send_y, half)),
+    )
+    for s, above, below in places:
+        upper, lower = block(ti ^ s)
+        put(*above, upper)
+        put(*below, lower)
+
+
+def halves_of(values):
+    half = values.shape[0] // 2
+    return values[:half], values[half:]
+
+
+def expert_kernel(*refs, pieces, halves, direct, staged, extra):
     ti = place()[2]
+    if extra:
+        added, refs = refs[0], refs[1:]
     xs, (gate_w, up_w, down_w) = refs[: pieces * halves], refs[pieces * halves :][:3]
     rest = refs[pieces * halves + 3 :]
     chunks = pieces
@@ -153,11 +171,20 @@
     hidden = (gate / (1.0 + jnp.exp(-gate)) * up).astype(jnp.bfloat16)
     if staged:
         copies[-1].wait()
+    if staged:
+        ys[0][...] = jnp.dot(hidden, downs[...], preferred_element_type=jnp.float32).astype(
+            jnp.bfloat16
+        )
+        return
     cols = ys[0].shape[1]
 
     def block(n):
         at = pl.ds(pl.multiple_of(n * cols, cols), cols)
-        return jnp.dot(hidden, downs[:, at], preferred_element_type=jnp.float32)
+        above, below = halves_of(jnp.dot(hidden, downs[:, at], preferred_element_type=jnp.float32))
+        if not extra:
+            return [above], [below]
+        more_above, more_below = halves_of(added[:, at])
+        return [above, more_above], [below, more_below]
 
     spread_out(block, ti, ys, direct)
 
@@ -166,26 +193,37 @@
     return [sds((rows, cols))] * (tp if direct else 4)
 
 
-def run_expert(xs, halves, gate_w, up_w, down_w, tp, direct):
+def run_expert(xs, halves, gate_w, up_w, down_w, tp, direct, extra=()):
     rows = xs[0].shape[0] * halves
     width, hidden = gate_w.shape
-    shapes = out_shapes(rows, down_w.shape[1] // tp, tp, direct)
     pieces = len(xs) // halves
     staged = pieces == 1
+    if staged:
+        shapes = [sds((rows, down_w.shape[1]))]
+    else:
+        total = rows + sum(x.shape[0] for x in extra)
+        shapes = out_shapes(total, down_w.shape[1] // tp, tp, direct)
     scratch = [pltpu.VMEM((2, rows, width // tp), jnp.bfloat16)]
     if staged:
         part = pltpu.VMEM((tp, width // tp, hidden), jnp.bfloat16)
         scratch += [part, part, pltpu.VMEM(down_w.shape, jnp.bfloat16), DMA((2 * tp + 1,))]
         gate_w, up_w, down_w = far(gate_w), far(up_w), far(down_w)
     return pl.pallas_call(
-        lambda *refs: expert_kernel(*refs, pieces=pieces, halves=halves, direct=direct, staged=staged),
+        lambda *refs: expert_kernel(
+            *refs,
+            pieces=pieces,
+            halves=halves,
+            direct=direct,
+            staged=staged,
+            extra=len(extra) > 0,
+        ),
         out_shape=shapes,
-        in_specs=[VM] * len(xs) + [FAR if staged else VM] * 3,
+        in_specs=[VM] * (len(extra) + len(xs)) + [FAR if staged else VM] * 3,
         out_specs=[VM] * len(shapes),
         scratch_shapes=scratch,
         cost_estimate=cost(6 * rows * width * hidden),
         compiler_params=limit(24),
-    )(*xs, gate_w, up_w, down_w)
+    )(*extra, *xs, gate_w, up_w, down_w)
 
 
 def combine_kernel(slots, weights, *refs, count):
@@ -194,10 +232,7 @@
     own = [column(slots[k : k + 1, :]) for k in range(TOP_K)]
     scale = [column(weights[k : k + 1, :]) for k in range(TOP_K)]
     group = back[0].shape[0]
-    total = None
-    for part in shared:
-        part = part[...].astype(jnp.float32)
-        total = part if total is None else total + part
+    total = jnp.concatenate([part[...] for part in shared], axis=0)
     picked = [None] * TOP_K
     for s in range(count):
         slot_col = lax.broadcasted_iota(jnp.int32, (tokens, group), 1) + s * group
@@ -329,7 +364,8 @@
 
     def block(n):
         at = pl.ds(pl.multiple_of(n * cols, cols), cols)
-        return jnp.dot(rows, weight[:, at], preferred_element_type=jnp.float32)
+        above, below = halves_of(jnp.dot(rows, weight[:, at], preferred_element_type=jnp.float32))
+        return [above], [below]
 
     spread_out(block, ti, outs, direct)
 
@@ -449,8 +485,12 @@
     def along_tp(x, s):
         return lax.ppermute(x, "tp", [(i, i ^ s) for i in range(tp)])
 
-    def exchange(parts, move):
-        return [parts[0]] + [move(parts[s], s) for s in range(1, len(parts))]
+    def exchange(parts, move, near_first=False):
+        moved = {}
+        turns = range(1, len(parts))
+        for s in turns if near_first else reversed(turns):
+            moved[s] = move(parts[s], s)
+        return [parts[0]] + [moved[s] for s in range(1, len(parts))]
 
     direct = tp != 4
 
@@ -527,13 +567,12 @@
             name="rope",
         compiler_params=limit(8),
         )(far(query_pairs), far(key_pairs), far(value_rows), cosine, sine)
-        packs = exchange(packs, along_z)
+        packs = exchange(packs, along_z, near_first=True)
         others = [swap(packs[0])]
-        others += [swap(p) for p in packs[1:]]
+        for s in range(1, chips):
+            others.append(swap(packs[s]))
 
     shared = run_expert([xn], 1, shared_gate, shared_up, shared_down, tp, True)
-    shared = exchange(shared, along_tp)
-
     own, other = pl.pallas_call(
         lambda *refs: pack_kernel(*refs, count=chips, cap=cap),
         out_shape=[sds((chips * cap, slice_width))] * 2,
@@ -545,8 +584,13 @@
     )(*arrived)
     other = swap(other)
     slices = gather_tp(own, other)
-    terms = run_expert(slices, 2, gate_weight[0], up_weight[0], down_weight[0], tp, direct)
-    summed = [x.astype(jnp.bfloat16) for x in reduce_tp(terms)]
+    terms = run_expert(
+        slices, 2, gate_weight[0], up_weight[0], down_weight[0], tp, direct, extra=shared
+    )
+    summed = reduce_tp(terms)
+    routed = chips * cap
+    shared = [x[routed:] for x in summed]
+    summed = [x[:routed].astype(jnp.bfloat16) for x in summed]
 
     if spread:
         heads_out = pl.pallas_call(
@@ -598,7 +642,7 @@
     moe_out = pl.pallas_call(
         lambda *refs: combine_kernel(*refs, count=chips),
         out_shape=sds((tokens, slice_width)),
-        in_specs=[VM] * (2 + chips + tp),
+        in_specs=[VM] * (2 + chips + len(shared)),
         out_specs=VM,
         cost_estimate=cost(4e8),
         name="combine",

time: 132 us -> 124 us (0.939)
  waiting for transfers between devices: 62.5 us -> 57.9 us
  starting transfers between devices: 43.5 us -> 39.8 us
    ppermute x17 -> x14, waiting for transfers between devices: 24.6 us -> 20.4 us  [along_tp(): return lax.ppermute(x, 'tp', [(i, i ^ s) for i in range(tp)])]
    ppermute x17 -> x14, starting transfers between devices: 19.6 us -> 16.6 us  [along_tp(): return lax.ppermute(x, 'tp', [(i, i ^ s) for i in range(tp)])]
  transfers between devices with their start and end apart: 35 -> 32, of which waited for: 15 -> 13; matrix products, arithmetic and copies ran while one was open for 1% -> 1% of each run, Pallas kernels for 15% -> 16%
where the time goes in v2:
time: 124 us
  waiting for transfers between devices  57.9 us (47%)
  starting transfers between devices  39.8 us (32%)
  Pallas kernels  22.5 us (18%)
  other arithmetic  2.31 us (2%)
    ppermute x12, waiting for transfers between devices, along_z(): lax.ppermute(x, 'ep', [(i, 2 * (i // 2 ^ s) + i % 2) for i in range(ep)])  37 us
    ppermute x12, starting transfers between devices, along_z(): lax.ppermute(x, 'ep', [(i, 2 * (i // 2 ^ s) + i % 2) for i in range(ep)])  21.9 us
    ppermute x14, waiting for transfers between devices, along_tp(): return lax.ppermute(x, 'tp', [(i, i ^ s) for i in range(tp)])  20.4 us
    ppermute x14, starting transfers between devices, along_tp(): return lax.ppermute(x, 'tp', [(i, i ^ s) for i in range(tp)])  16.6 us
    pallas_call x1, Pallas kernels, inner(): pl.pallas_call(lambda *refs: attend_kernel(*refs, count=chips, rows=rows,...  9.95 us
    pallas_call x2, Pallas kernels, run_expert(): pl.pallas_call(lambda *refs: expert_kernel(*refs, pieces=pieces, halves=h...  6.64 us
  transfers between devices with their start and end apart: 32, of which 13 were waited for; matrix products, arithmetic and copies ran while one was open for 1% of the time, Pallas kernels for 16%

profile of v2, /device:TPU:0, one launch (start us, length us, event | category | flops | bytes accessed | tf_op | source)
XLA Modules:
  0.0 123.5 jit_solution(8876361552301362777)
XLA Ops:
  0.7 0.8 fusion
  1.4 1.9 %rope.1 = (bf16[1152,128]{1,0:T(8,128)(2,1)S(1)}, bf16[1152,128]{1,0:T(8,128)(2,1)S(1)}, bf16[1152,128]{1,0:T(8,128)(2,1)S(1)}, bf16[1152,128]{1,0:T(8,128)(2,1)S(1)}) custom-call(bf16[384,512]{1,0:T(8,128)(2,1)} %refs_0_.2, bf16[384,512]{1,0:T(8,128)(2,1)} %refs_1_.2, bf16[384,512]{1,0:T(8,128)(2,1)} %refs_2_.2, f32[384,128]{1,0:T(8,128)S(1)} %get-tuple-element.61.refs_3_, ...), custom_call_target="tpu_custom_call" | custom-call | flops 400000000 | tf_op jit(solution)/shard_map/rope/pallas_call | solution.py:560
  3.4 3.1 %collective-permute-start = (bf16[1152,128]{1,0:T(8,128)(2,1)S(1)}, bf16[1152,128]{1,0:T(8,128)(2,1)S(1)}, u32[]{:S(2)}, u32[]{:S(2)}) collective-permute-start(bf16[1152,128]{1,0:T(8,128)(2,1)S(1)} %get-tuple-element.27), channel_id=1, source_target_pairs={{0,8},{4,12},{8,0},{12,4},{16,24},{20,28},{24,16},{28,20},{1,9},{5... | collective-permute-start | bytes 884744 | tf_op jit(solution)/shard_map/ppermute | solution.py:480
  6.5 2.6 %collective-permute-start.1 = (bf16[1152,128]{1,0:T(8,128)(2,1)S(1)}, bf16[1152,128]{1,0:T(8,128)(2,1)S(1)}, u32[]{:S(2)}, u32[]{:S(2)}) collective-permute-start(bf16[1152,128]{1,0:T(8,128)(2,1)S(1)} %get-tuple-element.28), channel_id=1, source_target_pairs={{0,16},{4,20},{8,24},{12,28},{16,0},{20,4},{24,8},{28,12},{1,17},{... | collective-permute-start | bytes 884744 | tf_op jit(solution)/shard_map/ppermute | solution.py:480
  9.1 0.0 collective-permute-start.2
  9.1 1.7 %dispatch.1 = (bf16[160,2048]{1,0:T(8,128)(2,1)S(1)}, s32[2,160]{1,0:T(2,128)S(1)}, bf16[100,512]{1,0:T(8,128)(2,1)S(1)}, bf16[100,512]{1,0:T(8,128)(2,1)S(1)}, ...) custom-call(bf16[160,2048]{1,0:T(8,128)(2,1)} %refs_0_.3, f32[1,2048]{1,0:T(1,128)} %bitcast.14, s32[2,160]{1,0:T(2,128)} %bitcast.15), custom_call_target="tpu_custom_call" | custom-call | flops 400000000 | tf_op jit(solution)/shard_map/dispatch/pallas_call | solution.py:529
  10.8 1.0 collective-permute-start.14
  11.8 3.5 %collective-permute-start.15 = (bf16[100,512]{1,0:T(8,128)(2,1)S(1)}, bf16[100,512]{1,0:T(8,128)(2,1)S(1)}, u32[]{:S(2)}, u32[]{:S(2)}) collective-permute-start(bf16[100,512]{1,0:T(8,128)(2,1)S(1)} %get-tuple-element.42), channel_id=1, source_target_pairs={{0,16},{4,20},{8,24},{12,28},{16,0},{20,4},{24,8},{28,12},{1,17},{... | collective-permute-start | bytes 307208 | tf_op jit(solution)/shard_map/ppermute | solution.py:480
  15.2 13.7 %collective-permute-done.14.refs_1_ = bf16[100,512]{1,0:T(8,128)(2,1)S(1)} collective-permute-done((bf16[100,512]{1,0:T(8,128)(2,1)S(1)}, bf16[100,512]{1,0:T(8,128)(2,1)S(1)}, u32[]{:S(2)}, u32[]{:S(2)}) %collective-permute-start.14) | collective-permute-done | bytes 102432 | tf_op jit(solution)/shard_map/ppermute | solution.py:480
  28.9 2.7 %collective-permute-start.16 = (bf16[100,512]{1,0:T(8,128)(2,1)S(1)}, bf16[100,512]{1,0:T(8,128)(2,1)S(1)}, u32[]{:S(2)}, u32[]{:S(2)}) collective-permute-start(bf16[100,512]{1,0:T(8,128)(2,1)S(1)} %get-tuple-element.43), channel_id=1, source_target_pairs={{0,24},{4,28},{8,16},{12,20},{16,8},{20,12},{24,0},{28,4},{1,25},{... | collective-permute-start | bytes 307208 | tf_op jit(solution)/shard_map/ppermute | solution.py:480
  31.6 11.3 %collective-permute-done.15.refs_2_ = bf16[100,512]{1,0:T(8,128)(2,1)S(1)} collective-permute-done((bf16[100,512]{1,0:T(8,128)(2,1)S(1)}, bf16[100,512]{1,0:T(8,128)(2,1)S(1)}, u32[]{:S(2)}, u32[]{:S(2)}) %collective-permute-start.15) | collective-permute-done | bytes 102432 | tf_op jit(solution)/shard_map/ppermute | solution.py:480
  42.9 0.5 collective-permute-start.4
  43.4 0.1 collective-permute-start.5
  43.4 0.4 collective-permute-start.6
  43.9 0.1 collective-permute-start.20
  44.1 0.4 collective-permute-done.3.refs_6_
  44.4 1.5 %collective-permute-start.17 = (bf16[200,512]{1,0:T(8,128)(2,1)S(1)}, bf16[200,512]{1,0:T(8,128)(2,1)S(1)}, u32[]{:S(2)}, u32[]{:S(2)}) collective-permute-start(bf16[200,512]{1,0:T(8,128)(2,1)S(1)} %get-tuple-element.44.refs_1_), channel_id=1, source_target_pairs={{0,1},{1,0},{2,3},{3,2},{4,5},{5,4},{6,7},{7,6},{8,9},{9,8},{10,11... | collective-permute-start | bytes 614408 | tf_op jit(solution)/shard_map/ppermute | solution.py:486
  45.9 0.1 collective-permute-done.20.refs_5_
  46.0 1.5 %collective-permute-start.22 = (bf16[200,512]{1,0:T(8,128)(2,1)S(1)}, bf16[200,512]{1,0:T(8,128)(2,1)S(1)}, u32[]{:S(2)}, u32[]{:S(2)}) collective-permute-start(bf16[200,512]{1,0:T(8,128)(2,1)S(1)} %collective-permute-done.20.refs_5_), channel_id=1, source_target_pairs={{0,2},{1,3},{2,0},{3,1},{4,6},{5,7},{6,4},{7,5},{8,10},{9,11},{10,... | collective-permute-start | bytes 614408 | tf_op jit(solution)/shard_map/ppermute | solution.py:486
  47.5 0.0 copy-start
  47.6 9.9 %attend.1 = (bf16[384,128]{1,0:T(8,128)(2,1)S(1)}, bf16[384,128]{1,0:T(8,128)(2,1)S(1)}, bf16[384,128]{1,0:T(8,128)(2,1)S(1)}, bf16[384,128]{1,0:T(8,128)(2,1)S(1)}) custom-call(f32[1,4]{1,0:T(1,128)S(1)} %bitcast.12, f32[1,128]{1,0:T(1,128)S(1)} %bitcast.13, bf16[1152,128]{1,0:T(8,128)(2,1)S(1)} %get-tuple-element.26.refs_2_, ...), custom_call_target="tpu_custom_call" | custom-call | flops 4000000000 | tf_op jit(solution)/shard_map/attend/pallas_call | solution.py:596
  57.5 0.3 collective-permute-start.7
  57.8 2.8 %collective-permute-start.8 = (bf16[384,128]{1,0:T(8,128)(2,1)S(1)}, bf16[384,128]{1,0:T(8,128)(2,1)S(1)}, u32[]{:S(2)}, u32[]{:S(2)}) collective-permute-start(bf16[384,128]{1,0:T(8,128)(2,1)S(1)} %get-tuple-element.32), channel_id=1, source_target_pairs={{0,16},{4,20},{8,24},{12,28},{16,0},{20,4},{24,8},{28,12},{1,17},{... | collective-permute-start | bytes 294920 | tf_op jit(solution)/shard_map/ppermute | solution.py:480
  60.6 1.3 %collective-permute-start.9 = (bf16[384,128]{1,0:T(8,128)(2,1)S(1)}, bf16[384,128]{1,0:T(8,128)(2,1)S(1)}, u32[]{:S(2)}, u32[]{:S(2)}) collective-permute-start(bf16[384,128]{1,0:T(8,128)(2,1)S(1)} %get-tuple-element.33), channel_id=1, source_target_pairs={{0,24},{4,28},{8,16},{12,20},{16,8},{20,12},{24,0},{28,4},{1,25},{... | collective-permute-start | bytes 294920 | tf_op jit(solution)/shard_map/ppermute | solution.py:480
  62.0 0.5 collective-permute-start.18
  62.5 1.5 %collective-permute-start.21 = (bf16[200,512]{1,0:T(8,128)(2,1)S(1)}, bf16[200,512]{1,0:T(8,128)(2,1)S(1)}, u32[]{:S(2)}, u32[]{:S(2)}) collective-permute-start(bf16[200,512]{1,0:T(8,128)(2,1)S(1)} %collective-permute-done.20.refs_5_), channel_id=1, source_target_pairs={{0,1},{1,0},{2,3},{3,2},{4,5},{5,4},{6,7},{7,6},{8,9},{9,8},{10,11... | collective-permute-start | bytes 614408 | tf_op jit(solution)/shard_map/ppermute | solution.py:486
  64.0 1.5 %collective-permute-start.19 = (bf16[200,512]{1,0:T(8,128)(2,1)S(1)}, bf16[200,512]{1,0:T(8,128)(2,1)S(1)}, u32[]{:S(2)}, u32[]{:S(2)}) collective-permute-start(bf16[200,512]{1,0:T(8,128)(2,1)S(1)} %collective-permute-done.17.refs_2_), channel_id=1, source_target_pairs={{0,2},{1,3},{2,0},{3,1},{4,6},{5,7},{6,4},{7,5},{8,10},{9,11},{10,... | collective-permute-start | bytes 614408 | tf_op jit(solution)/shard_map/ppermute | solution.py:486
  65.5 3.0 %collective-permute-done.8.refs_2_ = bf16[384,128]{1,0:T(8,128)(2,1)S(1)} collective-permute-done((bf16[384,128]{1,0:T(8,128)(2,1)S(1)}, bf16[384,128]{1,0:T(8,128)(2,1)S(1)}, u32[]{:S(2)}, u32[]{:S(2)}) %collective-permute-start.8) | collective-permute-done | bytes 98336 | tf_op jit(solution)/shard_map/ppermute | solution.py:480
  68.5 1.4 %collective-permute-start.23 = (bf16[200,512]{1,0:T(8,128)(2,1)S(1)}, bf16[200,512]{1,0:T(8,128)(2,1)S(1)}, u32[]{:S(2)}, u32[]{:S(2)}) collective-permute-start(bf16[200,512]{1,0:T(8,128)(2,1)S(1)} %collective-permute-done.22.refs_7_), channel_id=1, source_target_pairs={{0,1},{1,0},{2,3},{3,2},{4,5},{5,4},{6,7},{7,6},{8,9},{9,8},{10,11... | collective-permute-start | bytes 614408 | tf_op jit(solution)/shard_map/ppermute | solution.py:486
  69.9 1.0 project.1
  70.9 0.7 collective-permute-start.10
  71.7 3.6 %shard_map.167.refs_0_ = bf16[160,2048]{1,0:T(8,128)(2,1)S(1)} custom-call(bf16[160,2048]{1,0:T(8,128)(2,1)S(1)} %get-tuple-element.39.refs_0_, bf16[2048,512]{1,0:T(8,128)(2,1)} %refs_1_.3, bf16[2048,512]{1,0:T(8,128)(2,1)} %refs_2_.3, bf16[512,2048]{1,0:T(8,128)(2,1)} %refs_3_.1), custom_call_target="tpu_custom_call" | custom-call | flops 1006632960 | tf_op jit(solution)/shard_map/pallas_call | solution.py:211
  75.3 0.6 collective-permute-start.12
  75.9 0.6 collective-permute-done.23.refs_8_
  76.5 3.0 %shard_map.168 = (bf16[560,512]{1,0:T(8,128)(2,1)S(1)}, bf16[560,512]{1,0:T(8,128)(2,1)S(1)}, bf16[560,512]{1,0:T(8,128)(2,1)S(1)}, bf16[560,512]{1,0:T(8,128)(2,1)S(1)}) custom-call(bf16[160,2048]{1,0:T(8,128)(2,1)S(1)} %shard_map.167.refs_0_, bf16[200,512]{1,0:T(8,128)(2,1)S(1)} %get-tuple-element.44.refs_1_, ...), custom_call_target="tpu_custom_call" | custom-call | flops 2516582400 | tf_op jit(solution)/shard_map/pallas_call | solution.py:211
  79.5 1.4 %collective-permute-start.24 = (bf16[560,512]{1,0:T(8,128)(2,1)S(1)}, bf16[560,512]{1,0:T(8,128)(2,1)S(1)}, u32[]{:S(2)}, u32[]{:S(2)}) collective-permute-start(bf16[560,512]{1,0:T(8,128)(2,1)S(1)} %get-tuple-element.47), channel_id=1, source_target_pairs={{0,1},{1,0},{2,3},{3,2},{4,5},{5,4},{6,7},{7,6},{8,9},{9,8},{10,11... | collective-permute-start | bytes 1720328 | tf_op jit(solution)/shard_map/ppermute | solution.py:486
  81.0 0.9 collective-permute-start.26
  81.9 1.2 collective-permute-done.10
  83.1 0.1 add_convert_fusion.5
  83.1 2.3 %collective-permute-start.11 = (bf16[192,512]{1,0:T(8,128)(2,1)S(1)}, bf16[192,512]{1,0:T(8,128)(2,1)S(1)}, u32[]{:S(2)}, u32[]{:S(2)}) collective-permute-start(bf16[192,512]{1,0:T(8,128)(2,1)S(1)} %add_convert_fusion.5), channel_id=1, source_target_pairs={{0,2},{1,3},{2,0},{3,1},{4,6},{5,7},{6,4},{7,5},{8,10},{9,11},{10,... | collective-permute-start | bytes 589832 | tf_op jit(solution)/shard_map/ppermute | solution.py:486
  85.4 1.8 %collective-permute-done.12 = bf16[384,512]{1,0:T(8,128)(2,1)S(1)} collective-permute-done((bf16[384,512]{1,0:T(8,128)(2,1)S(1)}, bf16[384,512]{1,0:T(8,128)(2,1)S(1)}, u32[]{:S(2)}, u32[]{:S(2)}) %collective-permute-start.12) | collective-permute-done | bytes 393248 | tf_op jit(solution)/shard_map/ppermute | solution.py:486
  87.3 0.1 add_convert_fusion.3
  87.3 1.0 collective-permute-start.13
  88.3 11.5 %collective-permute-done.11 = bf16[192,512]{1,0:T(8,128)(2,1)S(1)} collective-permute-done((bf16[192,512]{1,0:T(8,128)(2,1)S(1)}, bf16[192,512]{1,0:T(8,128)(2,1)S(1)}, u32[]{:S(2)}, u32[]{:S(2)}) %collective-permute-start.11) | collective-permute-done | bytes 196640 | tf_op jit(solution)/shard_map/ppermute | solution.py:486
  99.8 0.1 add_convert_fusion.4
  99.9 0.1 add_convert_fusion.2
  100.0 0.1 add_convert_fusion
  100.1 1.4 %collective-permute-start.27 = (bf16[280,512]{1,0:T(8,128)(2,1)S(1)}, bf16[280,512]{1,0:T(8,128)(2,1)S(1)}, u32[]{:S(2)}, u32[]{:S(2)}) collective-permute-start(bf16[280,512]{1,0:T(8,128)(2,1)S(1)} %add_convert_fusion), channel_id=1, source_target_pairs={{0,1},{1,0},{2,3},{3,2},{4,5},{5,4},{6,7},{7,6},{8,9},{9,8},{10,11... | collective-permute-start | bytes 860168 | tf_op jit(solution)/shard_map/ppermute | solution.py:486
  101.5 0.1 add_convert_fusion.1
  101.6 0.4 collective-permute-start.25
  102.0 0.8 pad_maximum_fusion
  102.8 4.0 %collective-permute-done.27 = bf16[280,512]{1,0:T(8,128)(2,1)S(1)} collective-permute-done((bf16[280,512]{1,0:T(8,128)(2,1)S(1)}, bf16[280,512]{1,0:T(8,128)(2,1)S(1)}, u32[]{:S(2)}, u32[]{:S(2)}) %collective-permute-start.27) | collective-permute-done | bytes 286752 | tf_op jit(solution)/shard_map/ppermute | solution.py:486
  106.8 0.1 convert_add_fusion
  106.9 0.0 copy-start.4
  107.0 0.1 collective-permute-start.28
  107.1 1.2 collective-permute-done.25
  108.3 0.1 fusion.6
  108.5 0.0 collective-permute-done.28
  108.6 2.2 %collective-permute-start.31 = (bf16[100,512]{1,0:T(8,128)(2,1)S(1)}, bf16[100,512]{1,0:T(8,128)(2,1)S(1)}, u32[]{:S(2)}, u32[]{:S(2)}) collective-permute-start(bf16[100,512]{1,0:T(8,128)(2,1)S(1)} %pad_maximum_fusion.4), channel_id=1, source_target_pairs={{0,24},{4,28},{8,16},{12,20},{16,8},{20,12},{24,0},{28,4},{1,25},{... | collective-permute-start | bytes 307208 | tf_op jit(solution)/shard_map/ppermute | solution.py:480
  110.8 2.4 %collective-permute-start.30 = (bf16[100,512]{1,0:T(8,128)(2,1)S(1)}, bf16[100,512]{1,0:T(8,128)(2,1)S(1)}, u32[]{:S(2)}, u32[]{:S(2)}) collective-permute-start(bf16[100,512]{1,0:T(8,128)(2,1)S(1)} %pad_maximum_fusion.3), channel_id=1, source_target_pairs={{0,16},{4,20},{8,24},{12,28},{16,0},{20,4},{24,8},{28,12},{1,17},{... | collective-permute-start | bytes 307208 | tf_op jit(solution)/shard_map/ppermute | solution.py:480
  113.2 0.1 collective-permute-start.29
  113.3 2.2 %collective-permute-done.31.refs_5_ = bf16[100,512]{1,0:T(8,128)(2,1)S(1)} collective-permute-done((bf16[100,512]{1,0:T(8,128)(2,1)S(1)}, bf16[100,512]{1,0:T(8,128)(2,1)S(1)}, u32[]{:S(2)}, u32[]{:S(2)}) %collective-permute-start.31) | collective-permute-done | bytes 102432 | tf_op jit(solution)/shard_map/ppermute | solution.py:480
  115.6 6.7 %collective-permute-done.30.refs_4_ = bf16[100,512]{1,0:T(8,128)(2,1)S(1)} collective-permute-done((bf16[100,512]{1,0:T(8,128)(2,1)S(1)}, bf16[100,512]{1,0:T(8,128)(2,1)S(1)}, u32[]{:S(2)}, u32[]{:S(2)}) %collective-permute-start.30) | collective-permute-done | bytes 102432 | tf_op jit(solution)/shard_map/ppermute | solution.py:480
  122.3 1.2 combine.1
  (43 shorter events, 0.4 us)
Async XLA Ops:
  0.6 46.9 %copy-start.5 = (f32[4]{0:T(128)S(1)}, f32[4]{0:T(128)}, u32[]{:S(2)}) copy-start(f32[4]{0:T(128)} %param.19) | copy-start | bytes 52
  0.6 46.9 %copy-start.6 = (f32[128]{0:T(128)S(1)}, f32[128]{0:T(128)}, u32[]{:S(2)}) copy-start(f32[128]{0:T(128)} %param.20) | copy-start | bytes 1540
  3.4 39.5 %collective-permute-start = (bf16[1152,128]{1,0:T(8,128)(2,1)S(1)}, bf16[1152,128]{1,0:T(8,128)(2,1)S(1)}, u32[]{:S(2)}, u32[]{:S(2)}) collective-permute-start(bf16[1152,128]{1,0:T(8,128)(2,1)S(1)} %get-tuple-element.27), channel_id=1, source_target_pairs={{0,8},{4,12},{8,0},{12,4},{16,24},{20,28},{24,16},{28,20},{1,9},{5... | collective-permute-start | bytes 884744 | tf_op jit(solution)/shard_map/ppermute | solution.py:480
  6.5 36.9 %collective-permute-start.1 = (bf16[1152,128]{1,0:T(8,128)(2,1)S(1)}, bf16[1152,128]{1,0:T(8,128)(2,1)S(1)}, u32[]{:S(2)}, u32[]{:S(2)}) collective-permute-start(bf16[1152,128]{1,0:T(8,128)(2,1)S(1)} %get-tuple-element.28), channel_id=1, source_target_pairs={{0,16},{4,20},{8,24},{12,28},{16,0},{20,4},{24,8},{28,12},{1,17},{... | collective-permute-start | bytes 884744 | tf_op jit(solution)/shard_map/ppermute | solution.py:480
  9.1 34.4 %collective-permute-start.2 = (bf16[1152,128]{1,0:T(8,128)(2,1)S(1)}, bf16[1152,128]{1,0:T(8,128)(2,1)S(1)}, u32[]{:S(2)}, u32[]{:S(2)}) collective-permute-start(bf16[1152,128]{1,0:T(8,128)(2,1)S(1)} %get-tuple-element.29), channel_id=1, source_target_pairs={{0,24},{4,28},{8,16},{12,20},{16,8},{20,12},{24,0},{28,4},{1,25},{... | collective-permute-start | bytes 884744 | tf_op jit(solution)/shard_map/ppermute | solution.py:480
  10.8 18.1 %collective-permute-start.14 = (bf16[100,512]{1,0:T(8,128)(2,1)S(1)}, bf16[100,512]{1,0:T(8,128)(2,1)S(1)}, u32[]{:S(2)}, u32[]{:S(2)}) collective-permute-start(bf16[100,512]{1,0:T(8,128)(2,1)S(1)} %get-tuple-element.41), channel_id=1, source_target_pairs={{0,8},{4,12},{8,0},{12,4},{16,24},{20,28},{24,16},{28,20},{1,9},{5... | collective-permute-start | bytes 307208 | tf_op jit(solution)/shard_map/ppermute | solution.py:480
  11.8 31.1 %collective-permute-start.15 = (bf16[100,512]{1,0:T(8,128)(2,1)S(1)}, bf16[100,512]{1,0:T(8,128)(2,1)S(1)}, u32[]{:S(2)}, u32[]{:S(2)}) collective-permute-start(bf16[100,512]{1,0:T(8,128)(2,1)S(1)} %get-tuple-element.42), channel_id=1, source_target_pairs={{0,16},{4,20},{8,24},{12,28},{16,0},{20,4},{24,8},{28,12},{1,17},{... | collective-permute-start | bytes 307208 | tf_op jit(solution)/shard_map/ppermute | solution.py:480
  28.9 15.0 %collective-permute-start.16 = (bf16[100,512]{1,0:T(8,128)(2,1)S(1)}, bf16[100,512]{1,0:T(8,128)(2,1)S(1)}, u32[]{:S(2)}, u32[]{:S(2)}) collective-permute-start(bf16[100,512]{1,0:T(8,128)(2,1)S(1)} %get-tuple-element.43), channel_id=1, source_target_pairs={{0,24},{4,28},{8,16},{12,20},{16,8},{20,12},{24,0},{28,4},{1,25},{... | collective-permute-start | bytes 307208 | tf_op jit(solution)/shard_map/ppermute | solution.py:480
  42.9 1.6 %collective-permute-start.3 = (bf16[1152,128]{1,0:T(8,128)(2,1)S(1)}, bf16[1152,128]{1,0:T(8,128)(2,1)S(1)}, u32[]{:S(2)}, u32[]{:S(2)}) collective-permute-start(bf16[1152,128]{1,0:T(8,128)(2,1)S(1)} %get-tuple-element.26.refs_2_), channel_id=1, source_target_pairs={{0,4},{4,0},{8,12},{12,8},{16,20},{20,16},{24,28},{28,24},{1,5},{5... | collective-permute-start | bytes 884744 | tf_op jit(solution)/shard_map/ppermute | solution.py:483
  42.9 4.7 %collective-permute-start.4 = (bf16[1152,128]{1,0:T(8,128)(2,1)S(1)}, bf16[1152,128]{1,0:T(8,128)(2,1)S(1)}, u32[]{:S(2)}, u32[]{:S(2)}) collective-permute-start(bf16[1152,128]{1,0:T(8,128)(2,1)S(1)} %collective-permute-done.refs_3_), channel_id=1, source_target_pairs={{0,4},{4,0},{8,12},{12,8},{16,20},{20,16},{24,28},{28,24},{1,5},{5... | collective-permute-start | bytes 884744 | tf_op jit(solution)/shard_map/ppermute | solution.py:483
  43.4 4.1 %collective-permute-start.5 = (bf16[1152,128]{1,0:T(8,128)(2,1)S(1)}, bf16[1152,128]{1,0:T(8,128)(2,1)S(1)}, u32[]{:S(2)}, u32[]{:S(2)}) collective-permute-start(bf16[1152,128]{1,0:T(8,128)(2,1)S(1)} %collective-permute-done.1.refs_4_), channel_id=1, source_target_pairs={{0,4},{4,0},{8,12},{12,8},{16,20},{20,16},{24,28},{28,24},{1,5},{5... | collective-permute-start | bytes 884744 | tf_op jit(solution)/shard_map/ppermute | solution.py:483
  43.4 4.1 %collective-permute-start.6 = (bf16[1152,128]{1,0:T(8,128)(2,1)S(1)}, bf16[1152,128]{1,0:T(8,128)(2,1)S(1)}, u32[]{:S(2)}, u32[]{:S(2)}) collective-permute-start(bf16[1152,128]{1,0:T(8,128)(2,1)S(1)} %collective-permute-done.2.refs_5_), channel_id=1, source_target_pairs={{0,4},{4,0},{8,12},{12,8},{16,20},{20,16},{24,28},{28,24},{1,5},{5... | collective-permute-start | bytes 884744 | tf_op jit(solution)/shard_map/ppermute | solution.py:483
  43.9 2.1 %collective-permute-start.20 = (bf16[200,512]{1,0:T(8,128)(2,1)S(1)}, bf16[200,512]{1,0:T(8,128)(2,1)S(1)}, u32[]{:S(2)}, u32[]{:S(2)}) collective-permute-start(bf16[200,512]{1,0:T(8,128)(2,1)S(1)} %get-tuple-element.45), channel_id=1, source_target_pairs={{0,4},{4,0},{8,12},{12,8},{16,20},{20,16},{24,28},{28,24},{1,5},{5... | collective-permute-start | bytes 614408 | tf_op jit(solution)/shard_map/ppermute | solution.py:483
  44.4 17.5 %collective-permute-start.17 = (bf16[200,512]{1,0:T(8,128)(2,1)S(1)}, bf16[200,512]{1,0:T(8,128)(2,1)S(1)}, u32[]{:S(2)}, u32[]{:S(2)}) collective-permute-start(bf16[200,512]{1,0:T(8,128)(2,1)S(1)} %get-tuple-element.44.refs_1_), channel_id=1, source_target_pairs={{0,1},{1,0},{2,3},{3,2},{4,5},{5,4},{6,7},{7,6},{8,9},{9,8},{10,11... | collective-permute-start | bytes 614408 | tf_op jit(solution)/shard_map/ppermute | solution.py:486
  46.0 16.5 %collective-permute-start.22 = (bf16[200,512]{1,0:T(8,128)(2,1)S(1)}, bf16[200,512]{1,0:T(8,128)(2,1)S(1)}, u32[]{:S(2)}, u32[]{:S(2)}) collective-permute-start(bf16[200,512]{1,0:T(8,128)(2,1)S(1)} %collective-permute-done.20.refs_5_), channel_id=1, source_target_pairs={{0,2},{1,3},{2,0},{3,1},{4,6},{5,7},{6,4},{7,5},{8,10},{9,11},{10,... | collective-permute-start | bytes 614408 | tf_op jit(solution)/shard_map/ppermute | solution.py:486
  47.5 22.3 %copy-start = (bf16[512,2048]{1,0:T(8,128)(2,1)S(1)}, bf16[512,2048]{1,0:T(8,128)(2,1)}, u32[]{:S(2)}) copy-start(bf16[512,2048]{1,0:T(8,128)(2,1)} %refs_4_.1) | copy-start | bytes 6291460
  57.5 6.5 %collective-permute-start.7 = (bf16[384,128]{1,0:T(8,128)(2,1)S(1)}, bf16[384,128]{1,0:T(8,128)(2,1)S(1)}, u32[]{:S(2)}, u32[]{:S(2)}) collective-permute-start(bf16[384,128]{1,0:T(8,128)(2,1)S(1)} %get-tuple-element.31), channel_id=1, source_target_pairs={{0,8},{4,12},{8,0},{12,4},{16,24},{20,28},{24,16},{28,20},{1,9},{5... | collective-permute-start | bytes 294920 | tf_op jit(solution)/shard_map/ppermute | solution.py:480
  57.8 10.7 %collective-permute-start.8 = (bf16[384,128]{1,0:T(8,128)(2,1)S(1)}, bf16[384,128]{1,0:T(8,128)(2,1)S(1)}, u32[]{:S(2)}, u32[]{:S(2)}) collective-permute-start(bf16[384,128]{1,0:T(8,128)(2,1)S(1)} %get-tuple-element.32), channel_id=1, source_target_pairs={{0,16},{4,20},{8,24},{12,28},{16,0},{20,4},{24,8},{28,12},{1,17},{... | collective-permute-start | bytes 294920 | tf_op jit(solution)/shard_map/ppermute | solution.py:480
  60.6 9.3 %collective-permute-start.9 = (bf16[384,128]{1,0:T(8,128)(2,1)S(1)}, bf16[384,128]{1,0:T(8,128)(2,1)S(1)}, u32[]{:S(2)}, u32[]{:S(2)}) collective-permute-start(bf16[384,128]{1,0:T(8,128)(2,1)S(1)} %get-tuple-element.33), channel_id=1, source_target_pairs={{0,24},{4,28},{8,16},{12,20},{16,8},{20,12},{24,0},{28,4},{1,25},{... | collective-permute-start | bytes 294920 | tf_op jit(solution)/shard_map/ppermute | solution.py:480
  62.0 13.3 %collective-permute-start.18 = (bf16[200,512]{1,0:T(8,128)(2,1)S(1)}, bf16[200,512]{1,0:T(8,128)(2,1)S(1)}, u32[]{:S(2)}, u32[]{:S(2)}) collective-permute-start(bf16[200,512]{1,0:T(8,128)(2,1)S(1)} %get-tuple-element.44.refs_1_), channel_id=1, source_target_pairs={{0,2},{1,3},{2,0},{3,1},{4,6},{5,7},{6,4},{7,5},{8,10},{9,11},{10,... | collective-permute-start | bytes 614408 | tf_op jit(solution)/shard_map/ppermute | solution.py:486
  62.5 13.4 %collective-permute-start.21 = (bf16[200,512]{1,0:T(8,128)(2,1)S(1)}, bf16[200,512]{1,0:T(8,128)(2,1)S(1)}, u32[]{:S(2)}, u32[]{:S(2)}) collective-permute-start(bf16[200,512]{1,0:T(8,128)(2,1)S(1)} %collective-permute-done.20.refs_5_), channel_id=1, source_target_pairs={{0,1},{1,0},{2,3},{3,2},{4,5},{5,4},{6,7},{7,6},{8,9},{9,8},{10,11... | collective-permute-start | bytes 614408 | tf_op jit(solution)/shard_map/ppermute | solution.py:486
  64.0 11.9 %collective-permute-start.19 = (bf16[200,512]{1,0:T(8,128)(2,1)S(1)}, bf16[200,512]{1,0:T(8,128)(2,1)S(1)}, u32[]{:S(2)}, u32[]{:S(2)}) collective-permute-start(bf16[200,512]{1,0:T(8,128)(2,1)S(1)} %collective-permute-done.17.refs_2_), channel_id=1, source_target_pairs={{0,2},{1,3},{2,0},{3,1},{4,6},{5,7},{6,4},{7,5},{8,10},{9,11},{10,... | collective-permute-start | bytes 614408 | tf_op jit(solution)/shard_map/ppermute | solution.py:486
  68.5 7.9 %collective-permute-start.23 = (bf16[200,512]{1,0:T(8,128)(2,1)S(1)}, bf16[200,512]{1,0:T(8,128)(2,1)S(1)}, u32[]{:S(2)}, u32[]{:S(2)}) collective-permute-start(bf16[200,512]{1,0:T(8,128)(2,1)S(1)} %collective-permute-done.22.refs_7_), channel_id=1, source_target_pairs={{0,1},{1,0},{2,3},{3,2},{4,5},{5,4},{6,7},{7,6},{8,9},{9,8},{10,11... | collective-permute-start | bytes 614408 | tf_op jit(solution)/shard_map/ppermute | solution.py:486
  70.9 12.2 %collective-permute-start.10 = (bf16[384,512]{1,0:T(8,128)(2,1)S(1)}, bf16[384,512]{1,0:T(8,128)(2,1)S(1)}, u32[]{:S(2)}, u32[]{:S(2)}) collective-permute-start(bf16[384,512]{1,0:T(8,128)(2,1)S(1)} %get-tuple-element.35), channel_id=1, source_target_pairs={{0,1},{1,0},{2,3},{3,2},{4,5},{5,4},{6,7},{7,6},{8,9},{9,8},{10,11... | collective-permute-start | bytes 1179656 | tf_op jit(solution)/shard_map/ppermute | solution.py:486
  71.7 4.8 %copy-start.1 = (bf16[1,2048,512]{2,1,0:T(8,128)(2,1)S(1)}, bf16[1,2048,512]{2,1,0:T(8,128)(2,1)}, u32[]{:S(2)}) copy-start(bf16[1,2048,512]{2,1,0:T(8,128)(2,1)} %param.26) | copy-start | bytes 6291460
  71.7 4.8 %copy-start.2 = (bf16[1,2048,512]{2,1,0:T(8,128)(2,1)S(1)}, bf16[1,2048,512]{2,1,0:T(8,128)(2,1)}, u32[]{:S(2)}) copy-start(bf16[1,2048,512]{2,1,0:T(8,128)(2,1)} %param.27) | copy-start | bytes 6291460
  71.7 4.8 %copy-start.3 = (bf16[1,512,2048]{2,1,0:T(8,128)(2,1)S(1)}, bf16[1,512,2048]{2,1,0:T(8,128)(2,1)}, u32[]{:S(2)}) copy-start(bf16[1,512,2048]{2,1,0:T(8,128)(2,1)} %param.28) | copy-start | bytes 6291460
  75.3 12.0 %collective-permute-start.12 = (bf16[384,512]{1,0:T(8,128)(2,1)S(1)}, bf16[384,512]{1,0:T(8,128)(2,1)S(1)}, u32[]{:S(2)}, u32[]{:S(2)}) collective-permute-start(bf16[384,512]{1,0:T(8,128)(2,1)S(1)} %get-tuple-element.37), channel_id=1, source_target_pairs={{0,2},{1,3},{2,0},{3,1},{4,6},{5,7},{6,4},{7,5},{8,10},{9,11},{10,... | collective-permute-start | bytes 1179656 | tf_op jit(solution)/shard_map/ppermute | solution.py:486
  79.5 21.9 %collective-permute-start.24 = (bf16[560,512]{1,0:T(8,128)(2,1)S(1)}, bf16[560,512]{1,0:T(8,128)(2,1)S(1)}, u32[]{:S(2)}, u32[]{:S(2)}) collective-permute-start(bf16[560,512]{1,0:T(8,128)(2,1)S(1)} %get-tuple-element.47), channel_id=1, source_target_pairs={{0,1},{1,0},{2,3},{3,2},{4,5},{5,4},{6,7},{7,6},{8,9},{9,8},{10,11... | collective-permute-start | bytes 1720328 | tf_op jit(solution)/shard_map/ppermute | solution.py:486
  81.0 19.0 %collective-permute-start.26 = (bf16[560,512]{1,0:T(8,128)(2,1)S(1)}, bf16[560,512]{1,0:T(8,128)(2,1)S(1)}, u32[]{:S(2)}, u32[]{:S(2)}) collective-permute-start(bf16[560,512]{1,0:T(8,128)(2,1)S(1)} %get-tuple-element.49), channel_id=1, source_target_pairs={{0,2},{1,3},{2,0},{3,1},{4,6},{5,7},{6,4},{7,5},{8,10},{9,11},{10,... | collective-permute-start | bytes 1720328 | tf_op jit(solution)/shard_map/ppermute | solution.py:486
  83.1 16.7 %collective-permute-start.11 = (bf16[192,512]{1,0:T(8,128)(2,1)S(1)}, bf16[192,512]{1,0:T(8,128)(2,1)S(1)}, u32[]{:S(2)}, u32[]{:S(2)}) collective-permute-start(bf16[192,512]{1,0:T(8,128)(2,1)S(1)} %add_convert_fusion.5), channel_id=1, source_target_pairs={{0,2},{1,3},{2,0},{3,1},{4,6},{5,7},{6,4},{7,5},{8,10},{9,11},{10,... | collective-permute-start | bytes 589832 | tf_op jit(solution)/shard_map/ppermute | solution.py:486
  87.3 12.6 %collective-permute-start.13 = (bf16[192,512]{1,0:T(8,128)(2,1)S(1)}, bf16[192,512]{1,0:T(8,128)(2,1)S(1)}, u32[]{:S(2)}, u32[]{:S(2)}) collective-permute-start(bf16[192,512]{1,0:T(8,128)(2,1)S(1)} %add_convert_fusion.3), channel_id=1, source_target_pairs={{0,1},{1,0},{2,3},{3,2},{4,5},{5,4},{6,7},{7,6},{8,9},{9,8},{10,11... | collective-permute-start | bytes 589832 | tf_op jit(solution)/shard_map/ppermute | solution.py:486
  100.1 6.7 %collective-permute-start.27 = (bf16[280,512]{1,0:T(8,128)(2,1)S(1)}, bf16[280,512]{1,0:T(8,128)(2,1)S(1)}, u32[]{:S(2)}, u32[]{:S(2)}) collective-permute-start(bf16[280,512]{1,0:T(8,128)(2,1)S(1)} %add_convert_fusion), channel_id=1, source_target_pairs={{0,1},{1,0},{2,3},{3,2},{4,5},{5,4},{6,7},{7,6},{8,9},{9,8},{10,11... | collective-permute-start | bytes 860168 | tf_op jit(solution)/shard_map/ppermute | solution.py:486
  101.6 6.7 %collective-permute-start.25 = (bf16[280,512]{1,0:T(8,128)(2,1)S(1)}, bf16[280,512]{1,0:T(8,128)(2,1)S(1)}, u32[]{:S(2)}, u32[]{:S(2)}) collective-permute-start(bf16[280,512]{1,0:T(8,128)(2,1)S(1)} %add_convert_fusion.1), channel_id=1, source_target_pairs={{0,2},{1,3},{2,0},{3,1},{4,6},{5,7},{6,4},{7,5},{8,10},{9,11},{10,... | collective-permute-start | bytes 860168 | tf_op jit(solution)/shard_map/ppermute | solution.py:486
  106.9 15.4 %copy-start.4 = (f32[160,2]{0,1:T(2,128)S(1)}, f32[160,2]{0,1:T(2,128)}, u32[]{:S(2)}) copy-start(f32[160,2]{0,1:T(2,128)} %param.25) | copy-start | bytes 3844
  107.0 1.5 %collective-permute-start.28 = (bf16[200,512]{1,0:T(8,128)(2,1)S(1)}, bf16[200,512]{1,0:T(8,128)(2,1)S(1)}, u32[]{:S(2)}, u32[]{:S(2)}) collective-permute-start(bf16[200,512]{1,0:T(8,128)(2,1)S(1)} %slice.151), channel_id=1, source_target_pairs={{0,4},{4,0},{8,12},{12,8},{16,20},{20,16},{24,28},{28,24},{1,5},{5... | collective-permute-start | bytes 614408 | tf_op jit(solution)/shard_map/ppermute | solution.py:483
  108.6 7.0 %collective-permute-start.31 = (bf16[100,512]{1,0:T(8,128)(2,1)S(1)}, bf16[100,512]{1,0:T(8,128)(2,1)S(1)}, u32[]{:S(2)}, u32[]{:S(2)}) collective-permute-start(bf16[100,512]{1,0:T(8,128)(2,1)S(1)} %pad_maximum_fusion.4), channel_id=1, source_target_pairs={{0,24},{4,28},{8,16},{12,20},{16,8},{20,12},{24,0},{28,4},{1,25},{... | collective-permute-start | bytes 307208 | tf_op jit(solution)/shard_map/ppermute | solution.py:480
  110.8 11.5 %collective-permute-start.30 = (bf16[100,512]{1,0:T(8,128)(2,1)S(1)}, bf16[100,512]{1,0:T(8,128)(2,1)S(1)}, u32[]{:S(2)}, u32[]{:S(2)}) collective-permute-start(bf16[100,512]{1,0:T(8,128)(2,1)S(1)} %pad_maximum_fusion.3), channel_id=1, source_target_pairs={{0,16},{4,20},{8,24},{12,28},{16,0},{20,4},{24,8},{28,12},{1,17},{... | collective-permute-start | bytes 307208 | tf_op jit(solution)/shard_map/ppermute | solution.py:480
  113.2 9.1 %collective-permute-start.29 = (bf16[100,512]{1,0:T(8,128)(2,1)S(1)}, bf16[100,512]{1,0:T(8,128)(2,1)S(1)}, u32[]{:S(2)}, u32[]{:S(2)}) collective-permute-start(bf16[100,512]{1,0:T(8,128)(2,1)S(1)} %pad_maximum_fusion.2), channel_id=1, source_target_pairs={{0,8},{4,12},{8,0},{12,4},{16,24},{20,28},{24,16},{28,20},{1,9},{5... | collective-permute-start | bytes 307208 | tf_op jit(solution)/shard_map/ppermute | solution.py:480

commit v3 on v2

--- a/solution.py
+++ b/solution.py
@@ -226,25 +226,34 @@
     )(*extra, *xs, gate_w, up_w, down_w)
 
 
-def combine_kernel(slots, weights, *refs, count):
-    back, shared, out = refs[:count], refs[count:-1], refs[-1]
-    tokens = slots.shape[1]
-    own = [column(slots[k : k + 1, :]) for k in range(TOP_K)]
-    scale = [column(weights[k : k + 1, :]) for k in range(TOP_K)]
-    group = back[0].shape[0]
+def picks_kernel(slots, weights, scale, *picks):
+    tokens, width = picks[0].shape
+    at = lax.broadcasted_iota(jnp.int32, (tokens, width), 1)
+    for k, pick in enumerate(picks):
+        own = at == column(slots[k : k + 1, :])
+        pick[...] = own.astype(jnp.float32).astype(jnp.bfloat16)
+        scale[:, k : k + 1] = column(weights[k : k + 1, :])
+
+
+def finish_kernel(scale, *refs, count, sums):
+    picks, refs = refs[:TOP_K], refs[TOP_K:]
+    back, shared, refs = refs[:count], refs[count : count + 2], refs[count + 2 :]
+    out = refs[len(sums)]
+    rows = jnp.concatenate([part[...] for part in back], axis=0)
     total = jnp.concatenate([part[...] for part in shared], axis=0)
-    picked = [None] * TOP_K
-    for s in range(count):
-        slot_col = lax.broadcasted_iota(jnp.int32, (tokens, group), 1) + s * group
-        rows = back[s][...]
-        for k in range(TOP_K):
-            pick = (slot_col == own[k]).astype(jnp.float32).astype(jnp.bfloat16)
-            term = jnp.dot(pick, rows, preferred_element_type=jnp.float32)
-            picked[k] = term if picked[k] is None else picked[k] + term
-    routed = scale[0] * picked[0]
-    for k in range(1, TOP_K):
-        routed = routed + scale[k] * picked[k]
+    routed = None
+    for k, pick in enumerate(picks):
+        term = jnp.dot(pick[...], rows, preferred_element_type=jnp.float32)
+        term = scale[:, k : k + 1] * term
+        routed = term if routed is None else routed + term
     out[...] = (routed + total).astype(jnp.bfloat16)
+    if sums:
+        mixed = refs[len(sums) + 1]
+        half = mixed.shape[0] // 2
+        assert len(sums) == 6
+        for n in range(2):
+            keep, got, mid = (ref[:half, :].astype(jnp.float32) for ref in refs[3 * n : 3 * n + 3])
+            mixed[n * half : (n + 1) * half, :] = (keep + got + mid).astype(jnp.bfloat16)
 
 
 def rope_kernel(q_far, k_far, v_far, cosine, sine, *refs, size):
@@ -506,7 +515,7 @@
         own_3, other_3 = along_tp(own_1, 2), along_tp(other_2, 1)
         return [own, own_1, own_2, own_3, other, other_1, other_2, other_3]
 
-    def reduce_tp(parts):
+    def reduce_tp(parts, open_end=False):
         up = lambda x: x.astype(jnp.float32)
         if direct:
             total = sum(up(p) for p in exchange(parts, along_tp))
@@ -514,6 +523,13 @@
             return total[:half], total[half:]
         send_x, keep_x, send_y, keep_y = parts
         half = send_x.shape[0] // 2
+        if open_end:
+            far_x, far_y = along_tp(send_x[half:], 1), along_tp(send_y[half:], 2)
+            got_x, got_y = along_tp(send_x[:half], 1), along_tp(send_y[:half], 2)
+            mid_x = (up(keep_x[half:]) + up(far_x)).astype(jnp.bfloat16)
+            mid_y = (up(keep_y[half:]) + up(far_y)).astype(jnp.bfloat16)
+            mid_x, mid_y = along_tp(mid_x, 2), along_tp(mid_y, 1)
+            return [keep_x, got_x, mid_x, keep_y, got_y, mid_y]
         got_x, got_y = along_tp(send_x, 1), along_tp(send_y, 2)
         mid_x = (up(keep_x[half:]) + up(got_x[half:])).astype(jnp.bfloat16)
         mid_y = (up(keep_y[half:]) + up(got_y[half:])).astype(jnp.bfloat16)
@@ -543,6 +559,15 @@
         compiler_params=limit(8),
     )(far(moe_input), far(ffn_gain.reshape(1, -1)), far(routes.T))
     arrived = exchange(parts, along_z)
+    picks = pl.pallas_call(
+        picks_kernel,
+        out_shape=[sds((tokens, TOP_K), jnp.float32)] + [sds((tokens, ep * cap))] * TOP_K,
+        in_specs=[VM] * 2,
+        out_specs=[VM] * (1 + TOP_K),
+        cost_estimate=cost(1e8),
+        compiler_params=limit(8),
+        name="picks",
+    )(slots, route_weight.T)
 
     rows = query_pairs.shape[0]
     heads = head_lambda.shape[0]
@@ -592,6 +617,7 @@
     shared = [x[routed:] for x in summed]
     summed = [x[:routed].astype(jnp.bfloat16) for x in summed]
 
+    sums = []
     if spread:
         heads_out = pl.pallas_call(
             lambda *refs: attend_kernel(*refs, count=chips, rows=rows, size=size),
@@ -614,7 +640,8 @@
         compiler_params=limit(32),
         )(head_lambda.reshape(1, -1), head_gain.reshape(1, -1), *packs, *others)
         normed = exchange(heads_out, along_z)
-        shapes = out_shapes(rows, out_weight.shape[1] // tp, tp, direct)
+        cols = out_weight.shape[1] // tp
+        shapes = out_shapes(rows, cols, tp, direct)
         mixer = pl.pallas_call(
             lambda *refs: project_kernel(*refs, count=chips, direct=direct),
             out_shape=shapes,
@@ -625,7 +652,10 @@
             name="project",
             compiler_params=limit(12),
         )(*normed, out_weight)
-        attn_out = jnp.concatenate(reduce_tp(mixer), axis=0).astype(jnp.bfloat16)
+        sums = reduce_tp(mixer, open_end=not direct)
+        if direct:
+            attn_out = jnp.concatenate(sums, axis=0).astype(jnp.bfloat16)
+            sums = []
     else:
         head_rows = gathered_attention(query_pairs, key_pairs, value_rows, head_lambda, head_gain)[0]
         mixer = jnp.dot(head_rows, out_weight, preferred_element_type=jnp.float32)
@@ -639,15 +669,21 @@
         for s in range(chips)
     ]
     groups = exchange(groups, along_z)
-    moe_out = pl.pallas_call(
-        lambda *refs: combine_kernel(*refs, count=chips),
-        out_shape=sds((tokens, slice_width)),
-        in_specs=[VM] * (2 + chips + len(shared)),
-        out_specs=VM,
+    outs = [sds((tokens, slice_width))]
+    if sums:
+        outs.append(sds((rows, cols)))
+    finished = pl.pallas_call(
+        lambda *refs: finish_kernel(*refs, count=chips, sums=sums),
+        out_shape=outs,
+        in_specs=[VM] * (1 + TOP_K + chips + len(shared) + len(sums)),
+        out_specs=[VM] * len(outs),
         cost_estimate=cost(4e8),
-        name="combine",
-        compiler_params=limit(10),
-    )(slots, route_weight.T, *groups, *shared)
+        compiler_params=limit(12),
+        name="finish",
+    )(*picks, *groups, *shared, *sums)
+    moe_out = finished[0]
+    if sums:
+        attn_out = finished[1]
     return (attn_out, moe_out)
 
 

time: 124 us -> 124 us (level)
  starting transfers between devices: 39.8 us -> 44.2 us
  waiting for transfers between devices: 57.9 us -> 53.7 us
    ppermute x12, waiting for transfers between devices: 37 us -> 32.2 us  [along_z(): lax.ppermute(x, 'ep', [(i, 2 * (i // 2 ^ s) + i % 2) for i in range(ep)])]
    ppermute x14 -> x16, starting transfers between devices: 16.6 us -> 20.3 us  [along_tp(): return lax.ppermute(x, 'tp', [(i, i ^ s) for i in range(tp)])]
    ppermute x14 -> x16, waiting for transfers between devices: 20.4 us -> 19.8 us  [along_tp(): return lax.ppermute(x, 'tp', [(i, i ^ s) for i in range(tp)])]
  transfers between devices with their start and end apart: 32 -> 34, of which waited for: 13 -> 12; matrix products, arithmetic and copies ran while one was open for 1% -> 1% of each run, Pallas kernels for 16% -> 13%
where the time goes in v3:
time: 124 us
  waiting for transfers between devices  53.7 us (43%)
  starting transfers between devices  44.2 us (36%)
  Pallas kernels  22.8 us (18%)
  other arithmetic  1.34 us (1%)
    ppermute x12, waiting for transfers between devices, along_z(): lax.ppermute(x, 'ep', [(i, 2 * (i // 2 ^ s) + i % 2) for i in range(ep)])  32.2 us
    ppermute x12, starting transfers between devices, along_z(): lax.ppermute(x, 'ep', [(i, 2 * (i // 2 ^ s) + i % 2) for i in range(ep)])  22.7 us
    ppermute x16, starting transfers between devices, along_tp(): return lax.ppermute(x, 'tp', [(i, i ^ s) for i in range(tp)])  20.3 us
    ppermute x16, waiting for transfers between devices, along_tp(): return lax.ppermute(x, 'tp', [(i, i ^ s) for i in range(tp)])  19.8 us
    pallas_call x1, Pallas kernels, inner(): pl.pallas_call(lambda *refs: attend_kernel(*refs, count=chips, rows=rows,...  9.95 us
    pallas_call x2, Pallas kernels, run_expert(): pl.pallas_call(lambda *refs: expert_kernel(*refs, pieces=pieces, halves=h...  6.63 us
  transfers between devices with their start and end apart: 34, of which 12 were waited for; matrix products, arithmetic and copies ran while one was open for 1% of the time, Pallas kernels for 13%

profile of v3, /device:TPU:0, one launch (start us, length us, event | category | flops | bytes accessed | tf_op | source)
XLA Modules:
  0.0 123.7 jit_solution(3868579335995762688)
XLA Ops:
  0.7 0.8 fusion
  1.4 1.9 %rope.1 = (bf16[1152,128]{1,0:T(8,128)(2,1)S(1)}, bf16[1152,128]{1,0:T(8,128)(2,1)S(1)}, bf16[1152,128]{1,0:T(8,128)(2,1)S(1)}, bf16[1152,128]{1,0:T(8,128)(2,1)S(1)}) custom-call(bf16[384,512]{1,0:T(8,128)(2,1)} %refs_0_.3, bf16[384,512]{1,0:T(8,128)(2,1)} %refs_1_.3, bf16[384,512]{1,0:T(8,128)(2,1)} %refs_2_.3, f32[384,128]{1,0:T(8,128)S(1)} %get-tuple-element.75.refs_3_, ...), custom_call_target="tpu_custom_call" | custom-call | flops 400000000 | tf_op jit(solution)/shard_map/rope/pallas_call | solution.py:585
  3.4 3.1 %collective-permute-start.18 = (bf16[1152,128]{1,0:T(8,128)(2,1)S(1)}, bf16[1152,128]{1,0:T(8,128)(2,1)S(1)}, u32[]{:S(2)}, u32[]{:S(2)}) collective-permute-start(bf16[1152,128]{1,0:T(8,128)(2,1)S(1)} %get-tuple-element.47), channel_id=1, source_target_pairs={{0,8},{4,12},{8,0},{12,4},{16,24},{20,28},{24,16},{28,20},{1,9},{5... | collective-permute-start | bytes 884744 | tf_op jit(solution)/shard_map/ppermute | solution.py:489
  6.5 2.6 %collective-permute-start.19 = (bf16[1152,128]{1,0:T(8,128)(2,1)S(1)}, bf16[1152,128]{1,0:T(8,128)(2,1)S(1)}, u32[]{:S(2)}, u32[]{:S(2)}) collective-permute-start(bf16[1152,128]{1,0:T(8,128)(2,1)S(1)} %get-tuple-element.48), channel_id=1, source_target_pairs={{0,16},{4,20},{8,24},{12,28},{16,0},{20,4},{24,8},{28,12},{1,17},{... | collective-permute-start | bytes 884744 | tf_op jit(solution)/shard_map/ppermute | solution.py:489
  9.1 1.7 %dispatch.1 = (bf16[160,2048]{1,0:T(8,128)(2,1)S(1)}, s32[2,160]{1,0:T(2,128)S(1)}, bf16[100,512]{1,0:T(8,128)(2,1)S(1)}, bf16[100,512]{1,0:T(8,128)(2,1)S(1)}, ...) custom-call(bf16[160,2048]{1,0:T(8,128)(2,1)} %refs_0_.2, f32[1,2048]{1,0:T(1,128)} %bitcast.14, s32[2,160]{1,0:T(2,128)} %bitcast.15), custom_call_target="tpu_custom_call" | custom-call | flops 400000000 | tf_op jit(solution)/shard_map/dispatch/pallas_call | solution.py:545
  10.8 1.0 collective-permute-start
  11.8 3.5 %collective-permute-start.1 = (bf16[100,512]{1,0:T(8,128)(2,1)S(1)}, bf16[100,512]{1,0:T(8,128)(2,1)S(1)}, u32[]{:S(2)}, u32[]{:S(2)}) collective-permute-start(bf16[100,512]{1,0:T(8,128)(2,1)S(1)} %get-tuple-element.38), channel_id=1, source_target_pairs={{0,16},{4,20},{8,24},{12,28},{16,0},{20,4},{24,8},{28,12},{1,17},{... | collective-permute-start | bytes 307208 | tf_op jit(solution)/shard_map/ppermute | solution.py:489
  15.2 13.7 %collective-permute-done.refs_1_ = bf16[100,512]{1,0:T(8,128)(2,1)S(1)} collective-permute-done((bf16[100,512]{1,0:T(8,128)(2,1)S(1)}, bf16[100,512]{1,0:T(8,128)(2,1)S(1)}, u32[]{:S(2)}, u32[]{:S(2)}) %collective-permute-start) | collective-permute-done | bytes 102432 | tf_op jit(solution)/shard_map/ppermute | solution.py:489
  28.9 2.7 %collective-permute-start.2 = (bf16[100,512]{1,0:T(8,128)(2,1)S(1)}, bf16[100,512]{1,0:T(8,128)(2,1)S(1)}, u32[]{:S(2)}, u32[]{:S(2)}) collective-permute-start(bf16[100,512]{1,0:T(8,128)(2,1)S(1)} %get-tuple-element.39), channel_id=1, source_target_pairs={{0,24},{4,28},{8,16},{12,20},{16,8},{20,12},{24,0},{28,4},{1,25},{... | collective-permute-start | bytes 307208 | tf_op jit(solution)/shard_map/ppermute | solution.py:489
  31.6 11.3 %collective-permute-done.1.refs_2_ = bf16[100,512]{1,0:T(8,128)(2,1)S(1)} collective-permute-done((bf16[100,512]{1,0:T(8,128)(2,1)S(1)}, bf16[100,512]{1,0:T(8,128)(2,1)S(1)}, u32[]{:S(2)}, u32[]{:S(2)}) %collective-permute-start.1) | collective-permute-done | bytes 102432 | tf_op jit(solution)/shard_map/ppermute | solution.py:489
  42.9 0.5 collective-permute-start.22
  43.4 0.1 collective-permute-start.23
  43.4 0.4 collective-permute-start.24
  43.9 0.1 collective-permute-start.6
  44.1 0.4 collective-permute-done.21.refs_6_
  44.4 1.5 %collective-permute-start.3 = (bf16[200,512]{1,0:T(8,128)(2,1)S(1)}, bf16[200,512]{1,0:T(8,128)(2,1)S(1)}, u32[]{:S(2)}, u32[]{:S(2)}) collective-permute-start(bf16[200,512]{1,0:T(8,128)(2,1)S(1)} %get-tuple-element.40.refs_1_), channel_id=1, source_target_pairs={{0,1},{1,0},{2,3},{3,2},{4,5},{5,4},{6,7},{7,6},{8,9},{9,8},{10,11... | collective-permute-start | bytes 614408 | tf_op jit(solution)/shard_map/ppermute | solution.py:495
  45.9 0.1 collective-permute-done.6.refs_5_
  46.0 1.5 %collective-permute-start.8 = (bf16[200,512]{1,0:T(8,128)(2,1)S(1)}, bf16[200,512]{1,0:T(8,128)(2,1)S(1)}, u32[]{:S(2)}, u32[]{:S(2)}) collective-permute-start(bf16[200,512]{1,0:T(8,128)(2,1)S(1)} %collective-permute-done.6.refs_5_), channel_id=1, source_target_pairs={{0,2},{1,3},{2,0},{3,1},{4,6},{5,7},{6,4},{7,5},{8,10},{9,11},{10,... | collective-permute-start | bytes 614408 | tf_op jit(solution)/shard_map/ppermute | solution.py:495
  47.5 0.0 copy-start.4
  47.6 9.9 %attend.1 = (bf16[384,128]{1,0:T(8,128)(2,1)S(1)}, bf16[384,128]{1,0:T(8,128)(2,1)S(1)}, bf16[384,128]{1,0:T(8,128)(2,1)S(1)}, bf16[384,128]{1,0:T(8,128)(2,1)S(1)}) custom-call(f32[1,4]{1,0:T(1,128)S(1)} %bitcast.12, f32[1,128]{1,0:T(1,128)S(1)} %bitcast.13, bf16[1152,128]{1,0:T(8,128)(2,1)S(1)} %get-tuple-element.46.refs_2_, ...), custom_call_target="tpu_custom_call" | custom-call | flops 4000000000 | tf_op jit(solution)/shard_map/attend/pallas_call | solution.py:622
  57.5 0.3 collective-permute-start.25
  57.8 2.8 %collective-permute-start.26 = (bf16[384,128]{1,0:T(8,128)(2,1)S(1)}, bf16[384,128]{1,0:T(8,128)(2,1)S(1)}, u32[]{:S(2)}, u32[]{:S(2)}) collective-permute-start(bf16[384,128]{1,0:T(8,128)(2,1)S(1)} %get-tuple-element.52), channel_id=1, source_target_pairs={{0,16},{4,20},{8,24},{12,28},{16,0},{20,4},{24,8},{28,12},{1,17},{... | collective-permute-start | bytes 294920 | tf_op jit(solution)/shard_map/ppermute | solution.py:489
  60.6 0.5 collective-permute-start.4
  61.1 1.5 %collective-permute-start.7 = (bf16[200,512]{1,0:T(8,128)(2,1)S(1)}, bf16[200,512]{1,0:T(8,128)(2,1)S(1)}, u32[]{:S(2)}, u32[]{:S(2)}) collective-permute-start(bf16[200,512]{1,0:T(8,128)(2,1)S(1)} %collective-permute-done.6.refs_5_), channel_id=1, source_target_pairs={{0,1},{1,0},{2,3},{3,2},{4,5},{5,4},{6,7},{7,6},{8,9},{9,8},{10,11... | collective-permute-start | bytes 614408 | tf_op jit(solution)/shard_map/ppermute | solution.py:495
  62.6 1.5 %collective-permute-start.5 = (bf16[200,512]{1,0:T(8,128)(2,1)S(1)}, bf16[200,512]{1,0:T(8,128)(2,1)S(1)}, u32[]{:S(2)}, u32[]{:S(2)}) collective-permute-start(bf16[200,512]{1,0:T(8,128)(2,1)S(1)} %collective-permute-done.3.refs_2_), channel_id=1, source_target_pairs={{0,2},{1,3},{2,0},{3,1},{4,6},{5,7},{6,4},{7,5},{8,10},{9,11},{10,... | collective-permute-start | bytes 614408 | tf_op jit(solution)/shard_map/ppermute | solution.py:495
  64.2 1.4 %collective-permute-start.9 = (bf16[200,512]{1,0:T(8,128)(2,1)S(1)}, bf16[200,512]{1,0:T(8,128)(2,1)S(1)}, u32[]{:S(2)}, u32[]{:S(2)}) collective-permute-start(bf16[200,512]{1,0:T(8,128)(2,1)S(1)} %collective-permute-done.8.refs_7_), channel_id=1, source_target_pairs={{0,1},{1,0},{2,3},{3,2},{4,5},{5,4},{6,7},{7,6},{8,9},{9,8},{10,11... | collective-permute-start | bytes 614408 | tf_op jit(solution)/shard_map/ppermute | solution.py:495
  65.5 2.2 %collective-permute-start.27 = (bf16[384,128]{1,0:T(8,128)(2,1)S(1)}, bf16[384,128]{1,0:T(8,128)(2,1)S(1)}, u32[]{:S(2)}, u32[]{:S(2)}) collective-permute-start(bf16[384,128]{1,0:T(8,128)(2,1)S(1)} %get-tuple-element.53), channel_id=1, source_target_pairs={{0,24},{4,28},{8,16},{12,20},{16,8},{20,12},{24,0},{28,4},{1,25},{... | collective-permute-start | bytes 294920 | tf_op jit(solution)/shard_map/ppermute | solution.py:489
  67.8 0.2 picks.1
  68.0 0.0 copy-start
  68.0 0.0 copy-start.2
  68.0 3.6 %shard_map.167.refs_0_ = bf16[160,2048]{1,0:T(8,128)(2,1)S(1)} custom-call(bf16[160,2048]{1,0:T(8,128)(2,1)S(1)} %get-tuple-element.35.refs_0_, bf16[2048,512]{1,0:T(8,128)(2,1)} %refs_1_.2, bf16[2048,512]{1,0:T(8,128)(2,1)} %refs_2_.2, bf16[512,2048]{1,0:T(8,128)(2,1)} %refs_3_.1), custom_call_target="tpu_custom_call" | custom-call | flops 1006632960 | tf_op jit(solution)/shard_map/pallas_call | solution.py:211
  71.6 0.0 copy-start.1
  71.6 0.3 collective-permute-done.27.refs_3_
  71.9 1.0 project.1
  73.1 0.5 copy-done.1
  73.5 3.0 %shard_map.168 = (bf16[560,512]{1,0:T(8,128)(2,1)S(1)}, bf16[560,512]{1,0:T(8,128)(2,1)S(1)}, bf16[560,512]{1,0:T(8,128)(2,1)S(1)}, bf16[560,512]{1,0:T(8,128)(2,1)S(1)}) custom-call(bf16[160,2048]{1,0:T(8,128)(2,1)S(1)} %shard_map.167.refs_0_, bf16[200,512]{1,0:T(8,128)(2,1)S(1)} %get-tuple-element.40.refs_1_, ...), custom_call_target="tpu_custom_call" | custom-call | flops 2516582400 | tf_op jit(solution)/shard_map/pallas_call | solution.py:211
  76.6 0.6 collective-permute-start.12
  77.2 1.6 %collective-permute-start.28 = (bf16[192,512]{1,0:T(8,128)(2,1)S(1)}, bf16[192,512]{1,0:T(8,128)(2,1)S(1)}, u32[]{:S(2)}, u32[]{:S(2)}) collective-permute-start(bf16[192,512]{1,0:T(8,128)(2,1)S(1)} %get-tuple-element.65), channel_id=1, source_target_pairs={{0,1},{1,0},{2,3},{3,2},{4,5},{5,4},{6,7},{7,6},{8,9},{9,8},{10,11... | collective-permute-start | bytes 589832 | tf_op jit(solution)/shard_map/ppermute | solution.py:495
  78.7 0.5 collective-permute-start.29
  79.3 1.5 %collective-permute-start.10 = (bf16[560,512]{1,0:T(8,128)(2,1)S(1)}, bf16[560,512]{1,0:T(8,128)(2,1)S(1)}, u32[]{:S(2)}, u32[]{:S(2)}) collective-permute-start(bf16[560,512]{1,0:T(8,128)(2,1)S(1)} %get-tuple-element.43), channel_id=1, source_target_pairs={{0,1},{1,0},{2,3},{3,2},{4,5},{5,4},{6,7},{7,6},{8,9},{9,8},{10,11... | collective-permute-start | bytes 1720328 | tf_op jit(solution)/shard_map/ppermute | solution.py:495
  80.8 1.6 %collective-permute-start.31 = (bf16[192,512]{1,0:T(8,128)(2,1)S(1)}, bf16[192,512]{1,0:T(8,128)(2,1)S(1)}, u32[]{:S(2)}, u32[]{:S(2)}) collective-permute-start(bf16[192,512]{1,0:T(8,128)(2,1)S(1)} %get-tuple-element.63), channel_id=1, source_target_pairs={{0,2},{1,3},{2,0},{3,1},{4,6},{5,7},{6,4},{7,5},{8,10},{9,11},{10,... | collective-permute-start | bytes 589832 | tf_op jit(solution)/shard_map/ppermute | solution.py:495
  82.4 6.8 %collective-permute-done.29 = bf16[192,512]{1,0:T(8,128)(2,1)S(1)} collective-permute-done((bf16[192,512]{1,0:T(8,128)(2,1)S(1)}, bf16[192,512]{1,0:T(8,128)(2,1)S(1)}, u32[]{:S(2)}, u32[]{:S(2)}) %collective-permute-start.29) | collective-permute-done | bytes 196640 | tf_op jit(solution)/shard_map/ppermute | solution.py:495
  89.2 1.5 %collective-permute-start.32 = (bf16[192,512]{1,0:T(8,128)(2,1)S(1)}, bf16[192,512]{1,0:T(8,128)(2,1)S(1)}, u32[]{:S(2)}, u32[]{:S(2)}) collective-permute-start(bf16[192,512]{1,0:T(8,128)(2,1)S(1)} %get-tuple-element.62), channel_id=1, source_target_pairs={{0,2},{1,3},{2,0},{3,1},{4,6},{5,7},{6,4},{7,5},{8,10},{9,11},{10,... | collective-permute-start | bytes 589832 | tf_op jit(solution)/shard_map/ppermute | solution.py:495
  90.7 0.1 add_convert_fusion.3
  90.8 1.7 %collective-permute-done.12 = bf16[560,512]{1,0:T(8,128)(2,1)S(1)} collective-permute-done((bf16[560,512]{1,0:T(8,128)(2,1)S(1)}, bf16[560,512]{1,0:T(8,128)(2,1)S(1)}, u32[]{:S(2)}, u32[]{:S(2)}) %collective-permute-start.12) | collective-permute-done | bytes 573472 | tf_op jit(solution)/shard_map/ppermute | solution.py:495
  92.5 0.5 collective-permute-start.30
  93.0 0.1 add_convert_fusion
  93.1 5.7 %collective-permute-done.10 = bf16[560,512]{1,0:T(8,128)(2,1)S(1)} collective-permute-done((bf16[560,512]{1,0:T(8,128)(2,1)S(1)}, bf16[560,512]{1,0:T(8,128)(2,1)S(1)}, u32[]{:S(2)}, u32[]{:S(2)}) %collective-permute-start.10) | collective-permute-done | bytes 573472 | tf_op jit(solution)/shard_map/ppermute | solution.py:495
  98.8 1.5 %collective-permute-start.13 = (bf16[280,512]{1,0:T(8,128)(2,1)S(1)}, bf16[280,512]{1,0:T(8,128)(2,1)S(1)}, u32[]{:S(2)}, u32[]{:S(2)}) collective-permute-start(bf16[280,512]{1,0:T(8,128)(2,1)S(1)} %add_convert_fusion), channel_id=1, source_target_pairs={{0,1},{1,0},{2,3},{3,2},{4,5},{5,4},{6,7},{7,6},{8,9},{9,8},{10,11... | collective-permute-start | bytes 860168 | tf_op jit(solution)/shard_map/ppermute | solution.py:495
  100.3 0.1 add_convert_fusion.1
  100.4 1.6 %collective-permute-start.11 = (bf16[280,512]{1,0:T(8,128)(2,1)S(1)}, bf16[280,512]{1,0:T(8,128)(2,1)S(1)}, u32[]{:S(2)}, u32[]{:S(2)}) collective-permute-start(bf16[280,512]{1,0:T(8,128)(2,1)S(1)} %add_convert_fusion.1), channel_id=1, source_target_pairs={{0,2},{1,3},{2,0},{3,1},{4,6},{5,7},{6,4},{7,5},{8,10},{9,11},{10,... | collective-permute-start | bytes 860168 | tf_op jit(solution)/shard_map/ppermute | solution.py:495
  102.0 0.1 add_convert_fusion.2
  102.1 5.5 %collective-permute-done.13 = bf16[280,512]{1,0:T(8,128)(2,1)S(1)} collective-permute-done((bf16[280,512]{1,0:T(8,128)(2,1)S(1)}, bf16[280,512]{1,0:T(8,128)(2,1)S(1)}, u32[]{:S(2)}, u32[]{:S(2)}) %collective-permute-start.13) | collective-permute-done | bytes 286752 | tf_op jit(solution)/shard_map/ppermute | solution.py:495
  107.6 1.5 %collective-permute-start.33 = (bf16[192,512]{1,0:T(8,128)(2,1)S(1)}, bf16[192,512]{1,0:T(8,128)(2,1)S(1)}, u32[]{:S(2)}, u32[]{:S(2)}) collective-permute-start(bf16[192,512]{1,0:T(8,128)(2,1)S(1)} %add_convert_fusion.2), channel_id=1, source_target_pairs={{0,1},{1,0},{2,3},{3,2},{4,5},{5,4},{6,7},{7,6},{8,9},{9,8},{10,11... | collective-permute-start | bytes 589832 | tf_op jit(solution)/shard_map/ppermute | solution.py:495
  109.1 0.1 convert_add_fusion
  109.2 0.1 collective-permute-start.14
  109.3 0.1 fusion.6
  109.5 1.2 %collective-permute-done.14 = bf16[200,512]{1,0:T(8,128)(2,1)S(1)} collective-permute-done((bf16[200,512]{1,0:T(8,128)(2,1)S(1)}, bf16[200,512]{1,0:T(8,128)(2,1)S(1)}, u32[]{:S(2)}, u32[]{:S(2)}) %collective-permute-start.14) | collective-permute-done | bytes 204832 | tf_op jit(solution)/shard_map/ppermute | solution.py:492
  110.8 0.1 collective-permute-start.15
  111.0 2.4 %collective-permute-start.16 = (bf16[100,512]{1,0:T(8,128)(2,1)S(1)}, bf16[100,512]{1,0:T(8,128)(2,1)S(1)}, u32[]{:S(2)}, u32[]{:S(2)}) collective-permute-start(bf16[100,512]{1,0:T(8,128)(2,1)S(1)} %pad_maximum_fusion.2), channel_id=1, source_target_pairs={{0,16},{4,20},{8,24},{12,28},{16,0},{20,4},{24,8},{28,12},{1,17},{... | collective-permute-start | bytes 307208 | tf_op jit(solution)/shard_map/ppermute | solution.py:489
  113.3 2.1 %collective-permute-start.17 = (bf16[100,512]{1,0:T(8,128)(2,1)S(1)}, bf16[100,512]{1,0:T(8,128)(2,1)S(1)}, u32[]{:S(2)}, u32[]{:S(2)}) collective-permute-start(bf16[100,512]{1,0:T(8,128)(2,1)S(1)} %pad_maximum_fusion.3), channel_id=1, source_target_pairs={{0,24},{4,28},{8,16},{12,20},{16,8},{20,12},{24,0},{28,4},{1,25},{... | collective-permute-start | bytes 307208 | tf_op jit(solution)/shard_map/ppermute | solution.py:489
  115.5 1.7 %collective-permute-done.15.refs_4_ = bf16[100,512]{1,0:T(8,128)(2,1)S(1)} collective-permute-done((bf16[100,512]{1,0:T(8,128)(2,1)S(1)}, bf16[100,512]{1,0:T(8,128)(2,1)S(1)}, u32[]{:S(2)}, u32[]{:S(2)}) %collective-permute-start.15) | collective-permute-done | bytes 102432 | tf_op jit(solution)/shard_map/ppermute | solution.py:489
  117.2 5.2 %collective-permute-done.16.refs_5_ = bf16[100,512]{1,0:T(8,128)(2,1)S(1)} collective-permute-done((bf16[100,512]{1,0:T(8,128)(2,1)S(1)}, bf16[100,512]{1,0:T(8,128)(2,1)S(1)}, u32[]{:S(2)}, u32[]{:S(2)}) %collective-permute-start.16) | collective-permute-done | bytes 102432 | tf_op jit(solution)/shard_map/ppermute | solution.py:489
  122.4 1.3 %finish.1 = (bf16[160,512]{1,0:T(8,128)(2,1)}, bf16[384,512]{1,0:T(8,128)(2,1)}) custom-call(f32[160,2]{1,0:T(8,128)S(1)} %get-tuple-element.32.refs_0_, bf16[160,400]{1,0:T(8,128)(2,1)S(1)} %get-tuple-element.33.refs_1_, bf16[160,400]{1,0:T(8,128)(2,1)S(1)} %get-tuple-element.34.refs_2_, bf16[100,512]{1,0:T(8,128)(2,1)S(1)} %pad_maximum_fusion.refs_3_, ...), custom_call_target="tpu_custom_call" | custom-call | flops 400000000 | tf_op jit(solution)/shard_map/finish/pallas_call | solution.py:675
  (47 shorter events, 0.4 us)
Async XLA Ops:
  0.6 46.9 %copy-start.5 = (f32[4]{0:T(128)S(1)}, f32[4]{0:T(128)}, u32[]{:S(2)}) copy-start(f32[4]{0:T(128)} %param.19) | copy-start | bytes 52
  0.6 46.9 %copy-start.6 = (f32[128]{0:T(128)S(1)}, f32[128]{0:T(128)}, u32[]{:S(2)}) copy-start(f32[128]{0:T(128)} %param.20) | copy-start | bytes 1540
  3.4 39.5 %collective-permute-start.18 = (bf16[1152,128]{1,0:T(8,128)(2,1)S(1)}, bf16[1152,128]{1,0:T(8,128)(2,1)S(1)}, u32[]{:S(2)}, u32[]{:S(2)}) collective-permute-start(bf16[1152,128]{1,0:T(8,128)(2,1)S(1)} %get-tuple-element.47), channel_id=1, source_target_pairs={{0,8},{4,12},{8,0},{12,4},{16,24},{20,28},{24,16},{28,20},{1,9},{5... | collective-permute-start | bytes 884744 | tf_op jit(solution)/shard_map/ppermute | solution.py:489
  6.5 36.9 %collective-permute-start.19 = (bf16[1152,128]{1,0:T(8,128)(2,1)S(1)}, bf16[1152,128]{1,0:T(8,128)(2,1)S(1)}, u32[]{:S(2)}, u32[]{:S(2)}) collective-permute-start(bf16[1152,128]{1,0:T(8,128)(2,1)S(1)} %get-tuple-element.48), channel_id=1, source_target_pairs={{0,16},{4,20},{8,24},{12,28},{16,0},{20,4},{24,8},{28,12},{1,17},{... | collective-permute-start | bytes 884744 | tf_op jit(solution)/shard_map/ppermute | solution.py:489
  9.1 34.4 %collective-permute-start.20 = (bf16[1152,128]{1,0:T(8,128)(2,1)S(1)}, bf16[1152,128]{1,0:T(8,128)(2,1)S(1)}, u32[]{:S(2)}, u32[]{:S(2)}) collective-permute-start(bf16[1152,128]{1,0:T(8,128)(2,1)S(1)} %get-tuple-element.49), channel_id=1, source_target_pairs={{0,24},{4,28},{8,16},{12,20},{16,8},{20,12},{24,0},{28,4},{1,25},{... | collective-permute-start | bytes 884744 | tf_op jit(solution)/shard_map/ppermute | solution.py:489
  10.8 18.1 %collective-permute-start = (bf16[100,512]{1,0:T(8,128)(2,1)S(1)}, bf16[100,512]{1,0:T(8,128)(2,1)S(1)}, u32[]{:S(2)}, u32[]{:S(2)}) collective-permute-start(bf16[100,512]{1,0:T(8,128)(2,1)S(1)} %get-tuple-element.37), channel_id=1, source_target_pairs={{0,8},{4,12},{8,0},{12,4},{16,24},{20,28},{24,16},{28,20},{1,9},{5... | collective-permute-start | bytes 307208 | tf_op jit(solution)/shard_map/ppermute | solution.py:489
  11.8 31.1 %collective-permute-start.1 = (bf16[100,512]{1,0:T(8,128)(2,1)S(1)}, bf16[100,512]{1,0:T(8,128)(2,1)S(1)}, u32[]{:S(2)}, u32[]{:S(2)}) collective-permute-start(bf16[100,512]{1,0:T(8,128)(2,1)S(1)} %get-tuple-element.38), channel_id=1, source_target_pairs={{0,16},{4,20},{8,24},{12,28},{16,0},{20,4},{24,8},{28,12},{1,17},{... | collective-permute-start | bytes 307208 | tf_op jit(solution)/shard_map/ppermute | solution.py:489
  28.9 15.0 %collective-permute-start.2 = (bf16[100,512]{1,0:T(8,128)(2,1)S(1)}, bf16[100,512]{1,0:T(8,128)(2,1)S(1)}, u32[]{:S(2)}, u32[]{:S(2)}) collective-permute-start(bf16[100,512]{1,0:T(8,128)(2,1)S(1)} %get-tuple-element.39), channel_id=1, source_target_pairs={{0,24},{4,28},{8,16},{12,20},{16,8},{20,12},{24,0},{28,4},{1,25},{... | collective-permute-start | bytes 307208 | tf_op jit(solution)/shard_map/ppermute | solution.py:489
  42.9 1.6 %collective-permute-start.21 = (bf16[1152,128]{1,0:T(8,128)(2,1)S(1)}, bf16[1152,128]{1,0:T(8,128)(2,1)S(1)}, u32[]{:S(2)}, u32[]{:S(2)}) collective-permute-start(bf16[1152,128]{1,0:T(8,128)(2,1)S(1)} %get-tuple-element.46.refs_2_), channel_id=1, source_target_pairs={{0,4},{4,0},{8,12},{12,8},{16,20},{20,16},{24,28},{28,24},{1,5},{5... | collective-permute-start | bytes 884744 | tf_op jit(solution)/shard_map/ppermute | solution.py:492
  42.9 4.7 %collective-permute-start.22 = (bf16[1152,128]{1,0:T(8,128)(2,1)S(1)}, bf16[1152,128]{1,0:T(8,128)(2,1)S(1)}, u32[]{:S(2)}, u32[]{:S(2)}) collective-permute-start(bf16[1152,128]{1,0:T(8,128)(2,1)S(1)} %collective-permute-done.18.refs_3_), channel_id=1, source_target_pairs={{0,4},{4,0},{8,12},{12,8},{16,20},{20,16},{24,28},{28,24},{1,5},{5... | collective-permute-start | bytes 884744 | tf_op jit(solution)/shard_map/ppermute | solution.py:492
  43.4 4.1 %collective-permute-start.23 = (bf16[1152,128]{1,0:T(8,128)(2,1)S(1)}, bf16[1152,128]{1,0:T(8,128)(2,1)S(1)}, u32[]{:S(2)}, u32[]{:S(2)}) collective-permute-start(bf16[1152,128]{1,0:T(8,128)(2,1)S(1)} %collective-permute-done.19.refs_4_), channel_id=1, source_target_pairs={{0,4},{4,0},{8,12},{12,8},{16,20},{20,16},{24,28},{28,24},{1,5},{5... | collective-permute-start | bytes 884744 | tf_op jit(solution)/shard_map/ppermute | solution.py:492
  43.4 4.1 %collective-permute-start.24 = (bf16[1152,128]{1,0:T(8,128)(2,1)S(1)}, bf16[1152,128]{1,0:T(8,128)(2,1)S(1)}, u32[]{:S(2)}, u32[]{:S(2)}) collective-permute-start(bf16[1152,128]{1,0:T(8,128)(2,1)S(1)} %collective-permute-done.20.refs_5_), channel_id=1, source_target_pairs={{0,4},{4,0},{8,12},{12,8},{16,20},{20,16},{24,28},{28,24},{1,5},{5... | collective-permute-start | bytes 884744 | tf_op jit(solution)/shard_map/ppermute | solution.py:492
  43.9 2.1 %collective-permute-start.6 = (bf16[200,512]{1,0:T(8,128)(2,1)S(1)}, bf16[200,512]{1,0:T(8,128)(2,1)S(1)}, u32[]{:S(2)}, u32[]{:S(2)}) collective-permute-start(bf16[200,512]{1,0:T(8,128)(2,1)S(1)} %get-tuple-element.41), channel_id=1, source_target_pairs={{0,4},{4,0},{8,12},{12,8},{16,20},{20,16},{24,28},{28,24},{1,5},{5... | collective-permute-start | bytes 614408 | tf_op jit(solution)/shard_map/ppermute | solution.py:492
  44.4 16.7 %collective-permute-start.3 = (bf16[200,512]{1,0:T(8,128)(2,1)S(1)}, bf16[200,512]{1,0:T(8,128)(2,1)S(1)}, u32[]{:S(2)}, u32[]{:S(2)}) collective-permute-start(bf16[200,512]{1,0:T(8,128)(2,1)S(1)} %get-tuple-element.40.refs_1_), channel_id=1, source_target_pairs={{0,1},{1,0},{2,3},{3,2},{4,5},{5,4},{6,7},{7,6},{8,9},{9,8},{10,11... | collective-permute-start | bytes 614408 | tf_op jit(solution)/shard_map/ppermute | solution.py:495
  46.0 16.6 %collective-permute-start.8 = (bf16[200,512]{1,0:T(8,128)(2,1)S(1)}, bf16[200,512]{1,0:T(8,128)(2,1)S(1)}, u32[]{:S(2)}, u32[]{:S(2)}) collective-permute-start(bf16[200,512]{1,0:T(8,128)(2,1)S(1)} %collective-permute-done.6.refs_5_), channel_id=1, source_target_pairs={{0,2},{1,3},{2,0},{3,1},{4,6},{5,7},{6,4},{7,5},{8,10},{9,11},{10,... | collective-permute-start | bytes 614408 | tf_op jit(solution)/shard_map/ppermute | solution.py:495
  47.5 20.2 %copy-start.4 = (f32[160,2]{0,1:T(2,128)S(1)}, f32[160,2]{0,1:T(2,128)}, u32[]{:S(2)}) copy-start(f32[160,2]{0,1:T(2,128)} %param.25) | copy-start | bytes 3844
  57.5 6.6 %collective-permute-start.25 = (bf16[384,128]{1,0:T(8,128)(2,1)S(1)}, bf16[384,128]{1,0:T(8,128)(2,1)S(1)}, u32[]{:S(2)}, u32[]{:S(2)}) collective-permute-start(bf16[384,128]{1,0:T(8,128)(2,1)S(1)} %get-tuple-element.51), channel_id=1, source_target_pairs={{0,8},{4,12},{8,0},{12,4},{16,24},{20,28},{24,16},{28,20},{1,9},{5... | collective-permute-start | bytes 294920 | tf_op jit(solution)/shard_map/ppermute | solution.py:489
  57.8 7.7 %collective-permute-start.26 = (bf16[384,128]{1,0:T(8,128)(2,1)S(1)}, bf16[384,128]{1,0:T(8,128)(2,1)S(1)}, u32[]{:S(2)}, u32[]{:S(2)}) collective-permute-start(bf16[384,128]{1,0:T(8,128)(2,1)S(1)} %get-tuple-element.52), channel_id=1, source_target_pairs={{0,16},{4,20},{8,24},{12,28},{16,0},{20,4},{24,8},{28,12},{1,17},{... | collective-permute-start | bytes 294920 | tf_op jit(solution)/shard_map/ppermute | solution.py:489
  60.6 12.4 %collective-permute-start.4 = (bf16[200,512]{1,0:T(8,128)(2,1)S(1)}, bf16[200,512]{1,0:T(8,128)(2,1)S(1)}, u32[]{:S(2)}, u32[]{:S(2)}) collective-permute-start(bf16[200,512]{1,0:T(8,128)(2,1)S(1)} %get-tuple-element.40.refs_1_), channel_id=1, source_target_pairs={{0,2},{1,3},{2,0},{3,1},{4,6},{5,7},{6,4},{7,5},{8,10},{9,11},{10,... | collective-permute-start | bytes 614408 | tf_op jit(solution)/shard_map/ppermute | solution.py:495
  61.1 11.9 %collective-permute-start.7 = (bf16[200,512]{1,0:T(8,128)(2,1)S(1)}, bf16[200,512]{1,0:T(8,128)(2,1)S(1)}, u32[]{:S(2)}, u32[]{:S(2)}) collective-permute-start(bf16[200,512]{1,0:T(8,128)(2,1)S(1)} %collective-permute-done.6.refs_5_), channel_id=1, source_target_pairs={{0,1},{1,0},{2,3},{3,2},{4,5},{5,4},{6,7},{7,6},{8,9},{9,8},{10,11... | collective-permute-start | bytes 614408 | tf_op jit(solution)/shard_map/ppermute | solution.py:495
  62.6 10.4 %collective-permute-start.5 = (bf16[200,512]{1,0:T(8,128)(2,1)S(1)}, bf16[200,512]{1,0:T(8,128)(2,1)S(1)}, u32[]{:S(2)}, u32[]{:S(2)}) collective-permute-start(bf16[200,512]{1,0:T(8,128)(2,1)S(1)} %collective-permute-done.3.refs_2_), channel_id=1, source_target_pairs={{0,2},{1,3},{2,0},{3,1},{4,6},{5,7},{6,4},{7,5},{8,10},{9,11},{10,... | collective-permute-start | bytes 614408 | tf_op jit(solution)/shard_map/ppermute | solution.py:495
  64.2 8.9 %collective-permute-start.9 = (bf16[200,512]{1,0:T(8,128)(2,1)S(1)}, bf16[200,512]{1,0:T(8,128)(2,1)S(1)}, u32[]{:S(2)}, u32[]{:S(2)}) collective-permute-start(bf16[200,512]{1,0:T(8,128)(2,1)S(1)} %collective-permute-done.8.refs_7_), channel_id=1, source_target_pairs={{0,1},{1,0},{2,3},{3,2},{4,5},{5,4},{6,7},{7,6},{8,9},{9,8},{10,11... | collective-permute-start | bytes 614408 | tf_op jit(solution)/shard_map/ppermute | solution.py:495
  65.5 6.4 %collective-permute-start.27 = (bf16[384,128]{1,0:T(8,128)(2,1)S(1)}, bf16[384,128]{1,0:T(8,128)(2,1)S(1)}, u32[]{:S(2)}, u32[]{:S(2)}) collective-permute-start(bf16[384,128]{1,0:T(8,128)(2,1)S(1)} %get-tuple-element.53), channel_id=1, source_target_pairs={{0,24},{4,28},{8,16},{12,20},{16,8},{20,12},{24,0},{28,4},{1,25},{... | collective-permute-start | bytes 294920 | tf_op jit(solution)/shard_map/ppermute | solution.py:489
  68.0 4.0 %copy-start = (bf16[512,2048]{1,0:T(8,128)(2,1)S(1)}, bf16[512,2048]{1,0:T(8,128)(2,1)}, u32[]{:S(2)}) copy-start(bf16[512,2048]{1,0:T(8,128)(2,1)} %refs_4_.1) | copy-start | bytes 6291460
  68.0 5.0 %copy-start.2 = (bf16[1,2048,512]{2,1,0:T(8,128)(2,1)S(1)}, bf16[1,2048,512]{2,1,0:T(8,128)(2,1)}, u32[]{:S(2)}) copy-start(bf16[1,2048,512]{2,1,0:T(8,128)(2,1)} %param.27) | copy-start | bytes 6291460
  68.0 5.0 %copy-start.3 = (bf16[1,512,2048]{2,1,0:T(8,128)(2,1)S(1)}, bf16[1,512,2048]{2,1,0:T(8,128)(2,1)}, u32[]{:S(2)}) copy-start(bf16[1,512,2048]{2,1,0:T(8,128)(2,1)} %param.28) | copy-start | bytes 6291460
  71.6 1.9 %copy-start.1 = (bf16[1,2048,512]{2,1,0:T(8,128)(2,1)S(1)}, bf16[1,2048,512]{2,1,0:T(8,128)(2,1)}, u32[]{:S(2)}) copy-start(bf16[1,2048,512]{2,1,0:T(8,128)(2,1)} %param.26) | copy-start | bytes 6291460
  76.6 15.9 %collective-permute-start.12 = (bf16[560,512]{1,0:T(8,128)(2,1)S(1)}, bf16[560,512]{1,0:T(8,128)(2,1)S(1)}, u32[]{:S(2)}, u32[]{:S(2)}) collective-permute-start(bf16[560,512]{1,0:T(8,128)(2,1)S(1)} %get-tuple-element.45), channel_id=1, source_target_pairs={{0,2},{1,3},{2,0},{3,1},{4,6},{5,7},{6,4},{7,5},{8,10},{9,11},{10,... | collective-permute-start | bytes 1720328 | tf_op jit(solution)/shard_map/ppermute | solution.py:495
  77.2 33.8 %collective-permute-start.28 = (bf16[192,512]{1,0:T(8,128)(2,1)S(1)}, bf16[192,512]{1,0:T(8,128)(2,1)S(1)}, u32[]{:S(2)}, u32[]{:S(2)}) collective-permute-start(bf16[192,512]{1,0:T(8,128)(2,1)S(1)} %get-tuple-element.65), channel_id=1, source_target_pairs={{0,1},{1,0},{2,3},{3,2},{4,5},{5,4},{6,7},{7,6},{8,9},{9,8},{10,11... | collective-permute-start | bytes 589832 | tf_op jit(solution)/shard_map/ppermute | solution.py:495
  78.7 10.5 %collective-permute-start.29 = (bf16[192,512]{1,0:T(8,128)(2,1)S(1)}, bf16[192,512]{1,0:T(8,128)(2,1)S(1)}, u32[]{:S(2)}, u32[]{:S(2)}) collective-permute-start(bf16[192,512]{1,0:T(8,128)(2,1)S(1)} %get-tuple-element.64), channel_id=1, source_target_pairs={{0,1},{1,0},{2,3},{3,2},{4,5},{5,4},{6,7},{7,6},{8,9},{9,8},{10,11... | collective-permute-start | bytes 589832 | tf_op jit(solution)/shard_map/ppermute | solution.py:495
  79.3 19.5 %collective-permute-start.10 = (bf16[560,512]{1,0:T(8,128)(2,1)S(1)}, bf16[560,512]{1,0:T(8,128)(2,1)S(1)}, u32[]{:S(2)}, u32[]{:S(2)}) collective-permute-start(bf16[560,512]{1,0:T(8,128)(2,1)S(1)} %get-tuple-element.43), channel_id=1, source_target_pairs={{0,1},{1,0},{2,3},{3,2},{4,5},{5,4},{6,7},{7,6},{8,9},{9,8},{10,11... | collective-permute-start | bytes 1720328 | tf_op jit(solution)/shard_map/ppermute | solution.py:495
  80.8 32.5 %collective-permute-start.31 = (bf16[192,512]{1,0:T(8,128)(2,1)S(1)}, bf16[192,512]{1,0:T(8,128)(2,1)S(1)}, u32[]{:S(2)}, u32[]{:S(2)}) collective-permute-start(bf16[192,512]{1,0:T(8,128)(2,1)S(1)} %get-tuple-element.63), channel_id=1, source_target_pairs={{0,2},{1,3},{2,0},{3,1},{4,6},{5,7},{6,4},{7,5},{8,10},{9,11},{10,... | collective-permute-start | bytes 589832 | tf_op jit(solution)/shard_map/ppermute | solution.py:495
  89.2 11.2 %collective-permute-start.32 = (bf16[192,512]{1,0:T(8,128)(2,1)S(1)}, bf16[192,512]{1,0:T(8,128)(2,1)S(1)}, u32[]{:S(2)}, u32[]{:S(2)}) collective-permute-start(bf16[192,512]{1,0:T(8,128)(2,1)S(1)} %get-tuple-element.62), channel_id=1, source_target_pairs={{0,2},{1,3},{2,0},{3,1},{4,6},{5,7},{6,4},{7,5},{8,10},{9,11},{10,... | collective-permute-start | bytes 589832 | tf_op jit(solution)/shard_map/ppermute | solution.py:495
  92.5 22.9 %collective-permute-start.30 = (bf16[192,512]{1,0:T(8,128)(2,1)S(1)}, bf16[192,512]{1,0:T(8,128)(2,1)S(1)}, u32[]{:S(2)}, u32[]{:S(2)}) collective-permute-start(bf16[192,512]{1,0:T(8,128)(2,1)S(1)} %add_convert_fusion.3), channel_id=1, source_target_pairs={{0,2},{1,3},{2,0},{3,1},{4,6},{5,7},{6,4},{7,5},{8,10},{9,11},{10,... | collective-permute-start | bytes 589832 | tf_op jit(solution)/shard_map/ppermute | solution.py:495
  98.8 8.7 %collective-permute-start.13 = (bf16[280,512]{1,0:T(8,128)(2,1)S(1)}, bf16[280,512]{1,0:T(8,128)(2,1)S(1)}, u32[]{:S(2)}, u32[]{:S(2)}) collective-permute-start(bf16[280,512]{1,0:T(8,128)(2,1)S(1)} %add_convert_fusion), channel_id=1, source_target_pairs={{0,1},{1,0},{2,3},{3,2},{4,5},{5,4},{6,7},{7,6},{8,9},{9,8},{10,11... | collective-permute-start | bytes 860168 | tf_op jit(solution)/shard_map/ppermute | solution.py:495
  100.4 8.8 %collective-permute-start.11 = (bf16[280,512]{1,0:T(8,128)(2,1)S(1)}, bf16[280,512]{1,0:T(8,128)(2,1)S(1)}, u32[]{:S(2)}, u32[]{:S(2)}) collective-permute-start(bf16[280,512]{1,0:T(8,128)(2,1)S(1)} %add_convert_fusion.1), channel_id=1, source_target_pairs={{0,2},{1,3},{2,0},{3,1},{4,6},{5,7},{6,4},{7,5},{8,10},{9,11},{10,... | collective-permute-start | bytes 860168 | tf_op jit(solution)/shard_map/ppermute | solution.py:495
  107.6 7.9 %collective-permute-start.33 = (bf16[192,512]{1,0:T(8,128)(2,1)S(1)}, bf16[192,512]{1,0:T(8,128)(2,1)S(1)}, u32[]{:S(2)}, u32[]{:S(2)}) collective-permute-start(bf16[192,512]{1,0:T(8,128)(2,1)S(1)} %add_convert_fusion.2), channel_id=1, source_target_pairs={{0,1},{1,0},{2,3},{3,2},{4,5},{5,4},{6,7},{7,6},{8,9},{9,8},{10,11... | collective-permute-start | bytes 589832 | tf_op jit(solution)/shard_map/ppermute | solution.py:495
  109.2 1.5 %collective-permute-start.14 = (bf16[200,512]{1,0:T(8,128)(2,1)S(1)}, bf16[200,512]{1,0:T(8,128)(2,1)S(1)}, u32[]{:S(2)}, u32[]{:S(2)}) collective-permute-start(bf16[200,512]{1,0:T(8,128)(2,1)S(1)} %slice.133), channel_id=1, source_target_pairs={{0,4},{4,0},{8,12},{12,8},{16,20},{20,16},{24,28},{28,24},{1,5},{5... | collective-permute-start | bytes 614408 | tf_op jit(solution)/shard_map/ppermute | solution.py:492
  110.8 6.4 %collective-permute-start.15 = (bf16[100,512]{1,0:T(8,128)(2,1)S(1)}, bf16[100,512]{1,0:T(8,128)(2,1)S(1)}, u32[]{:S(2)}, u32[]{:S(2)}) collective-permute-start(bf16[100,512]{1,0:T(8,128)(2,1)S(1)} %pad_maximum_fusion.1), channel_id=1, source_target_pairs={{0,8},{4,12},{8,0},{12,4},{16,24},{20,28},{24,16},{28,20},{1,9},{5... | collective-permute-start | bytes 307208 | tf_op jit(solution)/shard_map/ppermute | solution.py:489
  111.0 11.4 %collective-permute-start.16 = (bf16[100,512]{1,0:T(8,128)(2,1)S(1)}, bf16[100,512]{1,0:T(8,128)(2,1)S(1)}, u32[]{:S(2)}, u32[]{:S(2)}) collective-permute-start(bf16[100,512]{1,0:T(8,128)(2,1)S(1)} %pad_maximum_fusion.2), channel_id=1, source_target_pairs={{0,16},{4,20},{8,24},{12,28},{16,0},{20,4},{24,8},{28,12},{1,17},{... | collective-permute-start | bytes 307208 | tf_op jit(solution)/shard_map/ppermute | solution.py:489
  113.3 9.1 %collective-permute-start.17 = (bf16[100,512]{1,0:T(8,128)(2,1)S(1)}, bf16[100,512]{1,0:T(8,128)(2,1)S(1)}, u32[]{:S(2)}, u32[]{:S(2)}) collective-permute-start(bf16[100,512]{1,0:T(8,128)(2,1)S(1)} %pad_maximum_fusion.3), channel_id=1, source_target_pairs={{0,24},{4,28},{8,16},{12,20},{16,8},{20,12},{24,0},{28,4},{1,25},{... | collective-permute-start | bytes 307208 | tf_op jit(solution)/shard_map/ppermute | solution.py:489
